TPU v7x, 256 devices: a 2x2x32 block of a 4x8x32 slice. The times are simulated.
256 devices in a mesh: grp: 4 (over y, x), tp: 64 (over z, core).
Axes of the slice: x: 2, y: 2, z: 32, core: 2. Of those that a mesh axis runs over, the one named last changes fastest.
The devices are a block of a 4x8x32 slice.
Arguments:
- tokens: bfloat16 [256, 2048], P('grp'), parts along dimension 0, may hold values from -6 to 6
- norm_gain: float32 [2, 2048], replicated, may hold values from 0.1 to 1.9
- query_weight: bfloat16 [2, 2048, 2048], P(None, 'tp'), may hold values from -0.125 to 0.125
- key_weight: bfloat16 [2, 2048, 2048], P(None, 'tp'), may hold values from -0.125 to 0.125
- value_weight: bfloat16 [2, 2048, 2048], P(None, 'tp'), may hold values from -0.125 to 0.125
- outgate_weight: bfloat16 [2, 2048, 2048], P(None, 'tp'), may hold values from -0.125 to 0.125
- gate_weight: bfloat16 [2, 2048, 16], replicated, may hold values from -0.125 to 0.125
- forget_bias: float32 [2, 8], replicated, may hold values from 0 to 4
- proj_weight: bfloat16 [2, 2048, 2048], P(None, 'tp'), may hold values from -0.125 to 0.125
- cell_state: float32 [2, 256, 2048, 256], P(None, 'grp', 'tp'), parts along dimension 1, may hold values from -0.3 to 0.3
- normalizer: float32 [2, 256, 2048], P(None, 'grp', 'tp'), parts along dimension 1, may hold values from -0.3 to 0.3
- stabilizer: float32 [2, 256, 8], P(None, 'grp'), parts along dimension 1, may hold values from -2 to 2
Outputs:
- mixed: bfloat16 [256, 2048], P('grp', 'tp'), parts along dimension 0
- new_cell: float32 [2, 256, 2048, 256], P(None, 'grp', 'tp'), parts along dimension 1
- new_normalizer: float32 [2, 256, 2048], P(None, 'grp', 'tp'), parts along dimension 1
- new_stabilizer: float32 [2, 256, 8], P(None, 'grp'), parts along dimension 1
There are 4 independent parts, one for each index of `grp`. A program takes and returns all parts, laid end to end along the dimension named above; an argument that names none is the same for every part. Nothing has to cross between parts.
All inputs are finite; a program needn't handle non-finite values.
Results may differ from a plain program's by a relative error of at most 0.025.
Values may be sent and summed in bfloat16 or wider, within the bound.
No kernel may reach another device: no remote copies, remote signals or barrier semaphores. Data moves between devices by JAX's collectives and lax.ppermute only.
A program may use at most 64 MiB of HBM per device.

v0:
```python
import jax
import jax.numpy as jnp
from jax import lax
from jax.sharding import PartitionSpec as P

D = 2048
DH = 256
LAYERS = 2


epsilon = 1e-06


def from_partner(value, axis, apart):
    mask = 2**apart
    pairs = [(source, source ^ mask) for source in range(lax.axis_size(axis))]
    return lax.ppermute(value, axis, pairs)


def sent_to_all(shard, axis):
    length = lax.axis_size(axis)
    return lax.all_to_all(
        jnp.broadcast_to(shard[None], (length, *shard.shape)), axis, 0, 0, tiled=True
    )


def in_order(blocks, dim):
    blocks = jnp.moveaxis(blocks, 0, dim)
    dims = blocks.shape
    return blocks.reshape(*dims[:dim], dims[dim] * dims[dim + 1], *dims[dim + 2 :])


def gathered_copies(shard, axis, dim):
    blocks = sent_to_all(shard, axis)
    return in_order(blocks, dim)


def project(normed, weight):
    return lax.dot_general(
        normed, weight, (((1,), (1,)), ((), ())), preferred_element_type=jnp.float32
    )


def combine_halves(mine, theirs, lower):
    return jnp.where(
        lower, jnp.concatenate([mine, theirs], axis=1), jnp.concatenate([theirs, mine], axis=1)
    )


def one_cell(
    current,
    gain,
    w_query,
    w_key,
    w_value,
    w_outgate,
    w_gates,
    bias_forget,
    w_proj,
    cell,
    norm_vec,
    stab,
):
    heads = D // DH
    ncols = w_query.shape[0]
    group = DH // ncols
    device = lax.axis_index("tp")
    head = device // group
    cur_f = current.astype(jnp.float32)
    normed = (
        cur_f * lax.rsqrt(jnp.mean(cur_f * cur_f, axis=-1, keepdims=True) + epsilon) * gain
    ).astype(jnp.bfloat16)
    query = project(normed, w_query).astype(jnp.bfloat16)
    keys = (project(normed, w_key) * DH ** (-0.5)).astype(jnp.bfloat16)
    values = project(normed, w_value).astype(jnp.bfloat16)
    outgate = project(normed, w_outgate).astype(jnp.bfloat16)
    gates = jnp.dot(normed, w_gates, preferred_element_type=jnp.float32)
    in_gate = gates[:, :heads]
    log_forget = jax.nn.log_sigmoid(gates[:, heads:] + bias_forget)
    new_stab = jnp.maximum(log_forget + stab, in_gate)
    decay = jnp.exp(log_forget + stab - new_stab)
    weight_in = jnp.exp(in_gate - new_stab)
    select = (jnp.arange(heads) == head).astype(jnp.float32)
    my_decay = jnp.sum(decay * select, axis=-1)
    my_weight = jnp.sum(weight_in * select, axis=-1)
    my_stab = jnp.sum(new_stab * select, axis=-1)
    new_norm = my_decay[:, None] * norm_vec + my_weight[:, None] * keys.astype(jnp.float32)
    den_part = jnp.sum(query.astype(jnp.float32) * new_norm, axis=-1)
    q_head, k_head = (query, keys)
    denom = den_part
    for bit in range(group.bit_length() - 1):
        other_q, other_k = from_partner((q_head, k_head), "tp", bit)
        other_den = from_partner(denom, "tp", bit)
        lower = device // 2**bit % 2 == 0
        q_head = combine_halves(q_head, other_q, lower)
        k_head = combine_halves(k_head, other_k, lower)
        denom = denom + other_den
    outer = values.astype(jnp.float32)[:, :, None] * k_head.astype(jnp.float32)[:, None, :]
    new_cell = my_decay[:, None, None] * cell + my_weight[:, None, None] * outer
    numer = jnp.einsum(
        "bk,bek->be", q_head.astype(jnp.float32), new_cell, precision=lax.Precision.HIGHEST
    )
    readout = numer / jnp.maximum(jnp.abs(denom), jnp.exp(-my_stab))[:, None]
    branch = (jax.nn.sigmoid(outgate.astype(jnp.float32)) * readout).astype(jnp.bfloat16)
    summed = project(gathered_copies(branch, "tp", 1), w_proj)
    own_input = lax.dynamic_slice_in_dim(cur_f, device * ncols, ncols, 1)
    result = (own_input + summed).astype(jnp.bfloat16)
    return (result, new_cell, new_norm, new_stab)


def body(
    tokens,
    norm_gain,
    query_weight,
    key_weight,
    value_weight,
    outgate_weight,
    gate_weight,
    forget_bias,
    proj_weight,
    cell_state,
    normalizer,
    stabilizer,
):
    current = tokens
    cells = []
    norms = []
    stabs = []
    result = tokens
    for layer in range(LAYERS):
        result, new_cell, new_norm, new_stab = one_cell(
            current,
            norm_gain[layer],
            query_weight[layer],
            key_weight[layer],
            value_weight[layer],
            outgate_weight[layer],
            gate_weight[layer],
            forget_bias[layer],
            proj_weight[layer],
            cell_state[layer],
            normalizer[layer],
            stabilizer[layer],
        )
        cells.append(new_cell)
        norms.append(new_norm)
        stabs.append(new_stab)
        if layer + 1 < LAYERS:
            current = gathered_copies(result, "tp", 1)
    return (result, jnp.stack(cells), jnp.stack(norms), jnp.stack(stabs))


def solution(mesh):
    return jax.shard_map(
        body,
        mesh=mesh,
        in_specs=(
            P("grp", None),
            P(),
            P(None, "tp", None),
            P(None, "tp", None),
            P(None, "tp", None),
            P(None, "tp", None),
            P(),
            P(),
            P(None, "tp", None),
            P(None, "grp", "tp", None),
            P(None, "grp", "tp"),
            P(None, "grp", None),
        ),
        out_specs=(
            P("grp", "tp"),
            P(None, "grp", "tp", None),
            P(None, "grp", "tp"),
            P(None, "grp", None),
        ),
        check_vma=False,
    )
```

profile of v0, /device:TPU:37, one launch (start us, length us, event | category | flops | bytes accessed | tf_op | source)
XLA Modules:
  0.0 233.1 jit_solution(12848716380185168266)
XLA Ops:
  0.7 0.8 slice_reduce_fusion
  1.5 1.2 copy.36
  2.8 0.3 multiply_reduce_fusion.1
  3.1 1.6 fusion.12
  4.7 20.5 %collective-permute-start.3 = (bf16[64,32]{1,0:T(8,128)(2,1)S(1)}, bf16[64,32]{1,0:T(8,128)(2,1)S(1)}, u32[]{:S(2)}, u32[]{:S(2)}) collective-permute-start(bf16[64,32]{1,0:T(8,128)(2,1)S(1)} %fusion.12), channel_id=1, source_target_pairs={{0,1},{1,0},{2,3},{3,2},{4,5},{5,4},{6,7},{7,6},{8,9},{9,8},{10,11... | collective-permute-start | bytes 12296 | tf_op jit(solution)/shard_map/ppermute | solution.py:17
  25.2 0.6 convolution_convert_fusion.1
  25.9 0.2 collective-permute-start
  26.2 0.5 fusion.58
  26.8 0.2 fusion.70
  27.0 0.6 collective-permute-start.6
  27.6 0.5 fusion.27
  28.0 0.5 fusion.22
  28.5 0.1 collective-permute-start.7
  28.7 2.4 %collective-permute-done.7 = f32[64]{0:T(128)S(1)} collective-permute-done((f32[64]{0:T(128)S(1)}, f32[64]{0:T(128)S(1)}, u32[]{:S(2)}, u32[]{:S(2)}) %collective-permute-start.7) | collective-permute-done | bytes 288 | tf_op jit(solution)/shard_map/ppermute | solution.py:17
  31.2 3.2 %collective-permute-done.8 = f32[64]{0:T(128)S(1)} collective-permute-done((f32[64]{0:T(128)S(1)}, f32[64]{0:T(128)S(1)}, u32[]{:S(2)}, u32[]{:S(2)}) %collective-permute-start.8) | collective-permute-done | bytes 288 | tf_op jit(solution)/shard_map/ppermute | solution.py:17
  34.5 0.1 collective-permute-start.1
  34.8 1.6 collective-permute-start.4
  36.3 0.9 collective-permute-done.1
  37.3 0.1 collective-permute-start.2
  37.6 2.5 %collective-permute-start.5 = (bf16[64,128]{1,0:T(8,128)(2,1)S(1)}, bf16[64,128]{1,0:T(8,128)(2,1)S(1)}, u32[]{:S(2)}, u32[]{:S(2)}) collective-permute-start(bf16[64,128]{1,0:T(8,128)(2,1)S(1)} %maximum_select_fusion.7), channel_id=1, source_target_pairs={{0,4},{1,5},{2,6},{3,7},{4,0},{5,1},{6,2},{7,3},{8,12},{9,13},{10,... | collective-permute-start | bytes 49160 | tf_op jit(solution)/shard_map/ppermute | solution.py:17
  40.0 0.9 collective-permute-done.2
  40.9 0.2 collective-permute-done.5
  41.2 3.0 %fusion.4 = f32[64,1,32]{2,1,0:T(1,128)S(1)} fusion(f32[2,64,32,256]{3,2,1,0:T(8,128)} %param.21, f32[64,256]{1,0:T(8,128)S(1)} %fusion.65, f32[64,32]{1,0:T(8,128)S(1)} %copy.38, f32[64]{0:T(128)S(1)} %get-tuple-element.12, f32[64]{0:T(128)S(1)} %get-tuple-element.13, bf16[64,256,1]{1,0,2:T(8,128)(2,1)S(1)} %fusion.64), kind=kOutput, calls=%fused_computation.6 | convolution fusion | flops 8388608 | bytes 2212352 | tf_op jit(solution)/shard_map/bk,bek->be/dot_general | solution.py:100
  44.4 1.0 reshape.226
  45.4 20.5 %all-to-all-start = ((bf16[64,2,1024]{2,1,0:T(2,128)(2,1)}), bf16[64,2,1024]{2,1,0:T(2,128)(2,1)S(1)}, u32[]{:S(2)}, u32[]{:S(2)}) async-start(bf16[64,2,1024]{2,1,0:T(2,128)(2,1)} %reshape.226), calls=%async_computation | async-start | bytes 524288 | tf_op jit(solution)/shard_map/all_to_all | solution.py:22
  65.9 41.0 %all-to-all-done = bf16[64,2,1024]{2,1,0:T(2,128)(2,1)S(1)} async-done(((bf16[64,2,1024]{2,1,0:T(2,128)(2,1)}), bf16[64,2,1024]{2,1,0:T(2,128)(2,1)S(1)}, u32[]{:S(2)}, u32[]{:S(2)}) %all-to-all-start) | async-done | bytes 262176 | tf_op jit(solution)/shard_map/all_to_all | solution.py:22
  107.0 0.3 reshape.227
  107.3 0.2 fusion.14
  107.6 1.0 reshape.228
  108.6 6.8 %all-to-all-start.1 = ((bf16[64,2,1024]{2,1,0:T(2,128)(2,1)}), bf16[64,2,1024]{2,1,0:T(2,128)(2,1)S(1)}, u32[]{:S(2)}, u32[]{:S(2)}) async-start(bf16[64,2,1024]{2,1,0:T(2,128)(2,1)} %reshape.228), calls=%async_computation.1 | async-start | bytes 524288 | tf_op jit(solution)/shard_map/all_to_all | solution.py:22
  115.6 42.5 %all-to-all-done.1 = bf16[64,2,1024]{2,1,0:T(2,128)(2,1)S(1)} async-done(((bf16[64,2,1024]{2,1,0:T(2,128)(2,1)}), bf16[64,2,1024]{2,1,0:T(2,128)(2,1)S(1)}, u32[]{:S(2)}, u32[]{:S(2)}) %all-to-all-start.1) | async-done | bytes 262176 | tf_op jit(solution)/shard_map/all_to_all | solution.py:22
  158.1 0.3 reshape.229
  158.4 0.3 multiply_reduce_fusion
  158.7 0.3 multiply_convert_fusion
  159.1 0.2 fusion.56
  159.2 0.3 fusion.13
  159.6 0.3 convolution_convert_fusion
  160.1 0.2 fusion.71
  160.3 0.9 collective-permute-start.15
  161.1 0.8 collective-permute-done.15
  161.9 0.4 collective-permute-start.16
  162.4 0.2 fusion.21
  162.6 1.8 collective-permute-done.16
  164.4 0.2 fusion.16
  164.6 1.6 collective-permute-start.9
  166.2 0.1 collective-permute-start.12
  166.4 1.3 collective-permute-done.17
  167.8 0.5 collective-permute-start.10
  168.4 1.2 collective-permute-start.13
  169.6 0.9 collective-permute-done.10
  170.6 2.1 collective-permute-start.11
  172.8 0.5 collective-permute-start.14
  173.3 0.9 collective-permute-done.11
  174.2 2.2 collective-permute-done.14
  176.4 3.0 %fusion.1 = f32[64,1,32]{2,1,0:T(1,128)S(1)} fusion(f32[2,64,32,256]{3,2,1,0:T(8,128)} %param.21, f32[64,256]{1,0:T(8,128)S(1)} %fusion.67, f32[64,32]{1,0:T(8,128)S(1)} %copy.42, f32[64]{0:T(128)S(1)} %get-tuple-element.10, f32[64]{0:T(128)S(1)} %get-tuple-element.9, bf16[64,256,1]{1,0,2:T(8,128)(2,1)S(1)} %fusion.66), kind=kOutput, calls=%fused_computation.3 | convolution fusion | flops 8388608 | bytes 2212352 | tf_op jit(solution)/shard_map/bk,bek->be/dot_general | solution.py:100
  179.6 1.0 reshape.230
  180.6 8.7 %all-to-all-start.2 = ((bf16[64,2,1024]{2,1,0:T(2,128)(2,1)}), bf16[64,2,1024]{2,1,0:T(2,128)(2,1)S(1)}, u32[]{:S(2)}, u32[]{:S(2)}) async-start(bf16[64,2,1024]{2,1,0:T(2,128)(2,1)} %reshape.230), calls=%async_computation.2 | async-start | bytes 524288 | tf_op jit(solution)/shard_map/all_to_all | solution.py:22
  189.3 0.7 copy.47
  190.0 0.6 pad_maximum_fusion.2
  190.8 2.8 %multiply_add_fusion.1 = (f32[1,64,32,256]{3,2,1,0:T(8,128)S(1)}, f32[1,64,32,256]{3,2,1,0:T(8,128)S(1)}) fusion(f32[2,64,32,256]{3,2,1,0:T(8,128)} %param.21, f32[64,256]{1,0:T(8,128)S(1)} %fusion.65, f32[64,32]{1,0:T(8,128)S(1)} %copy.38, f32[64]{0:T(128)S(1)} %get-tuple-element.12, f32[64]{0:T(128)S(1)} %get-tuple-element.13, f32[64,256]{1,0:T(8,128)S(1)} %fusion.67, ...), kind=kLoop, calls=%fused_computation.8 | loop fusion | flops 4194304 | bytes 8537088 | tf_op jit(solution)/shard_map/add | solution.py:99
  193.5 2.3 %pad_maximum_fusion = f32[2,64,32,256]{3,2,1,0:T(8,128)} fusion(f32[1,64,32,256]{3,2,1,0:T(8,128)S(1)} %get-tuple-element.19, f32[1,64,32,256]{3,2,1,0:T(8,128)S(1)} %get-tuple-element.18), kind=kLoop, calls=%fused_computation | loop fusion | flops 1048576 | bytes 8388608 | tf_op jit(solution)/shard_map/stack | solution.py:150
  195.9 36.1 %all-to-all-done.2 = bf16[64,2,1024]{2,1,0:T(2,128)(2,1)S(1)} async-done(((bf16[64,2,1024]{2,1,0:T(2,128)(2,1)}), bf16[64,2,1024]{2,1,0:T(2,128)(2,1)S(1)}, u32[]{:S(2)}, u32[]{:S(2)}) %all-to-all-start.2) | async-done | bytes 262176 | tf_op jit(solution)/shard_map/all_to_all | solution.py:22
  232.0 0.3 reshape.231
  232.3 0.8 fusion.15
  (69 shorter events, 2.2 us)
Async XLA Ops:
  0.6 24.6 %copy-start.2 = (bf16[2,32,2048]{2,1,0:T(8,128)(2,1)S(1)}, bf16[2,32,2048]{2,1,0:T(8,128)(2,1)}, u32[]{:S(2)}) copy-start(bf16[2,32,2048]{2,1,0:T(8,128)(2,1)} %param.14) | copy-start | bytes 786436
  0.6 25.4 %copy-start.8 = (f32[2,8]{1,0:T(2,128)S(1)}, f32[2,8]{1,0:T(2,128)}, u32[]{:S(2)}) copy-start(f32[2,8]{1,0:T(2,128)} %param.19) | copy-start | bytes 196
  0.7 25.4 %copy-start.6 = (f32[2,64,32]{1,2,0:T(8,128)S(1)}, f32[2,64,32]{1,2,0:T(8,128)}, u32[]{:S(2)}) copy-start(f32[2,64,32]{1,2,0:T(8,128)} %param.22) | copy-start | bytes 49156
  0.7 25.5 %copy-start.5 = (bf16[2,2048,16]{1,2,0:T(8,128)(2,1)S(1)}, bf16[2,2048,16]{1,2,0:T(8,128)(2,1)}, u32[]{:S(2)}) copy-start(bf16[2,2048,16]{1,2,0:T(8,128)(2,1)} %param.18) | copy-start | bytes 393220
  2.7 23.9 %copy-start.7 = (f32[2,64,8]{1,2,0:T(8,128)S(1)}, f32[2,64,8]{1,2,0:T(8,128)}, u32[]{:S(2)}) copy-start(f32[2,64,8]{1,2,0:T(8,128)} %param.23) | copy-start | bytes 12292
  2.7 24.8 %copy-start.3 = (bf16[2,32,2048]{2,1,0:T(8,128)(2,1)S(1)}, bf16[2,32,2048]{2,1,0:T(8,128)(2,1)}, u32[]{:S(2)}) copy-start(bf16[2,32,2048]{2,1,0:T(8,128)(2,1)} %param.17) | copy-start | bytes 786436
  3.1 25.0 %copy-start.4 = (bf16[2,32,2048]{2,1,0:T(8,128)(2,1)S(1)}, bf16[2,32,2048]{2,1,0:T(8,128)(2,1)}, u32[]{:S(2)}) copy-start(bf16[2,32,2048]{2,1,0:T(8,128)(2,1)} %param.16) | copy-start | bytes 786436
  4.7 30.0 %collective-permute-start.3 = (bf16[64,32]{1,0:T(8,128)(2,1)S(1)}, bf16[64,32]{1,0:T(8,128)(2,1)S(1)}, u32[]{:S(2)}, u32[]{:S(2)}) collective-permute-start(bf16[64,32]{1,0:T(8,128)(2,1)S(1)} %fusion.12), channel_id=1, source_target_pairs={{0,1},{1,0},{2,3},{3,2},{4,5},{5,4},{6,7},{7,6},{8,9},{9,8},{10,11... | collective-permute-start | bytes 12296 | tf_op jit(solution)/shard_map/ppermute | solution.py:17
  25.9 8.6 %collective-permute-start = (bf16[64,32]{1,0:T(8,128)(2,1)S(1)}, bf16[64,32]{1,0:T(8,128)(2,1)S(1)}, u32[]{:S(2)}, u32[]{:S(2)}) collective-permute-start(bf16[64,32]{1,0:T(8,128)(2,1)S(1)} %convolution_convert_fusion.1), channel_id=1, source_target_pairs={{0,1},{1,0},{2,3},{3,2},{4,5},{5,4},{6,7},{7,6},{8,9},{9,8},{10,11... | collective-permute-start | bytes 12296 | tf_op jit(solution)/shard_map/ppermute | solution.py:17
  27.0 1.5 collective-permute-start.6
  28.5 2.5 %collective-permute-start.7 = (f32[64]{0:T(128)S(1)}, f32[64]{0:T(128)S(1)}, u32[]{:S(2)}, u32[]{:S(2)}) collective-permute-start(f32[64]{0:T(128)S(1)} %add.134), channel_id=1, source_target_pairs={{0,2},{1,3},{2,0},{3,1},{4,6},{5,7},{6,4},{7,5},{8,10},{9,11},{10,... | collective-permute-start | bytes 776 | tf_op jit(solution)/shard_map/ppermute | solution.py:17
  31.1 3.3 %collective-permute-start.8 = (f32[64]{0:T(128)S(1)}, f32[64]{0:T(128)S(1)}, u32[]{:S(2)}, u32[]{:S(2)}) collective-permute-start(f32[64]{0:T(128)S(1)} %add.135), channel_id=1, source_target_pairs={{0,4},{1,5},{2,6},{3,7},{4,0},{5,1},{6,2},{7,3},{8,12},{9,13},{10,... | collective-permute-start | bytes 776 | tf_op jit(solution)/shard_map/ppermute | solution.py:17
  34.5 2.7 %collective-permute-start.1 = (bf16[64,64]{1,0:T(8,128)(2,1)S(1)}, bf16[64,64]{1,0:T(8,128)(2,1)S(1)}, u32[]{:S(2)}, u32[]{:S(2)}) collective-permute-start(bf16[64,64]{1,0:T(8,128)(2,1)S(1)} %maximum_select_fusion.4), channel_id=1, source_target_pairs={{0,2},{1,3},{2,0},{3,1},{4,6},{5,7},{6,4},{7,5},{8,10},{9,11},{10,... | collective-permute-start | bytes 24584 | tf_op jit(solution)/shard_map/ppermute | solution.py:17
  34.8 2.7 %collective-permute-start.4 = (bf16[64,64]{1,0:T(8,128)(2,1)S(1)}, bf16[64,64]{1,0:T(8,128)(2,1)S(1)}, u32[]{:S(2)}, u32[]{:S(2)}) collective-permute-start(bf16[64,64]{1,0:T(8,128)(2,1)S(1)} %maximum_select_fusion.6), channel_id=1, source_target_pairs={{0,2},{1,3},{2,0},{3,1},{4,6},{5,7},{6,4},{7,5},{8,10},{9,11},{10,... | collective-permute-start | bytes 24584 | tf_op jit(solution)/shard_map/ppermute | solution.py:17
  37.3 3.6 %collective-permute-start.2 = (bf16[64,128]{1,0:T(8,128)(2,1)S(1)}, bf16[64,128]{1,0:T(8,128)(2,1)S(1)}, u32[]{:S(2)}, u32[]{:S(2)}) collective-permute-start(bf16[64,128]{1,0:T(8,128)(2,1)S(1)} %maximum_select_fusion.5), channel_id=1, source_target_pairs={{0,4},{1,5},{2,6},{3,7},{4,0},{5,1},{6,2},{7,3},{8,12},{9,13},{10,... | collective-permute-start | bytes 49160 | tf_op jit(solution)/shard_map/ppermute | solution.py:17
  37.6 3.6 %collective-permute-start.5 = (bf16[64,128]{1,0:T(8,128)(2,1)S(1)}, bf16[64,128]{1,0:T(8,128)(2,1)S(1)}, u32[]{:S(2)}, u32[]{:S(2)}) collective-permute-start(bf16[64,128]{1,0:T(8,128)(2,1)S(1)} %maximum_select_fusion.7), channel_id=1, source_target_pairs={{0,4},{1,5},{2,6},{3,7},{4,0},{5,1},{6,2},{7,3},{8,12},{9,13},{10,... | collective-permute-start | bytes 49160 | tf_op jit(solution)/shard_map/ppermute | solution.py:17
  44.3 63.0 %copy-start = (bf16[2,32,2048]{2,1,0:T(8,128)(2,1)S(1)}, bf16[2,32,2048]{2,1,0:T(8,128)(2,1)}, u32[]{:S(2)}) copy-start(bf16[2,32,2048]{2,1,0:T(8,128)(2,1)} %param.20) | copy-start | bytes 786436
  45.4 61.6 %all-to-all-start = ((bf16[64,2,1024]{2,1,0:T(2,128)(2,1)}), bf16[64,2,1024]{2,1,0:T(2,128)(2,1)S(1)}, u32[]{:S(2)}, u32[]{:S(2)}) async-start(bf16[64,2,1024]{2,1,0:T(2,128)(2,1)} %reshape.226), calls=%async_computation | async-start | bytes 524288 | tf_op jit(solution)/shard_map/all_to_all | solution.py:22
  107.6 51.6 %copy-start.1 = (bf16[2,32,2048]{2,1,0:T(8,128)(2,1)S(1)}, bf16[2,32,2048]{2,1,0:T(8,128)(2,1)}, u32[]{:S(2)}) copy-start(bf16[2,32,2048]{2,1,0:T(8,128)(2,1)} %param.15) | copy-start | bytes 786436
  108.6 49.4 %all-to-all-start.1 = ((bf16[64,2,1024]{2,1,0:T(2,128)(2,1)}), bf16[64,2,1024]{2,1,0:T(2,128)(2,1)S(1)}, u32[]{:S(2)}, u32[]{:S(2)}) async-start(bf16[64,2,1024]{2,1,0:T(2,128)(2,1)} %reshape.228), calls=%async_computation.1 | async-start | bytes 524288 | tf_op jit(solution)/shard_map/all_to_all | solution.py:22
  160.3 1.7 collective-permute-start.15
  161.9 2.4 %collective-permute-start.16 = (f32[64]{0:T(128)S(1)}, f32[64]{0:T(128)S(1)}, u32[]{:S(2)}, u32[]{:S(2)}) collective-permute-start(f32[64]{0:T(128)S(1)} %add.147), channel_id=1, source_target_pairs={{0,2},{1,3},{2,0},{3,1},{4,6},{5,7},{6,4},{7,5},{8,10},{9,11},{10,... | collective-permute-start | bytes 776 | tf_op jit(solution)/shard_map/ppermute | solution.py:17
  164.4 3.3 %collective-permute-start.17 = (f32[64]{0:T(128)S(1)}, f32[64]{0:T(128)S(1)}, u32[]{:S(2)}, u32[]{:S(2)}) collective-permute-start(f32[64]{0:T(128)S(1)} %add.148), channel_id=1, source_target_pairs={{0,4},{1,5},{2,6},{3,7},{4,0},{5,1},{6,2},{7,3},{8,12},{9,13},{10,... | collective-permute-start | bytes 776 | tf_op jit(solution)/shard_map/ppermute | solution.py:17
  164.6 3.1 %collective-permute-start.9 = (bf16[64,32]{1,0:T(8,128)(2,1)S(1)}, bf16[64,32]{1,0:T(8,128)(2,1)S(1)}, u32[]{:S(2)}, u32[]{:S(2)}) collective-permute-start(bf16[64,32]{1,0:T(8,128)(2,1)S(1)} %convolution_convert_fusion), channel_id=1, source_target_pairs={{0,1},{1,0},{2,3},{3,2},{4,5},{5,4},{6,7},{7,6},{8,9},{9,8},{10,11... | collective-permute-start | bytes 12296 | tf_op jit(solution)/shard_map/ppermute | solution.py:17
  166.2 2.2 collective-permute-start.12
  167.8 2.7 %collective-permute-start.10 = (bf16[64,64]{1,0:T(8,128)(2,1)S(1)}, bf16[64,64]{1,0:T(8,128)(2,1)S(1)}, u32[]{:S(2)}, u32[]{:S(2)}) collective-permute-start(bf16[64,64]{1,0:T(8,128)(2,1)S(1)} %maximum_select_fusion.8), channel_id=1, source_target_pairs={{0,2},{1,3},{2,0},{3,1},{4,6},{5,7},{6,4},{7,5},{8,10},{9,11},{10,... | collective-permute-start | bytes 24584 | tf_op jit(solution)/shard_map/ppermute | solution.py:17
  168.4 4.3 %collective-permute-start.13 = (bf16[64,64]{1,0:T(8,128)(2,1)S(1)}, bf16[64,64]{1,0:T(8,128)(2,1)S(1)}, u32[]{:S(2)}, u32[]{:S(2)}) collective-permute-start(bf16[64,64]{1,0:T(8,128)(2,1)S(1)} %maximum_select_fusion.10), channel_id=1, source_target_pairs={{0,2},{1,3},{2,0},{3,1},{4,6},{5,7},{6,4},{7,5},{8,10},{9,11},{10,... | collective-permute-start | bytes 24584 | tf_op jit(solution)/shard_map/ppermute | solution.py:17
  170.6 3.6 %collective-permute-start.11 = (bf16[64,128]{1,0:T(8,128)(2,1)S(1)}, bf16[64,128]{1,0:T(8,128)(2,1)S(1)}, u32[]{:S(2)}, u32[]{:S(2)}) collective-permute-start(bf16[64,128]{1,0:T(8,128)(2,1)S(1)} %maximum_select_fusion.9), channel_id=1, source_target_pairs={{0,4},{1,5},{2,6},{3,7},{4,0},{5,1},{6,2},{7,3},{8,12},{9,13},{10,... | collective-permute-start | bytes 49160 | tf_op jit(solution)/shard_map/ppermute | solution.py:17
  172.8 3.6 %collective-permute-start.14 = (bf16[64,128]{1,0:T(8,128)(2,1)S(1)}, bf16[64,128]{1,0:T(8,128)(2,1)S(1)}, u32[]{:S(2)}, u32[]{:S(2)}) collective-permute-start(bf16[64,128]{1,0:T(8,128)(2,1)S(1)} %maximum_select_fusion.11), channel_id=1, source_target_pairs={{0,4},{1,5},{2,6},{3,7},{4,0},{5,1},{6,2},{7,3},{8,12},{9,13},{10,... | collective-permute-start | bytes 49160 | tf_op jit(solution)/shard_map/ppermute | solution.py:17
  180.6 51.4 %all-to-all-start.2 = ((bf16[64,2,1024]{2,1,0:T(2,128)(2,1)}), bf16[64,2,1024]{2,1,0:T(2,128)(2,1)S(1)}, u32[]{:S(2)}, u32[]{:S(2)}) async-start(bf16[64,2,1024]{2,1,0:T(2,128)(2,1)} %reshape.230), calls=%async_computation.2 | async-start | bytes 524288 | tf_op jit(solution)/shard_map/all_to_all | solution.py:22
where the time goes:
time: 234 us; the launch traced here: 233 us
  waiting for transfers between devices  135 us (58%)
  starting transfers between devices  69.1 us (30%)
  matrix products  11.9 us (5%)
  other arithmetic  8.32 us (4%)
  local copies, waits for them, and re-layouts  7.58 us (3%)
    all_to_all x3, waiting for transfers between devices, sent_to_all(): lax.all_to_all(jnp.broadcast_to(shard[None], (length, *shard.shape)), axi...  120 us
    all_to_all x3, starting transfers between devices, sent_to_all(): lax.all_to_all(jnp.broadcast_to(shard[None], (length, *shard.shape)), axi...  36 us
    ppermute x18, starting transfers between devices, from_partner(): return lax.ppermute(value, axis, pairs)  33.1 us
    ppermute x18, waiting for transfers between devices, from_partner(): return lax.ppermute(value, axis, pairs)  15.5 us
    unnamed x31, local copies, waits for them, and re-layouts  6.38 us
    dot_general x2, matrix products, one_cell(): jnp.einsum('bk,bek->be', q_head.astype(jnp.float32), new_cell, precision=...  6.01 us
    dot_general x10, matrix products, project(): lax.dot_general(normed, weight, (((1,), (1,)), ((), ())), preferred_eleme...  5.23 us
  transfers between devices with their start and end apart: 21, of which 14 were waited for; matrix products, arithmetic and copies ran while one was open for 5% of the time, Pallas kernels for 0%

commit v1 on v0

v1 whole, which is shorter than its diff:
```python
import jax
import jax.numpy as jnp
from jax import lax
from jax.sharding import PartitionSpec as P

EPSILON = 1e-06
NEAR = 4


def near_groups(total, size):
    return [[first + i for i in range(size)] for first in range(0, total, size)]


def far_groups(total, stride):
    return [list(range(first, total, stride)) for first in range(stride)]


def shared(block, groups):
    count = len(groups[0])
    copies = jnp.broadcast_to(block[None], (count, *block.shape))
    return lax.all_to_all(copies, "tp", 0, 0, tiled=True, axis_index_groups=groups)


def gathered(block_t):
    total = lax.axis_size("tp")
    columns, batch = block_t.shape
    half = columns // 2
    packed = jnp.concatenate([block_t[:half], block_t[half:]], axis=1)
    far = shared(packed, far_groups(total, NEAR))
    near = shared(far.reshape(-1, 2 * batch), near_groups(total, NEAR))
    near = near.reshape(NEAR, total // NEAR, half, 2, batch)
    return near.transpose(1, 0, 3, 2, 4).reshape(total * columns, batch)


def project(weight, normed_t):
    return lax.dot_general(
        weight, normed_t, (((1,), (0,)), ((), ())), preferred_element_type=jnp.float32
    )


def three_parts(value):
    high = lax.reduce_precision(value, 8, 7)
    middle = lax.reduce_precision(value - high, 8, 7)
    low = lax.reduce_precision(value - high - middle, 8, 7)
    return [part.astype(jnp.bfloat16) for part in (high, middle, low)]


def one_cell(cur_t, own_t, gain, w_query, w_key, w_value, w_outgate, w_gates, bias_forget, w_proj, cell, norm_vec, stab):
    total = lax.axis_size("tp")
    columns = w_query.shape[0]
    head_size = cell.shape[-1]
    heads = stab.shape[-1]
    batch = cur_t.shape[1]
    group = head_size // columns
    head = lax.axis_index("tp") // group
    cur_f = cur_t.astype(jnp.float32)
    scale = lax.rsqrt(jnp.mean(cur_f * cur_f, axis=0, keepdims=True) + EPSILON)
    normed = (cur_f * scale * gain[:, None]).astype(jnp.bfloat16)
    query = project(w_query, normed).astype(jnp.bfloat16)
    keys = (project(w_key, normed) * head_size ** (-0.5)).astype(jnp.bfloat16)
    gates = project(w_gates.T, normed)
    in_gate = gates[:heads]
    log_forget = jax.nn.log_sigmoid(gates[heads:] + bias_forget[:, None])
    stab_t = stab.T
    new_stab = jnp.maximum(log_forget + stab_t, in_gate)
    decay = jnp.exp(log_forget + stab_t - new_stab)
    weight_in = jnp.exp(in_gate - new_stab)
    select = (jnp.arange(heads) == head).astype(jnp.float32)[:, None]
    my_decay = jnp.sum(decay * select, axis=0)
    my_weight = jnp.sum(weight_in * select, axis=0)
    my_stab = jnp.sum(new_stab * select, axis=0)
    new_norm = my_decay[None] * norm_vec.T + my_weight[None] * keys.astype(jnp.float32)
    den_part = jnp.sum(query.astype(jnp.float32) * new_norm, axis=0)
    high, middle, low = three_parts(den_part)
    extra = jnp.concatenate([high, middle, low, jnp.zeros_like(low)]).reshape(2, 2 * batch)
    extra = jnp.concatenate([extra, jnp.zeros((14, 2 * batch), jnp.bfloat16)])
    message = jnp.concatenate([jnp.concatenate([query, keys], axis=1), extra])
    everyone = shared(message, near_groups(total, group))
    q_head = everyone[:, :columns, :batch].reshape(head_size, batch).T
    k_head = everyone[:, :columns, batch:].reshape(head_size, batch).T
    parts = everyone[:, columns : columns + 2].astype(jnp.float32)
    denom = jnp.sum(parts[:, 0, :batch] + parts[:, 0, batch:] + parts[:, 1, :batch], axis=0)
    values = project(w_value, normed).astype(jnp.bfloat16).T
    outgate = project(w_outgate, normed).astype(jnp.bfloat16)
    outer = values.astype(jnp.float32)[:, :, None] * k_head.astype(jnp.float32)[:, None, :]
    new_cell = my_decay[:, None, None] * cell + my_weight[:, None, None] * outer
    numer = jnp.einsum(
        "bk,bek->be", q_head.astype(jnp.float32), new_cell, precision=lax.Precision.HIGHEST
    )
    readout = numer.T / jnp.maximum(jnp.abs(denom), jnp.exp(-my_stab))[None]
    branch = (jax.nn.sigmoid(outgate.astype(jnp.float32)) * readout).astype(jnp.bfloat16)
    summed = project(w_proj, gathered(branch))
    result = (own_t.astype(jnp.float32) + summed).astype(jnp.bfloat16)
    return result, new_cell, new_norm.T, new_stab.T


def body(tokens, norm_gain, query_weight, key_weight, value_weight, outgate_weight, gate_weight, forget_bias, proj_weight, cell_state, normalizer, stabilizer):
    layers = query_weight.shape[0]
    columns = query_weight.shape[1]
    current = tokens.T
    result = lax.dynamic_slice_in_dim(current, lax.axis_index("tp") * columns, columns, 0)
    cells, norms, stabs = [], [], []
    for layer in range(layers):
        result, new_cell, new_norm, new_stab = one_cell(
            current,
            result,
            norm_gain[layer],
            query_weight[layer],
            key_weight[layer],
            value_weight[layer],
            outgate_weight[layer],
            gate_weight[layer],
            forget_bias[layer],
            proj_weight[layer],
            cell_state[layer],
            normalizer[layer],
            stabilizer[layer],
        )
        cells.append(new_cell)
        norms.append(new_norm)
        stabs.append(new_stab)
        if layer + 1 < layers:
            current = gathered(result)
    return (result.T, jnp.stack(cells), jnp.stack(norms), jnp.stack(stabs))


def solution(mesh):
    return jax.shard_map(
        body,
        mesh=mesh,
        in_specs=(
            P("grp", None),
            P(),
            P(None, "tp", None),
            P(None, "tp", None),
            P(None, "tp", None),
            P(None, "tp", None),
            P(),
            P(),
            P(None, "tp", None),
            P(None, "grp", "tp", None),
            P(None, "grp", "tp"),
            P(None, "grp", None),
        ),
        out_specs=(
            P("grp", "tp"),
            P(None, "grp", "tp", None),
            P(None, "grp", "tp"),
            P(None, "grp", None),
        ),
        check_vma=False,
    )
```

time: 234 us -> 185 us (0.79)
  waiting for transfers between devices: 135 us -> 20.2 us
  blocking collectives: 0 us -> 85 us
  starting transfers between devices: 69.1 us -> 48 us
  other arithmetic: 8.32 us -> 15.5 us
  matrix products: 11.9 us -> 6.4 us
    all_to_all x3 -> x5, waiting for transfers between devices: 120 us -> 20.2 us  [shared(): lax.all_to_all(copies, 'tp', 0, 0, tiled=True, axis_index_groups=groups)]
    all_to_all x0 -> x3, blocking collectives: none -> 85 us  [shared(): lax.all_to_all(copies, 'tp', 0, 0, tiled=True, axis_index_groups=groups)]
    ppermute x18 -> x0, starting transfers between devices: 33.1 us -> none  [from_partner(): return lax.ppermute(value, axis, pairs)]
    ppermute x18 -> x0, waiting for transfers between devices: 15.5 us -> none  [from_partner(): return lax.ppermute(value, axis, pairs)]
    all_to_all x3 -> x5, starting transfers between devices: 36 us -> 48 us  [shared(): lax.all_to_all(copies, 'tp', 0, 0, tiled=True, axis_index_groups=groups)]
    unnamed x31 -> x21, local copies, waits for them, and re-layouts: 6.38 us -> 0.29 us
    dot_general x14 -> x12, matrix products: 11.9 us -> 6.4 us  [project(): lax.dot_general(weight, normed_t, (((1,), (0,)), ((), ())), preferred_ele...]
    unnamed x0 -> x3, other arithmetic: none -> 4.73 us
  transfers between devices with their start and end apart: 21 -> 5, of which waited for: 14 -> 4; matrix products, arithmetic and copies ran while one was open for 5% -> 4% of each run, Pallas kernels for 0% -> 0%
where the time goes in v1:
time: 185 us; the launch traced here: 184 us
  blocking collectives  85 us (46%)
  starting transfers between devices  48 us (26%)
  waiting for transfers between devices  20.2 us (11%)
  other arithmetic  15.5 us (8%)
  local copies, waits for them, and re-layouts  7.67 us (4%)
  matrix products  6.4 us (3%)
    all_to_all x3, blocking collectives, shared(): lax.all_to_all(copies, 'tp', 0, 0, tiled=True, axis_index_groups=groups)  85 us
    all_to_all x5, starting transfers between devices, shared(): lax.all_to_all(copies, 'tp', 0, 0, tiled=True, axis_index_groups=groups)  48 us
    all_to_all x5, waiting for transfers between devices, shared(): lax.all_to_all(copies, 'tp', 0, 0, tiled=True, axis_index_groups=groups)  20.2 us
    dot_general x12, matrix products, project(): lax.dot_general(weight, normed_t, (((1,), (0,)), ((), ())), preferred_ele...  6.4 us
    unnamed x3, other arithmetic  4.73 us
    another operation x6, other arithmetic, body(): return (result.T, jnp.stack(cells), jnp.stack(norms), jnp.stack(stabs))  4.44 us
  transfers between devices with their start and end apart: 5, of which 4 were waited for; matrix products, arithmetic and copies ran while one was open for 4% of the time, Pallas kernels for 0%

profile of v1, /device:TPU:37, one launch (start us, length us, event | category | flops | bytes accessed | tf_op | source)
XLA Modules:
  0.0 183.7 jit_solution(13781097084648430743)
XLA Ops:
  0.7 0.8 slice_reduce_fusion
  1.5 1.1 fusion.33
  2.6 0.8 slice_bitcast_fusion
  3.4 1.2 convolution_bitcast_fusion
  4.6 1.3 fusion.19
  5.9 0.8 fusion.78
  6.6 0.1 multiply_reduce_fusion.4
  6.7 1.3 fusion.63
  8.2 0.1 fusion.76
  8.3 0.7 broadcast_in_dim.22
  9.0 23.7 %all-to-all-start = ((bf16[8,48,128]{2,1,0:T(8,128)(2,1)}), bf16[8,48,128]{2,1,0:T(8,128)(2,1)S(1)}, u32[]{:S(2)}, u32[]{:S(2)}) async-start(bf16[8,48,128]{2,1,0:T(8,128)(2,1)} %broadcast_in_dim.22), calls=%async_computation | async-start | bytes 196608 | tf_op jit(solution)/shard_map/all_to_all | solution.py:21
  32.7 0.3 fusion.20
  33.0 0.1 copy.47
  33.0 5.1 %all-to-all-done = bf16[8,48,128]{2,1,0:T(8,128)(2,1)S(1)} async-done(((bf16[8,48,128]{2,1,0:T(8,128)(2,1)}), bf16[8,48,128]{2,1,0:T(8,128)(2,1)S(1)}, u32[]{:S(2)}, u32[]{:S(2)}) %all-to-all-start) | async-done | bytes 98336 | tf_op jit(solution)/shard_map/all_to_all | solution.py:21
  38.1 0.1 fusion.88
  38.3 0.1 copy.69
  38.4 0.1 copy.48
  38.4 2.4 %fusion.7 = f32[64,32]{1,0:T(8,128)S(1)} fusion(f32[2,64,32,256]{3,2,1,0:T(8,128)} %param.21, f32[64,256]{1,0:T(8,128)S(1)} %copy.69, f32[64,256]{1,0:T(8,128)S(1)} %copy.48, f32[64,32]{1,0:T(8,128)S(1)} %copy.47, f32[64]{0:T(128)S(1)} %get-tuple-element.8, f32[64]{0:T(128)S(1)} %get-tuple-element.9), kind=kLoop, calls=%fused_computation.10 | loop fusion | flops 3143680 | bytes 2245120
  40.9 0.1 fusion.70
  41.0 0.3 fusion.30
  41.3 0.1 pad_maximum_fusion.3
  41.4 34.1 %all_to_all.40 = bf16[16,16,128]{2,1,0:T(8,128)(2,1)S(1)} all-to-all(bf16[16,16,128]{2,1,0:T(8,128)(2,1)S(1)} %broadcast_in_dim.23), channel_id=1, replica_groups={{0,4,8,12,16,20,24,28,32,36,40,44,48,52,56,60},{1,5,9,13,17,21,25,29,33..., dimensions={0} | all-to-all | bytes 131072 | tf_op jit(solution)/shard_map/all_to_all | solution.py:21
  75.6 0.7 broadcast_in_dim.25
  76.3 6.9 %all-to-all-start.2 = ((bf16[4,256,128]{2,1,0:T(8,128)(2,1)}), bf16[4,256,128]{2,1,0:T(8,128)(2,1)S(1)}, u32[]{:S(2)}, u32[]{:S(2)}) async-start(bf16[4,256,128]{2,1,0:T(8,128)(2,1)} %broadcast_in_dim.25), calls=%async_computation.2 | async-start | bytes 524288 | tf_op jit(solution)/shard_map/all_to_all | solution.py:21
  83.2 0.1 constant_dynamic-slice_fusion
  83.3 0.1 copy.68
  83.4 4.9 %all-to-all-done.2 = bf16[4,256,128]{2,1,0:T(8,128)(2,1)S(1)} async-done(((bf16[4,256,128]{2,1,0:T(8,128)(2,1)}), bf16[4,256,128]{2,1,0:T(8,128)(2,1)S(1)}, u32[]{:S(2)}, u32[]{:S(2)}) %all-to-all-start.2) | async-done | bytes 262176 | tf_op jit(solution)/shard_map/all_to_all | solution.py:21
  88.3 0.2 reshape.188
  88.5 0.1 copy.49
  88.7 0.2 fusion.8
  88.9 0.1 pad_maximum_fusion.4
  89.0 25.3 %all_to_all.41 = bf16[16,16,128]{2,1,0:T(8,128)(2,1)S(1)} all-to-all(bf16[16,16,128]{2,1,0:T(8,128)(2,1)S(1)} %broadcast_in_dim.26), channel_id=1, replica_groups={{0,4,8,12,16,20,24,28,32,36,40,44,48,52,56,60},{1,5,9,13,17,21,25,29,33..., dimensions={0} | all-to-all | bytes 131072 | tf_op jit(solution)/shard_map/all_to_all | solution.py:21
  114.3 0.7 broadcast_in_dim.28
  115.0 6.2 %all-to-all-start.4 = ((bf16[4,256,128]{2,1,0:T(8,128)(2,1)}), bf16[4,256,128]{2,1,0:T(8,128)(2,1)S(1)}, u32[]{:S(2)}, u32[]{:S(2)}) async-start(bf16[4,256,128]{2,1,0:T(8,128)(2,1)} %broadcast_in_dim.28), calls=%async_computation.4 | async-start | bytes 524288 | tf_op jit(solution)/shard_map/all_to_all | solution.py:21
  121.3 0.1 mul.319
  121.4 4.9 %all-to-all-done.4 = bf16[4,256,128]{2,1,0:T(8,128)(2,1)S(1)} async-done(((bf16[4,256,128]{2,1,0:T(8,128)(2,1)}), bf16[4,256,128]{2,1,0:T(8,128)(2,1)S(1)}, u32[]{:S(2)}, u32[]{:S(2)}) %all-to-all-start.4) | async-done | bytes 262176 | tf_op jit(solution)/shard_map/all_to_all | solution.py:21
  126.3 0.6 reshape.194
  127.0 1.1 multiply_reduce_fusion
  128.1 0.3 fusion.32
  128.4 0.2 convolution_bitcast_fusion.1
  128.6 0.2 fusion.9
  128.9 0.1 fusion.79
  128.9 0.1 multiply_reduce_fusion.1
  129.0 0.2 fusion.61
  129.4 0.7 broadcast_in_dim.29
  130.1 4.2 %all-to-all-start.5 = ((bf16[8,48,128]{2,1,0:T(8,128)(2,1)}), bf16[8,48,128]{2,1,0:T(8,128)(2,1)S(1)}, u32[]{:S(2)}, u32[]{:S(2)}) async-start(bf16[8,48,128]{2,1,0:T(8,128)(2,1)} %broadcast_in_dim.29), calls=%async_computation.5 | async-start | bytes 196608 | tf_op jit(solution)/shard_map/all_to_all | solution.py:21
  134.3 0.2 fusion.11
  134.5 0.1 copy.51
  134.6 5.2 %all-to-all-done.5 = bf16[8,48,128]{2,1,0:T(8,128)(2,1)S(1)} async-done(((bf16[8,48,128]{2,1,0:T(8,128)(2,1)}), bf16[8,48,128]{2,1,0:T(8,128)(2,1)S(1)}, u32[]{:S(2)}, u32[]{:S(2)}) %all-to-all-start.5) | async-done | bytes 98336 | tf_op jit(solution)/shard_map/all_to_all | solution.py:21
  139.8 0.1 fusion.87
  140.1 2.4 %fusion.3 = f32[64,32]{1,0:T(8,128)S(1)} fusion(f32[2,64,32,256]{3,2,1,0:T(8,128)} %param.21, f32[64,256]{1,0:T(8,128)S(1)} %copy.70, f32[64,256]{1,0:T(8,128)S(1)} %copy.52, f32[64,32]{1,0:T(8,128)S(1)} %copy.51, f32[64]{0:T(128)S(1)} %get-tuple-element.6, f32[64]{0:T(128)S(1)} %get-tuple-element.5), kind=kLoop, calls=%fused_computation.5 | loop fusion | flops 3143680 | bytes 2245120
  142.6 0.1 fusion.71
  142.7 0.2 fusion.28
  142.9 0.1 pad_maximum_fusion.5
  143.0 25.5 %all_to_all.42 = bf16[16,16,128]{2,1,0:T(8,128)(2,1)S(1)} all-to-all(bf16[16,16,128]{2,1,0:T(8,128)(2,1)S(1)} %broadcast_in_dim.30), channel_id=1, replica_groups={{0,4,8,12,16,20,24,28,32,36,40,44,48,52,56,60},{1,5,9,13,17,21,25,29,33..., dimensions={0} | all-to-all | bytes 131072 | tf_op jit(solution)/shard_map/all_to_all | solution.py:21
  168.6 0.7 broadcast_in_dim.32
  169.3 6.9 %all-to-all-start.7 = ((bf16[4,256,128]{2,1,0:T(8,128)(2,1)}), bf16[4,256,128]{2,1,0:T(8,128)(2,1)S(1)}, u32[]{:S(2)}, u32[]{:S(2)}) async-start(bf16[4,256,128]{2,1,0:T(8,128)(2,1)} %broadcast_in_dim.32), calls=%async_computation.7 | async-start | bytes 524288 | tf_op jit(solution)/shard_map/all_to_all | solution.py:21
  176.2 0.6 pad_maximum_fusion.2
  176.8 0.6 pad_maximum_fusion.1
  177.4 2.7 %multiply_add_fusion.1 = (f32[1,64,32,256]{3,2,1,0:T(8,128)S(1)}, f32[1,64,32,256]{3,2,1,0:T(8,128)S(1)}) fusion(f32[2,64,32,256]{3,2,1,0:T(8,128)} %param.21, f32[64,256]{1,0:T(8,128)S(1)} %copy.48, f32[64,32]{1,0:T(8,128)S(1)} %copy.47, f32[64]{0:T(128)S(1)} %get-tuple-element.8, f32[64]{0:T(128)S(1)} %get-tuple-element.9, f32[64,256]{1,0:T(8,128)S(1)} %copy.52, ...), kind=kLoop, calls=%fused_computation.12 | loop fusion | flops 4194304 | bytes 8537088 | tf_op jit(solution)/shard_map/add | solution.py:86
  180.2 2.3 %pad_maximum_fusion = f32[2,64,32,256]{3,2,1,0:T(8,128)} fusion(f32[1,64,32,256]{3,2,1,0:T(8,128)S(1)} %get-tuple-element.15, f32[1,64,32,256]{3,2,1,0:T(8,128)S(1)} %get-tuple-element.14), kind=kLoop, calls=%fused_computation | loop fusion | flops 1048576 | bytes 8388608 | tf_op jit(solution)/shard_map/stack | solution.py:124
  182.5 0.2 reshape.192
  182.8 0.1 copy.53
  182.9 0.8 fusion.10
  (48 shorter events, 0.8 us)
Async XLA Ops:
  0.6 32.0 %copy-start = (bf16[64,2048]{1,0:T(8,128)(2,1)S(1)}, bf16[64,2048]{1,0:T(8,128)(2,1)}, u32[]{:S(2)}) copy-start(bf16[64,2048]{1,0:T(8,128)(2,1)} %param.12) | copy-start | bytes 786436
  0.6 32.0 %copy-start.5 = (bf16[2,32,2048]{2,1,0:T(8,128)(2,1)S(1)}, bf16[2,32,2048]{2,1,0:T(8,128)(2,1)}, u32[]{:S(2)}) copy-start(bf16[2,32,2048]{2,1,0:T(8,128)(2,1)} %param.16) | copy-start | bytes 786436
  9.0 29.2 %all-to-all-start = ((bf16[8,48,128]{2,1,0:T(8,128)(2,1)}), bf16[8,48,128]{2,1,0:T(8,128)(2,1)S(1)}, u32[]{:S(2)}, u32[]{:S(2)}) async-start(bf16[8,48,128]{2,1,0:T(8,128)(2,1)} %broadcast_in_dim.22), calls=%async_computation | async-start | bytes 196608 | tf_op jit(solution)/shard_map/all_to_all | solution.py:21
  32.7 8.3 %copy-start.6 = (bf16[2,32,2048]{2,1,0:T(8,128)(2,1)S(1)}, bf16[2,32,2048]{2,1,0:T(8,128)(2,1)}, u32[]{:S(2)}) copy-start(bf16[2,32,2048]{2,1,0:T(8,128)(2,1)} %param.17) | copy-start | bytes 786436
  40.8 47.8 %copy-start.1 = (bf16[2,32,2048]{2,1,0:T(8,128)(2,1)S(1)}, bf16[2,32,2048]{2,1,0:T(8,128)(2,1)}, u32[]{:S(2)}) copy-start(bf16[2,32,2048]{2,1,0:T(8,128)(2,1)} %param.20) | copy-start | bytes 786436
  76.3 12.0 %all-to-all-start.2 = ((bf16[4,256,128]{2,1,0:T(8,128)(2,1)}), bf16[4,256,128]{2,1,0:T(8,128)(2,1)S(1)}, u32[]{:S(2)}, u32[]{:S(2)}) async-start(bf16[4,256,128]{2,1,0:T(8,128)(2,1)} %broadcast_in_dim.25), calls=%async_computation.2 | async-start | bytes 524288 | tf_op jit(solution)/shard_map/all_to_all | solution.py:21
  115.0 11.3 %all-to-all-start.4 = ((bf16[4,256,128]{2,1,0:T(8,128)(2,1)}), bf16[4,256,128]{2,1,0:T(8,128)(2,1)S(1)}, u32[]{:S(2)}, u32[]{:S(2)}) async-start(bf16[4,256,128]{2,1,0:T(8,128)(2,1)} %broadcast_in_dim.28), calls=%async_computation.4 | async-start | bytes 524288 | tf_op jit(solution)/shard_map/all_to_all | solution.py:21
  121.3 7.2 %copy-start.7 = (bf16[2,2048,16]{1,2,0:T(8,128)(2,1)S(1)}, bf16[2,2048,16]{1,2,0:T(8,128)(2,1)}, u32[]{:S(2)}) copy-start(bf16[2,2048,16]{1,2,0:T(8,128)(2,1)} %param.18) | copy-start | bytes 393220
  121.4 7.2 %copy-start.3 = (bf16[2,32,2048]{2,1,0:T(8,128)(2,1)S(1)}, bf16[2,32,2048]{2,1,0:T(8,128)(2,1)}, u32[]{:S(2)}) copy-start(bf16[2,32,2048]{2,1,0:T(8,128)(2,1)} %param.15) | copy-start | bytes 786436
  127.0 1.9 %copy-start.8 = (f32[2,64,8]{1,2,0:T(8,128)S(1)}, f32[2,64,8]{1,2,0:T(8,128)}, u32[]{:S(2)}) copy-start(f32[2,64,8]{1,2,0:T(8,128)} %param.23) | copy-start | bytes 12292
  127.0 2.1 %copy-start.2 = (f32[2,64,32]{1,2,0:T(8,128)S(1)}, f32[2,64,32]{1,2,0:T(8,128)}, u32[]{:S(2)}) copy-start(f32[2,64,32]{1,2,0:T(8,128)} %param.22) | copy-start | bytes 49156
  127.0 2.1 %copy-start.4 = (bf16[2,32,2048]{2,1,0:T(8,128)(2,1)S(1)}, bf16[2,32,2048]{2,1,0:T(8,128)(2,1)}, u32[]{:S(2)}) copy-start(bf16[2,32,2048]{2,1,0:T(8,128)(2,1)} %param.14) | copy-start | bytes 786436
  130.1 9.7 %all-to-all-start.5 = ((bf16[8,48,128]{2,1,0:T(8,128)(2,1)}), bf16[8,48,128]{2,1,0:T(8,128)(2,1)S(1)}, u32[]{:S(2)}, u32[]{:S(2)}) async-start(bf16[8,48,128]{2,1,0:T(8,128)(2,1)} %broadcast_in_dim.29), calls=%async_computation.5 | async-start | bytes 196608 | tf_op jit(solution)/shard_map/all_to_all | solution.py:21
  169.3 13.2 %all-to-all-start.7 = ((bf16[4,256,128]{2,1,0:T(8,128)(2,1)}), bf16[4,256,128]{2,1,0:T(8,128)(2,1)S(1)}, u32[]{:S(2)}, u32[]{:S(2)}) async-start(bf16[4,256,128]{2,1,0:T(8,128)(2,1)} %broadcast_in_dim.32), calls=%async_computation.7 | async-start | bytes 524288 | tf_op jit(solution)/shard_map/all_to_all | solution.py:21

commit v2 on v1

v2 whole, which is shorter than its diff:
```python
import functools

import jax
import jax.numpy as jnp
from jax import lax
from jax.experimental import pallas as pl
from jax.experimental.pallas import tpu as pltpu
from jax.sharding import PartitionSpec as P

EPSILON = 1e-06
NEAR = 4
CHUNKS = 4
UNROLLED = 8
F32 = jnp.float32
BF16 = jnp.bfloat16
LIMITED = pltpu.CompilerParams(vmem_limit_bytes=16 * 2**20)


def near_groups(total, size):
    return [[first + i for i in range(size)] for first in range(0, total, size)]


def far_groups(total, stride):
    return [list(range(first, total, stride)) for first in range(stride)]


def exchanged(copies, groups):
    return lax.all_to_all(copies, "tp", 0, 0, tiled=True, axis_index_groups=groups)


def from_partner(value, mask):
    pairs = [(source, source ^ mask) for source in range(lax.axis_size("tp"))]
    return lax.ppermute(value, "tp", pairs)


def gathered(copies, meanwhile=None):
    count, rows, lanes = copies.shape
    far = exchanged(copies, far_groups(lax.axis_size("tp"), NEAR))
    own = far.reshape(count * rows, lanes)
    second = from_partner(own, 2)
    first = from_partner(own, 1)
    made = None
    if meanwhile is not None:
        second, made = lax.optimization_barrier((second, meanwhile(own)))
    third = from_partner(second, 1)
    return (own, first, second, third), made


def whole(shape):
    return pl.BlockSpec(shape, lambda *_: (0,) * len(shape))


def one_layer(shape, layer):
    return pl.BlockSpec((None, *shape), lambda *_: (layer,) + (0,) * len(shape))


def smem():
    return pl.BlockSpec(memory_space=pltpu.SMEM)


def unpack(place_ref, pieces, stage_ref):
    own = place_ref[1]
    far, per, batch = stage_ref.shape
    half = per // (2 * NEAR)
    for flip, piece in enumerate(pieces):
        start = pl.multiple_of((own ^ flip) * 2 * half, 2 * half)
        both = piece[...].reshape(far, half, 2 * batch)
        stage_ref[:, pl.ds(start, half), :] = both[:, :, :batch]
        stage_ref[:, pl.ds(start + half, half), :] = both[:, :, batch:]


def front_rest(layer, place_ref, outs, bias_ref, stab_ref, norm_ref, message_ref, value_ref, open_ref, rows_ref, new_norm_ref, new_stab_ref, head_size):
    columns, batch = norm_ref.shape
    heads = stab_ref.shape[0]
    head = place_ref[0]
    query = outs[:columns].astype(BF16)
    keys = (outs[columns : 2 * columns] * head_size ** (-0.5)).astype(BF16)
    value_ref[...] = outs[2 * columns : 3 * columns].astype(BF16).astype(F32)
    open_ref[...] = jax.nn.sigmoid(outs[3 * columns : 4 * columns].astype(BF16).astype(F32))
    in_gate = outs[4 * columns : 4 * columns + heads]
    row = lax.broadcasted_iota(jnp.int32, (heads, heads), 0)
    col = lax.broadcasted_iota(jnp.int32, (heads, heads), 1)
    spread = jnp.broadcast_to(bias_ref[layer : layer + 1, :], (heads, heads))
    bias = jnp.sum(jnp.where(row == col, spread, 0.0), axis=1, keepdims=True)
    forget = outs[4 * columns + heads :] + bias
    log_forget = jnp.minimum(forget, 0.0) - jnp.log1p(jnp.exp(-jnp.abs(forget)))
    shifted = log_forget + stab_ref[...]
    new_stab = jnp.maximum(shifted, in_gate)
    decay = jnp.exp(shifted - new_stab)
    weight = jnp.exp(in_gate - new_stab)
    floor = jnp.exp(-new_stab)
    mine = lax.broadcasted_iota(jnp.int32, (heads, batch), 0) == head

    def own(table):
        return jnp.sum(jnp.where(mine, table, 0.0), axis=0, keepdims=True)

    decay, weight, floor = own(decay), own(weight), own(floor)
    new_norm = decay * norm_ref[...] + weight * keys.astype(F32)
    part = jnp.sum(query.astype(F32) * new_norm, axis=0, keepdims=True)
    high = part.astype(BF16).astype(F32)
    middle = (part - high).astype(BF16).astype(F32)
    low = part - high - middle
    none = jnp.zeros_like(low)
    extra = jnp.concatenate(
        [jnp.concatenate([high, middle], axis=1), jnp.concatenate([low, none], axis=1), jnp.zeros((14, 2 * batch), F32)]
    ).astype(BF16)
    message = jnp.concatenate([jnp.concatenate([query, keys], axis=1), extra])
    message_ref[...] = jnp.broadcast_to(message[None], message_ref.shape)
    rows_ref[...] = jnp.concatenate(
        [jnp.concatenate([decay, weight], axis=1), jnp.concatenate([floor, none], axis=1), jnp.zeros((6, 2 * batch), F32)]
    )
    new_norm_ref[...] = new_norm
    new_stab_ref[...] = new_stab


def first_front(place_ref, cell_ref, tokens_ref, gain_ref, wq_ref, wk_ref, wv_ref, wo_ref, wg_ref, *rest, head_size):
    *rest, held_ref, own_ref, arrived = rest
    fetch = pltpu.make_async_copy(cell_ref.at[0], held_ref, arrived)
    fetch.start()
    columns = own_ref.shape[0]
    near = NEAR * columns
    nearby = tokens_ref[:, pl.ds(pl.multiple_of(place_ref[2] * near, near), near)].astype(F32)
    turned = pltpu.roll(nearby, (NEAR - place_ref[1]) % NEAR * columns, 1).T
    own_ref[...] = turned[:columns].astype(BF16)
    current = tokens_ref[...].astype(F32)
    scale = lax.rsqrt(jnp.mean(current * current, axis=1, keepdims=True) + EPSILON)
    normed = (current * scale * gain_ref[0:1, :]).astype(BF16)
    weights = jnp.concatenate([wq_ref[...], wk_ref[...], wv_ref[...], wo_ref[...], wg_ref[...]])
    outs = lax.dot_general(weights, normed, (((1,), (1,)), ((), ())), preferred_element_type=F32)
    front_rest(0, place_ref, outs, *rest, head_size=head_size)
    fetch.wait()


def later_front(place_ref, cell_ref, own_ref, first_ref, second_ref, third_ref, gain_ref, wq_ref, wk_ref, wv_ref, wo_ref, wg_ref, *rest, layer, head_size):
    *rest, held_ref, arrived, stage_ref, normed_ref = rest
    fetch = pltpu.make_async_copy(cell_ref.at[layer], held_ref, arrived)
    fetch.start()
    unpack(place_ref, (own_ref, first_ref, second_ref, third_ref), stage_ref)
    far, per, batch = stage_ref.shape
    current = stage_ref[...].astype(F32)
    square = jnp.sum(jnp.sum(current * current, axis=0), axis=0, keepdims=True)
    scale = lax.rsqrt(square / (far * per) + EPSILON)
    gain = jnp.concatenate([gain_ref[layer : layer + 1, i * per : (i + 1) * per] for i in range(far)]).T
    for i in range(far):
        normed_ref[i * per : (i + 1) * per, :] = (current[i] * scale * gain[:, i : i + 1]).astype(BF16)
    weights = jnp.concatenate([wq_ref[...], wk_ref[...], wv_ref[...], wo_ref[...], wg_ref[...]])
    outs = jnp.dot(weights, normed_ref[...], preferred_element_type=F32)
    front_rest(layer, place_ref, outs, *rest, head_size=head_size)
    fetch.wait()


def in_hbm(*values):
    return [pltpu.with_memory_space_constraint(value, pltpu.HBM) for value in values]


def front(layer, place, current, norm_gain, projections, gates, bias, stab, norm, cell):
    _, columns, width = projections[0].shape
    heads, batch = stab.shape[1:]
    head_size = cell.shape[-1]
    group = head_size // columns
    far = lax.axis_size("tp") // NEAR
    out_shape = (
        jax.ShapeDtypeStruct((group, columns + 16, 2 * batch), BF16),
        jax.ShapeDtypeStruct((columns, batch), F32),
        jax.ShapeDtypeStruct((columns, batch), F32),
        jax.ShapeDtypeStruct((8, 2 * batch), F32),
        jax.ShapeDtypeStruct((columns, batch), F32),
        jax.ShapeDtypeStruct((heads, batch), F32),
        jax.ShapeDtypeStruct(cell.shape[1:], F32),
    )
    out_specs = [whole(out.shape) for out in out_shape[:-1]] + [pl.BlockSpec(memory_space=pl.ANY)]
    tail_specs = [whole(norm_gain.shape)] + [one_layer((columns, width), layer)] * 4 + [
        one_layer((2 * heads, width), layer),
        whole(bias.shape),
        one_layer((heads, batch), layer),
        one_layer((columns, batch), layer),
    ]
    tail = (norm_gain, *projections, gates, bias, stab, norm)
    head_specs = [smem(), pl.BlockSpec(memory_space=pl.ANY)]
    if layer == 0:
        out_shape = (*out_shape, jax.ShapeDtypeStruct((columns, batch), BF16))
        out_specs.append(whole((columns, batch)))
        return pl.pallas_call(
            functools.partial(first_front, head_size=head_size),
            grid=(1,),
            out_shape=out_shape,
            out_specs=out_specs,
            in_specs=head_specs + [whole((batch, width))] + tail_specs,
            scratch_shapes=[pltpu.SemaphoreType.DMA],
            compiler_params=LIMITED,
            name="front_first",
        )(place, *in_hbm(cell, current, *tail))
    per = width // far
    return pl.pallas_call(
        functools.partial(later_front, layer=layer, head_size=head_size),
        grid=(1,),
        out_shape=out_shape,
        out_specs=out_specs,
        in_specs=head_specs + [whole(current[0].shape)] * 4 + tail_specs,
        scratch_shapes=[
            pltpu.SemaphoreType.DMA,
            pltpu.VMEM((far, per, batch), BF16),
            pltpu.VMEM((width, batch), BF16),
        ],
        compiler_params=LIMITED,
        name="front_later",
    )(place, *in_hbm(cell), *current, *tail)


def head_rows(everyone_ref, columns):
    group, _, lanes = everyone_ref.shape
    return everyone_ref[:, :columns, :].astype(F32).reshape(group * columns, lanes)


def read_kernel(everyone_ref, value_ref, open_ref, rows_ref, cell_ref, copies_ref, turned_ref):
    columns, batch = value_ref.shape
    half_keys = cell_ref.shape[2] // 2
    both = head_rows(everyone_ref, columns)
    turned_ref[...] = both.T
    product = jnp.sum(both[:, :batch] * both[:, batch:], axis=0, keepdims=True)
    lane = lax.broadcasted_iota(jnp.int32, (columns, batch), 1)

    def some(step, sums):
        for i in range(UNROLLED):
            b = step * UNROLLED + i
            products = cell_ref[b] * turned_ref[pl.ds(b, 1), :]
            folded = products[:, :half_keys] + products[:, half_keys:]
            sums = jnp.where(lane == b, jnp.sum(folded, axis=1, keepdims=True), sums)
        return sums

    sums = lax.fori_loop(0, batch // UNROLLED, some, jnp.zeros((columns, batch), F32))
    parts = jnp.sum(everyone_ref[:, columns:, :].astype(F32), axis=0)
    denom = parts[0:1, :batch] + parts[0:1, batch:] + parts[1:2, :batch]
    decay = rows_ref[0:1, :batch]
    weight = rows_ref[0:1, batch:]
    floor = rows_ref[1:2, :batch]
    numer = decay * sums + value_ref[...] * (weight * product)
    readout = numer / jnp.maximum(jnp.abs(denom), floor)
    branch = (open_ref[...] * readout).astype(BF16)
    half = columns // 2
    packed = jnp.concatenate([branch[:half], branch[half:]], axis=1)
    copies_ref[...] = jnp.broadcast_to(packed[None], copies_ref.shape)


def read(everyone, value, opened, rows, held):
    columns, batch = value.shape
    far = lax.axis_size("tp") // NEAR
    out_shape = jax.ShapeDtypeStruct((far, columns // 2, 2 * batch), BF16)
    operands = (everyone, value, opened, rows, held)
    return pl.pallas_call(
        read_kernel,
        grid=(1,),
        out_shape=out_shape,
        in_specs=[whole(operand.shape) for operand in operands],
        out_specs=whole(out_shape.shape),
        scratch_shapes=[pltpu.VMEM((2 * batch, held.shape[-1]), F32)],
        compiler_params=LIMITED,
        name="read",
    )(*operands)


def update_kernel(layers, *refs):
    everyone_refs, value_refs, rows_refs, held_refs, norm_refs, stab_refs = (
        refs[k * layers : (k + 1) * layers] for k in range(6)
    )
    _, cell_ref, norms_ref, stabs_ref, turned_ref, decay_ref, added_ref = refs[6 * layers :]
    step = pl.program_id(0) % CHUNKS
    chunk, columns, keys = cell_ref.shape
    batch = added_ref.shape[1] // 2

    def one(layer):
        @pl.when(step == 0)
        def _():
            rows = rows_refs[layer]
            turned_ref[...] = head_rows(everyone_refs[layer], columns).T
            decay_ref[...] = jnp.broadcast_to(rows[0:1, :], (2 * batch, 2 * batch)).T
            scaled = value_refs[layer][...] * rows[0:1, batch:]
            added_ref[...] = jnp.concatenate([scaled, scaled], axis=1)
            norms_ref[layer] = norm_refs[layer][...]
            stabs_ref[layer] = stab_refs[layer][...]

        added = pltpu.roll(added_ref[...], batch - step * chunk, 1)
        for i in range(chunk):
            b = step * chunk + i
            key = turned_ref[pl.ds(batch + b, 1), :]
            decay = decay_ref[pl.ds(b, 1), :]
            decay = jnp.concatenate([decay] * (keys // decay.shape[1]), axis=1)
            cell_ref[i] = decay * held_refs[layer][i] + added[:, i : i + 1] * key

    for layer in range(layers):
        pl.when(pl.program_id(0) // CHUNKS == layer)(functools.partial(one, layer))


def update(memory, after):
    layers = len(memory)
    everyone, value, rows, held, norm, stab = zip(*memory)
    columns, batch = value[0].shape
    keys = held[0].shape[-1]
    chunk = batch // CHUNKS
    out_shape = (
        jax.ShapeDtypeStruct((layers, *held[0].shape), F32),
        jax.ShapeDtypeStruct((layers, *norm[0].shape), F32),
        jax.ShapeDtypeStruct((layers, *stab[0].shape), F32),
    )

    def held_spec(layer):
        return pl.BlockSpec((chunk, columns, keys), lambda i: (jnp.clip(i - layer * CHUNKS, 0, CHUNKS - 1), 0, 0))

    def wholes(values):
        return [whole(each.shape) for each in values]

    return pl.pallas_call(
        functools.partial(update_kernel, layers),
        grid=(layers * CHUNKS,),
        out_shape=out_shape,
        in_specs=wholes(everyone)
        + wholes(value)
        + wholes(rows)
        + [held_spec(layer) for layer in range(layers)]
        + wholes(norm)
        + wholes(stab)
        + [pl.BlockSpec(memory_space=pl.ANY)],
        out_specs=(
            pl.BlockSpec((None, chunk, columns, keys), lambda i: (i // CHUNKS, i % CHUNKS, 0, 0)),
            whole(out_shape[1].shape),
            whole(out_shape[2].shape),
        ),
        scratch_shapes=[
            pltpu.VMEM((2 * batch, keys), F32),
            pltpu.VMEM((2 * batch, 2 * batch), F32),
            pltpu.VMEM((columns, 2 * batch), F32),
        ],
        compiler_params=LIMITED,
        name="update",
    )(*everyone, *value, *rows, *held, *norm, *stab, after)


def proj_result(place_ref, pieces, weight_ref, residual_ref, stage_ref):
    unpack(place_ref, pieces, stage_ref)
    far, per, batch = stage_ref.shape
    summed = jnp.dot(weight_ref[...], stage_ref[...].reshape(far * per, batch), preferred_element_type=F32)
    return (residual_ref[...].astype(F32) + summed).astype(BF16)


def proj_kernel(place_ref, own_ref, first_ref, second_ref, third_ref, weight_ref, residual_ref, result_ref, *rest):
    *copies, stage_ref = rest
    pieces = (own_ref, first_ref, second_ref, third_ref)
    result = proj_result(place_ref, pieces, weight_ref, residual_ref, stage_ref)
    result_ref[...] = result
    half = result.shape[0] // 2
    for copies_ref in copies:
        packed = jnp.concatenate([result[:half], result[half:]], axis=1)
        copies_ref[...] = jnp.broadcast_to(packed[None], copies_ref.shape)


def proj(layer, place, pieces, weight, residual, send):
    _, columns, width = weight.shape
    batch = residual.shape[1]
    far = lax.axis_size("tp") // NEAR
    out_shape = [jax.ShapeDtypeStruct((columns, batch), BF16)]
    operands = [place, *pieces, weight, residual]
    in_specs = [smem()] + [whole(pieces[0].shape)] * 4 + [one_layer((columns, width), layer), whole(residual.shape)]
    if send:
        out_shape.append(jax.ShapeDtypeStruct((far, columns // 2, 2 * batch), BF16))
    return pl.pallas_call(
        proj_kernel,
        grid=(1,),
        out_shape=out_shape,
        out_specs=[whole(out.shape) for out in out_shape],
        in_specs=in_specs,
        scratch_shapes=[pltpu.VMEM((far, width // far, batch), BF16)],
        compiler_params=LIMITED,
        name="proj",
    )(*operands)


def body(tokens, norm_gain, query_weight, key_weight, value_weight, outgate_weight, gate_weight, forget_bias, proj_weight, cell_state, normalizer, stabilizer):
    layers, columns, _ = query_weight.shape
    head_size = cell_state.shape[-1]
    group = head_size // columns
    device = lax.axis_index("tp")
    place = jnp.stack([device // group, device % NEAR, device // NEAR]).astype(jnp.int32)
    gates = gate_weight.transpose(0, 2, 1)
    stab = stabilizer.transpose(0, 2, 1)
    norm = normalizer.transpose(0, 2, 1)
    projections = (query_weight, key_weight, value_weight, outgate_weight)
    residual = None
    current = tokens
    memory = []
    for layer in range(layers):
        message, value, opened, rows, new_norm, new_stab, held, *own_input = front(
            layer, place, current, norm_gain, projections, gates, forget_bias, stab, norm, cell_state
        )
        residual = own_input[0] if own_input else residual
        everyone = exchanged(message, near_groups(lax.axis_size("tp"), group))
        copies = read(everyone, value, opened, rows, held)
        memory.append((everyone, value, rows, held, new_norm, new_stab))
        last = layer + 1 == layers
        pieces, states = gathered(copies, functools.partial(update, memory) if last else None)
        residual, *copies = proj(layer, place, pieces, proj_weight, residual, not last)
        if not last:
            current, _ = gathered(copies[0])
    cells, norms, stabs = states
    return (residual.T, cells, norms.transpose(0, 2, 1), stabs.transpose(0, 2, 1))


def solution(mesh):
    return jax.shard_map(
        body,
        mesh=mesh,
        in_specs=(
            P("grp", None),
            P(),
            P(None, "tp", None),
            P(None, "tp", None),
            P(None, "tp", None),
            P(None, "tp", None),
            P(),
            P(),
            P(None, "tp", None),
            P(None, "grp", "tp", None),
            P(None, "grp", "tp"),
            P(None, "grp", None),
        ),
        out_specs=(
            P("grp", "tp"),
            P(None, "grp", "tp", None),
            P(None, "grp", "tp"),
            P(None, "grp", None),
        ),
        check_vma=False,
    )
```

time: 185 us -> 162 us (0.88)
  blocking collectives: 85 us -> 123 us
  starting transfers between devices: 48 us -> 18.9 us
  waiting for transfers between devices: 20.2 us -> 3 us
  Pallas kernels: 0 us -> 15.7 us
  other arithmetic: 15.5 us -> 0.08 us
  local copies, waits for them, and re-layouts: 7.67 us -> 0.05 us
  matrix products: 6.4 us -> 0 us
    all_to_all x5 -> x0, starting transfers between devices: 48 us -> none  [shared(): lax.all_to_all(copies, 'tp', 0, 0, tiled=True, axis_index_groups=groups)]
    all_to_all x3 -> x5, blocking collectives: 85 us -> 123 us  [exchanged(): lax.all_to_all(copies, 'tp', 0, 0, tiled=True, axis_index_groups=groups)]
    all_to_all x5 -> x0, waiting for transfers between devices: 20.2 us -> none  [shared(): lax.all_to_all(copies, 'tp', 0, 0, tiled=True, axis_index_groups=groups)]
    ppermute x0 -> x9, starting transfers between devices: none -> 18.9 us  [from_partner(): return lax.ppermute(value, 'tp', pairs)]
    pallas_call x0 -> x7, Pallas kernels: none -> 15.7 us  [the longest x1 4.79 us: update(): pl.pallas_call(functools.partial(update_kernel, layers), grid=(layers * C...]
    dot_general x12 -> x0, matrix products: 6.4 us -> none  [project(): lax.dot_general(weight, normed_t, (((1,), (0,)), ((), ())), preferred_ele...]
    unnamed x3 -> x0, other arithmetic: 4.73 us -> none
    another operation x6 -> x1, other arithmetic: 4.44 us -> 0.08 us  [body(): jnp.stack([device // group, device % NEAR, device // NEAR])]
  transfers between devices with their start and end apart: 5 -> 9, of which waited for: 4 -> 3; matrix products, arithmetic and copies ran while one was open for 4% -> 0% of each run, Pallas kernels for 0% -> 3%
where the time goes in v2:
time: 162 us
  blocking collectives  123 us (76%)
  starting transfers between devices  18.9 us (12%)
  Pallas kernels  15.7 us (10%)
  waiting for transfers between devices  3 us (2%)
    all_to_all x5, blocking collectives, exchanged(): lax.all_to_all(copies, 'tp', 0, 0, tiled=True, axis_index_groups=groups)  123 us
    ppermute x9, starting transfers between devices, from_partner(): return lax.ppermute(value, 'tp', pairs)  18.9 us
    pallas_call x1, Pallas kernels, update(): pl.pallas_call(functools.partial(update_kernel, layers), grid=(layers * C...  4.79 us
  transfers between devices with their start and end apart: 9, of which 3 were waited for; matrix products, arithmetic and copies ran while one was open for 0% of the time, Pallas kernels for 3%

profile of v2, /device:TPU:37, one launch (start us, length us, event | category | flops | bytes accessed | tf_op | source)
XLA Modules:
  0.0 161.8 jit_solution(18104837845725271354)
XLA Ops:
  0.6 0.0 copy-start.4
  0.7 0.1 pad_add_fusion.place_ref
  0.7 0.0 copy-start
  0.7 0.0 copy-start.1
  0.7 0.0 copy-start.2
  0.8 0.0 copy-start.3
  0.8 0.0 copy-start.5
  0.8 0.0 copy-start.6
  0.8 0.0 copy-start.7
  0.8 0.0 copy-start.8
  0.8 0.0 copy-start.9
  0.8 2.9 %front_first.1 = (bf16[8,48,128]{2,1,0:T(8,128)(2,1)S(1)}, f32[32,64]{1,0:T(8,128)S(1)}, f32[32,64]{1,0:T(8,128)S(1)}, f32[8,128]{1,0:T(8,128)S(1)}, f32[32,64]{...) custom-call(s32[3]{0:T(128)S(1)} %pad_add_fusion.place_ref, ...), custom_call_target="tpu_custom_call" | custom-call | tf_op jit(solution)/shard_map/front_first/pallas_call | solution.py:183
  3.7 28.3 %all_to_all.25.everyone_ref.refs_0_ = bf16[8,48,128]{2,1,0:T(8,128)(2,1)S(1)} all-to-all(bf16[8,48,128]{2,1,0:T(8,128)(2,1)S(1)} %get-tuple-element.28), channel_id=1, replica_groups={{0,1,2,3,4,5,6,7},{8,9,10,11,12,13,14,15},{16,17,18,19,20,21,22,23},{24..., dimensions={0} | all-to-all | bytes 196608 | tf_op jit(solution)/shard_map/all_to_all | solution.py:28
  32.0 1.2 read.2
  33.2 34.8 %all_to_all.26 = bf16[16,16,128]{2,1,0:T(8,128)(2,1)S(1)} all-to-all(bf16[16,16,128]{2,1,0:T(8,128)(2,1)S(1)} %read.2), channel_id=1, replica_groups={{0,4,8,12,16,20,24,28,32,36,40,44,48,52,56,60},{1,5,9,13,17,21,25,29,33..., dimensions={0} | all-to-all | bytes 131072 | tf_op jit(solution)/shard_map/all_to_all | solution.py:28
  68.0 0.2 collective-permute-start.1
  68.2 3.3 %collective-permute-start = (bf16[256,128]{1,0:T(8,128)(2,1)S(1)}, bf16[256,128]{1,0:T(8,128)(2,1)S(1)}, u32[]{:S(2)}, u32[]{:S(2)}) collective-permute-start(bf16[256,128]{1,0:T(8,128)(2,1)S(1)} %bitcast.22), channel_id=1, source_target_pairs={{0,1},{1,0},{2,3},{3,2},{4,5},{5,4},{6,7},{7,6},{8,9},{9,8},{10,11... | collective-permute-start | bytes 196616 | tf_op jit(solution)/shard_map/ppermute | solution.py:33
  71.5 0.0 collective-permute-done.1.second_ref
  71.5 4.3 %collective-permute-start.2 = (bf16[256,128]{1,0:T(8,128)(2,1)S(1)}, bf16[256,128]{1,0:T(8,128)(2,1)S(1)}, u32[]{:S(2)}, u32[]{:S(2)}) collective-permute-start(bf16[256,128]{1,0:T(8,128)(2,1)S(1)} %collective-permute-done.1.second_ref), channel_id=1, source_target_pairs={{0,1},{1,0},{2,3},{3,2},{4,5},{5,4},{6,7},{7,6},{8,9},{9,8},{10,11... | collective-permute-start | bytes 196616 | tf_op jit(solution)/shard_map/ppermute | solution.py:33
  75.8 0.0 collective-permute-done.first_ref
  75.8 0.9 collective-permute-done.2.third_ref
  76.7 0.0 copy-done.4
  76.7 1.0 proj.2
  77.7 25.4 %all_to_all.27 = bf16[16,16,128]{2,1,0:T(8,128)(2,1)S(1)} all-to-all(bf16[16,16,128]{2,1,0:T(8,128)(2,1)S(1)} %get-tuple-element.34), channel_id=1, replica_groups={{0,4,8,12,16,20,24,28,32,36,40,44,48,52,56,60},{1,5,9,13,17,21,25,29,33..., dimensions={0} | all-to-all | bytes 131072 | tf_op jit(solution)/shard_map/all_to_all | solution.py:28
  103.1 0.0 collective-permute-start.4
  103.1 3.2 %collective-permute-start.3 = (bf16[256,128]{1,0:T(8,128)(2,1)S(1)}, bf16[256,128]{1,0:T(8,128)(2,1)S(1)}, u32[]{:S(2)}, u32[]{:S(2)}) collective-permute-start(bf16[256,128]{1,0:T(8,128)(2,1)S(1)} %bitcast.19), channel_id=1, source_target_pairs={{0,1},{1,0},{2,3},{3,2},{4,5},{5,4},{6,7},{7,6},{8,9},{9,8},{10,11... | collective-permute-start | bytes 196616 | tf_op jit(solution)/shard_map/ppermute | solution.py:33
  106.3 0.0 collective-permute-done.4.second_ref
  106.3 4.3 %collective-permute-start.5 = (bf16[256,128]{1,0:T(8,128)(2,1)S(1)}, bf16[256,128]{1,0:T(8,128)(2,1)S(1)}, u32[]{:S(2)}, u32[]{:S(2)}) collective-permute-start(bf16[256,128]{1,0:T(8,128)(2,1)S(1)} %collective-permute-done.4.second_ref), channel_id=1, source_target_pairs={{0,1},{1,0},{2,3},{3,2},{4,5},{5,4},{6,7},{7,6},{8,9},{9,8},{10,11... | collective-permute-start | bytes 196616 | tf_op jit(solution)/shard_map/ppermute | solution.py:33
  110.6 0.0 collective-permute-done.3.first_ref
  110.6 0.9 collective-permute-done.5.third_ref
  111.5 0.0 copy-done
  111.5 0.0 copy-done.1
  111.5 0.0 copy-done.2
  111.5 0.0 copy-done.3
  111.5 0.0 copy-done.5
  111.5 0.0 copy-done.6
  111.5 0.0 copy-done.7
  111.5 0.0 copy-done.8
  111.5 0.0 copy-done.9
  111.5 3.1 %front_later.1 = (bf16[8,48,128]{2,1,0:T(8,128)(2,1)S(1)}, f32[32,64]{1,0:T(8,128)S(1)}, f32[32,64]{1,0:T(8,128)S(1)}, f32[8,128]{1,0:T(8,128)S(1)}, f32[32,64]{...) custom-call(s32[3]{0:T(128)S(1)} %pad_add_fusion.place_ref, f32[2,64,32,256]{3,2,1,0:T(8,128)} %cell_ref.3, ...), custom_call_target="tpu_custom_call" | custom-call | tf_op jit(solution)/shard_map/front_later/pallas_call | solution.py:194
  114.6 8.4 %all_to_all.28.everyone_ref.refs_1_ = bf16[8,48,128]{2,1,0:T(8,128)(2,1)S(1)} all-to-all(bf16[8,48,128]{2,1,0:T(8,128)(2,1)S(1)} %get-tuple-element.35), channel_id=1, replica_groups={{0,1,2,3,4,5,6,7},{8,9,10,11,12,13,14,15},{16,17,18,19,20,21,22,23},{24..., dimensions={0} | all-to-all | bytes 196608 | tf_op jit(solution)/shard_map/all_to_all | solution.py:28
  123.1 1.2 read.3
  124.3 26.3 %all_to_all.29 = bf16[16,16,128]{2,1,0:T(8,128)(2,1)S(1)} all-to-all(bf16[16,16,128]{2,1,0:T(8,128)(2,1)S(1)} %read.3), channel_id=1, replica_groups={{0,4,8,12,16,20,24,28,32,36,40,44,48,52,56,60},{1,5,9,13,17,21,25,29,33..., dimensions={0} | all-to-all | bytes 131072 | tf_op jit(solution)/shard_map/all_to_all | solution.py:28
  150.5 0.2 collective-permute-start.7
  150.7 3.3 %collective-permute-start.6 = (bf16[256,128]{1,0:T(8,128)(2,1)S(1)}, bf16[256,128]{1,0:T(8,128)(2,1)S(1)}, u32[]{:S(2)}, u32[]{:S(2)}) collective-permute-start(bf16[256,128]{1,0:T(8,128)(2,1)S(1)} %bitcast.13), channel_id=1, source_target_pairs={{0,1},{1,0},{2,3},{3,2},{4,5},{5,4},{6,7},{7,6},{8,9},{9,8},{10,11... | collective-permute-start | bytes 196616 | tf_op jit(solution)/shard_map/ppermute | solution.py:33
  154.0 4.8 %update.1 = (f32[2,64,32,256]{3,2,1,0:T(8,128)}, f32[2,32,64]{2,1,0:T(8,128)}, f32[2,8,64]{2,1,0:T(8,128)}) custom-call(bf16[8,48,128]{2,1,0:T(8,128)(2,1)S(1)} %all_to_all.25.everyone_ref.refs_0_, bf16[8,48,128]{2,1,0:T(8,128)(2,1)S(1)} %all_to_all.28.everyone_ref.refs_1_, f32[32,64]{1,0:T(8,128)S(1)} %get-tuple-element.29.value_ref.refs_2_, ...), custom_call_target="tpu_custom_call" | custom-call | tf_op jit(solution)/shard_map/update/pallas_call | solution.py:312
  158.8 0.0 collective-permute-done.7.second_ref
  158.8 0.2 collective-permute-start.8
  159.0 0.0 collective-permute-done.6.first_ref
  159.0 1.2 collective-permute-done.8.third_ref
  160.2 1.5 proj.3
Async XLA Ops:
  0.6 76.0 %copy-start.4 = (bf16[2,32,2048]{2,1,0:T(8,128)(2,1)S(1)}, bf16[2,32,2048]{2,1,0:T(8,128)(2,1)}, u32[]{:S(2)}) copy-start(bf16[2,32,2048]{2,1,0:T(8,128)(2,1)} %weight_ref.3) | copy-start | bytes 786436
  0.7 110.7 %copy-start = (bf16[2,32,2048]{2,1,0:T(8,128)(2,1)S(1)}, bf16[2,32,2048]{2,1,0:T(8,128)(2,1)}, u32[]{:S(2)}) copy-start(bf16[2,32,2048]{2,1,0:T(8,128)(2,1)} %wq_ref.3) | copy-start | bytes 786436
  0.7 110.7 %copy-start.1 = (bf16[2,32,2048]{2,1,0:T(8,128)(2,1)S(1)}, bf16[2,32,2048]{2,1,0:T(8,128)(2,1)}, u32[]{:S(2)}) copy-start(bf16[2,32,2048]{2,1,0:T(8,128)(2,1)} %wk_ref.3) | copy-start | bytes 786436
  0.7 110.7 %copy-start.2 = (bf16[2,32,2048]{2,1,0:T(8,128)(2,1)S(1)}, bf16[2,32,2048]{2,1,0:T(8,128)(2,1)}, u32[]{:S(2)}) copy-start(bf16[2,32,2048]{2,1,0:T(8,128)(2,1)} %wv_ref.3) | copy-start | bytes 786436
  0.8 110.7 %copy-start.3 = (bf16[2,32,2048]{2,1,0:T(8,128)(2,1)S(1)}, bf16[2,32,2048]{2,1,0:T(8,128)(2,1)}, u32[]{:S(2)}) copy-start(bf16[2,32,2048]{2,1,0:T(8,128)(2,1)} %wo_ref.3) | copy-start | bytes 786436
  0.8 110.7 %copy-start.5 = (bf16[2,2048,16]{1,2,0:T(8,128)(2,1)S(1)}, bf16[2,2048,16]{1,2,0:T(8,128)(2,1)}, u32[]{:S(2)}) copy-start(bf16[2,2048,16]{1,2,0:T(8,128)(2,1)} %param.18) | copy-start | bytes 393220
  0.8 110.7 %copy-start.6 = (f32[2,64,32]{1,2,0:T(8,128)S(1)}, f32[2,64,32]{1,2,0:T(8,128)}, u32[]{:S(2)}) copy-start(f32[2,64,32]{1,2,0:T(8,128)} %param.22) | copy-start | bytes 49156
  0.8 110.7 %copy-start.7 = (f32[2,2048]{1,0:T(2,128)S(1)}, f32[2,2048]{1,0:T(2,128)}, u32[]{:S(2)}) copy-start(f32[2,2048]{1,0:T(2,128)} %gain_ref.3) | copy-start | bytes 49156
  0.8 110.7 %copy-start.8 = (f32[2,64,8]{1,2,0:T(8,128)S(1)}, f32[2,64,8]{1,2,0:T(8,128)}, u32[]{:S(2)}) copy-start(f32[2,64,8]{1,2,0:T(8,128)} %param.23) | copy-start | bytes 12292
  0.8 110.7 %copy-start.9 = (f32[2,8]{1,0:T(2,128)S(1)}, f32[2,8]{1,0:T(2,128)}, u32[]{:S(2)}) copy-start(f32[2,8]{1,0:T(2,128)} %rest_0_.3) | copy-start | bytes 196
  68.0 3.5 %collective-permute-start.1 = (bf16[256,128]{1,0:T(8,128)(2,1)S(1)}, bf16[256,128]{1,0:T(8,128)(2,1)S(1)}, u32[]{:S(2)}, u32[]{:S(2)}) collective-permute-start(bf16[256,128]{1,0:T(8,128)(2,1)S(1)} %bitcast.21), channel_id=1, source_target_pairs={{0,2},{1,3},{2,0},{3,1},{4,6},{5,7},{6,4},{7,5},{8,10},{9,11},{10,... | collective-permute-start | bytes 196616 | tf_op jit(solution)/shard_map/ppermute | solution.py:33
  68.2 7.6 %collective-permute-start = (bf16[256,128]{1,0:T(8,128)(2,1)S(1)}, bf16[256,128]{1,0:T(8,128)(2,1)S(1)}, u32[]{:S(2)}, u32[]{:S(2)}) collective-permute-start(bf16[256,128]{1,0:T(8,128)(2,1)S(1)} %bitcast.22), channel_id=1, source_target_pairs={{0,1},{1,0},{2,3},{3,2},{4,5},{5,4},{6,7},{7,6},{8,9},{9,8},{10,11... | collective-permute-start | bytes 196616 | tf_op jit(solution)/shard_map/ppermute | solution.py:33
  71.5 5.2 %collective-permute-start.2 = (bf16[256,128]{1,0:T(8,128)(2,1)S(1)}, bf16[256,128]{1,0:T(8,128)(2,1)S(1)}, u32[]{:S(2)}, u32[]{:S(2)}) collective-permute-start(bf16[256,128]{1,0:T(8,128)(2,1)S(1)} %collective-permute-done.1.second_ref), channel_id=1, source_target_pairs={{0,1},{1,0},{2,3},{3,2},{4,5},{5,4},{6,7},{7,6},{8,9},{9,8},{10,11... | collective-permute-start | bytes 196616 | tf_op jit(solution)/shard_map/ppermute | solution.py:33
  103.1 3.2 %collective-permute-start.4 = (bf16[256,128]{1,0:T(8,128)(2,1)S(1)}, bf16[256,128]{1,0:T(8,128)(2,1)S(1)}, u32[]{:S(2)}, u32[]{:S(2)}) collective-permute-start(bf16[256,128]{1,0:T(8,128)(2,1)S(1)} %bitcast.18), channel_id=1, source_target_pairs={{0,2},{1,3},{2,0},{3,1},{4,6},{5,7},{6,4},{7,5},{8,10},{9,11},{10,... | collective-permute-start | bytes 196616 | tf_op jit(solution)/shard_map/ppermute | solution.py:33
  103.1 7.5 %collective-permute-start.3 = (bf16[256,128]{1,0:T(8,128)(2,1)S(1)}, bf16[256,128]{1,0:T(8,128)(2,1)S(1)}, u32[]{:S(2)}, u32[]{:S(2)}) collective-permute-start(bf16[256,128]{1,0:T(8,128)(2,1)S(1)} %bitcast.19), channel_id=1, source_target_pairs={{0,1},{1,0},{2,3},{3,2},{4,5},{5,4},{6,7},{7,6},{8,9},{9,8},{10,11... | collective-permute-start | bytes 196616 | tf_op jit(solution)/shard_map/ppermute | solution.py:33
  106.3 5.2 %collective-permute-start.5 = (bf16[256,128]{1,0:T(8,128)(2,1)S(1)}, bf16[256,128]{1,0:T(8,128)(2,1)S(1)}, u32[]{:S(2)}, u32[]{:S(2)}) collective-permute-start(bf16[256,128]{1,0:T(8,128)(2,1)S(1)} %collective-permute-done.4.second_ref), channel_id=1, source_target_pairs={{0,1},{1,0},{2,3},{3,2},{4,5},{5,4},{6,7},{7,6},{8,9},{9,8},{10,11... | collective-permute-start | bytes 196616 | tf_op jit(solution)/shard_map/ppermute | solution.py:33
  150.5 8.3 %collective-permute-start.7 = (bf16[256,128]{1,0:T(8,128)(2,1)S(1)}, bf16[256,128]{1,0:T(8,128)(2,1)S(1)}, u32[]{:S(2)}, u32[]{:S(2)}) collective-permute-start(bf16[256,128]{1,0:T(8,128)(2,1)S(1)} %bitcast.12), channel_id=1, source_target_pairs={{0,2},{1,3},{2,0},{3,1},{4,6},{5,7},{6,4},{7,5},{8,10},{9,11},{10,... | collective-permute-start | bytes 196616 | tf_op jit(solution)/shard_map/ppermute | solution.py:33
  150.7 8.3 %collective-permute-start.6 = (bf16[256,128]{1,0:T(8,128)(2,1)S(1)}, bf16[256,128]{1,0:T(8,128)(2,1)S(1)}, u32[]{:S(2)}, u32[]{:S(2)}) collective-permute-start(bf16[256,128]{1,0:T(8,128)(2,1)S(1)} %bitcast.13), channel_id=1, source_target_pairs={{0,1},{1,0},{2,3},{3,2},{4,5},{5,4},{6,7},{7,6},{8,9},{9,8},{10,11... | collective-permute-start | bytes 196616 | tf_op jit(solution)/shard_map/ppermute | solution.py:33
  158.8 1.4 collective-permute-start.8

commit v3 on v2

--- a/solution.py
+++ b/solution.py
@@ -11,6 +11,7 @@
 NEAR = 4
 CHUNKS = 4
 UNROLLED = 8
+PIECES = 8
 F32 = jnp.float32
 BF16 = jnp.bfloat16
 LIMITED = pltpu.CompilerParams(vmem_limit_bytes=16 * 2**20)
@@ -52,6 +53,10 @@
 
 def one_layer(shape, layer):
     return pl.BlockSpec((None, *shape), lambda *_: (layer,) + (0,) * len(shape))
+
+
+def anywhere():
+    return pl.BlockSpec(memory_space=pl.ANY)
 
 
 def smem():
@@ -113,11 +118,35 @@
     new_stab_ref[...] = new_stab
 
 
-def first_front(place_ref, cell_ref, tokens_ref, gain_ref, wq_ref, wk_ref, wv_ref, wo_ref, wg_ref, *rest, head_size):
-    *rest, held_ref, own_ref, arrived = rest
-    fetch = pltpu.make_async_copy(cell_ref.at[0], held_ref, arrived)
-    fetch.start()
+def fetched(source_ref, target_ref, arrived, pieces):
+    size = target_ref.shape[0] // pieces
+    return [
+        pltpu.make_async_copy(source_ref.at[pl.ds(k * size, size)], target_ref.at[pl.ds(k * size, size)], arrived.at[k])
+        for k in range(pieces)
+    ]
+
+
+def first_front(
+    place_ref, cell_ref, tokens_hbm, gain_hbm, wq_hbm, wk_hbm, wv_hbm, wo_hbm, wg_hbm, bias_hbm, stab_hbm, norm_hbm, *rest, head_size
+):
+    *outs, held_ref, own_ref, arrived, loaded, tokens_ref, gain_ref, weights_ref, bias_ref, stab_ref, norm_ref = rest
     columns = own_ref.shape[0]
+    gates = wg_hbm.shape[1]
+    sources = [tokens_hbm, gain_hbm, bias_hbm, stab_hbm.at[0], norm_hbm.at[0]]
+    targets = [tokens_ref, gain_ref, bias_ref, stab_ref, norm_ref]
+    for k, weight in enumerate((wq_hbm, wk_hbm, wv_hbm, wo_hbm)):
+        sources.append(weight.at[0])
+        targets.append(weights_ref.at[pl.ds(k * columns, columns)])
+    sources.append(wg_hbm.at[0])
+    targets.append(weights_ref.at[pl.ds(4 * columns, gates)])
+    loads = [pltpu.make_async_copy(a, b, loaded.at[k]) for k, (a, b) in enumerate(zip(sources, targets))]
+    for load in loads:
+        load.start()
+    fetches = fetched(cell_ref.at[0], held_ref, arrived, PIECES)
+    for fetch in fetches:
+        fetch.start()
+    loads[0].wait()
+    loads[1].wait()
     near = NEAR * columns
     nearby = tokens_ref[:, pl.ds(pl.multiple_of(place_ref[2] * near, near), near)].astype(F32)
     turned = pltpu.roll(nearby, (NEAR - place_ref[1]) % NEAR * columns, 1).T
@@ -125,16 +154,16 @@
     current = tokens_ref[...].astype(F32)
     scale = lax.rsqrt(jnp.mean(current * current, axis=1, keepdims=True) + EPSILON)
     normed = (current * scale * gain_ref[0:1, :]).astype(BF16)
-    weights = jnp.concatenate([wq_ref[...], wk_ref[...], wv_ref[...], wo_ref[...], wg_ref[...]])
-    outs = lax.dot_general(weights, normed, (((1,), (1,)), ((), ())), preferred_element_type=F32)
-    front_rest(0, place_ref, outs, *rest, head_size=head_size)
-    fetch.wait()
-
-
-def later_front(place_ref, cell_ref, own_ref, first_ref, second_ref, third_ref, gain_ref, wq_ref, wk_ref, wv_ref, wo_ref, wg_ref, *rest, layer, head_size):
-    *rest, held_ref, arrived, stage_ref, normed_ref = rest
-    fetch = pltpu.make_async_copy(cell_ref.at[layer], held_ref, arrived)
-    fetch.start()
+    for load in loads[2:]:
+        load.wait()
+    dots = lax.dot_general(weights_ref[...], normed, (((1,), (1,)), ((), ())), preferred_element_type=F32)
+    front_rest(0, place_ref, dots, bias_ref, stab_ref, norm_ref, *outs, head_size=head_size)
+    for fetch in fetches:
+        fetch.wait()
+
+
+def later_front(place_ref, own_ref, first_ref, second_ref, third_ref, gain_ref, wq_ref, wk_ref, wv_ref, wo_ref, wg_ref, *rest, layer, head_size):
+    *rest, stage_ref, normed_ref = rest
     unpack(place_ref, (own_ref, first_ref, second_ref, third_ref), stage_ref)
     far, per, batch = stage_ref.shape
     current = stage_ref[...].astype(F32)
@@ -146,11 +175,31 @@
     weights = jnp.concatenate([wq_ref[...], wk_ref[...], wv_ref[...], wo_ref[...], wg_ref[...]])
     outs = jnp.dot(weights, normed_ref[...], preferred_element_type=F32)
     front_rest(layer, place_ref, outs, *rest, head_size=head_size)
-    fetch.wait()
 
 
 def in_hbm(*values):
     return [pltpu.with_memory_space_constraint(value, pltpu.HBM) for value in values]
+
+
+def fetch_kernel(layer, cell_ref, after_ref, held_ref, arrived):
+    del after_ref
+    fetches = fetched(cell_ref.at[layer], held_ref, arrived, PIECES)
+    for fetch in fetches:
+        fetch.start()
+    for fetch in fetches:
+        fetch.wait()
+
+
+def fetch(layer, cell, after):
+    return pl.pallas_call(
+        functools.partial(fetch_kernel, layer),
+        out_shape=jax.ShapeDtypeStruct(cell.shape[1:], F32),
+        in_specs=[anywhere()] * 2,
+        out_specs=anywhere(),
+        scratch_shapes=[pltpu.SemaphoreType.DMA((PIECES,))],
+        compiler_params=LIMITED,
+        name="fetch",
+    )(*in_hbm(cell), after)
 
 
 def front(layer, place, current, norm_gain, projections, gates, bias, stab, norm, cell):
@@ -159,52 +208,59 @@
     head_size = cell.shape[-1]
     group = head_size // columns
     far = lax.axis_size("tp") // NEAR
-    out_shape = (
+    out_shape = [
         jax.ShapeDtypeStruct((group, columns + 16, 2 * batch), BF16),
         jax.ShapeDtypeStruct((columns, batch), F32),
         jax.ShapeDtypeStruct((columns, batch), F32),
         jax.ShapeDtypeStruct((8, 2 * batch), F32),
         jax.ShapeDtypeStruct((columns, batch), F32),
         jax.ShapeDtypeStruct((heads, batch), F32),
-        jax.ShapeDtypeStruct(cell.shape[1:], F32),
-    )
-    out_specs = [whole(out.shape) for out in out_shape[:-1]] + [pl.BlockSpec(memory_space=pl.ANY)]
-    tail_specs = [whole(norm_gain.shape)] + [one_layer((columns, width), layer)] * 4 + [
-        one_layer((2 * heads, width), layer),
-        whole(bias.shape),
-        one_layer((heads, batch), layer),
-        one_layer((columns, batch), layer),
     ]
-    tail = (norm_gain, *projections, gates, bias, stab, norm)
-    head_specs = [smem(), pl.BlockSpec(memory_space=pl.ANY)]
+    out_specs = [whole(out.shape) for out in out_shape]
     if layer == 0:
-        out_shape = (*out_shape, jax.ShapeDtypeStruct((columns, batch), BF16))
-        out_specs.append(whole((columns, batch)))
+        operands = (cell, current, norm_gain, *projections, gates, bias, stab, norm)
         return pl.pallas_call(
             functools.partial(first_front, head_size=head_size),
             grid=(1,),
-            out_shape=out_shape,
-            out_specs=out_specs,
-            in_specs=head_specs + [whole((batch, width))] + tail_specs,
-            scratch_shapes=[pltpu.SemaphoreType.DMA],
+            out_shape=out_shape + [jax.ShapeDtypeStruct(cell.shape[1:], F32), jax.ShapeDtypeStruct((columns, batch), BF16)],
+            out_specs=out_specs + [anywhere(), whole((columns, batch))],
+            in_specs=[smem()] + [anywhere()] * len(operands),
+            scratch_shapes=[
+                pltpu.SemaphoreType.DMA((PIECES,)),
+                pltpu.SemaphoreType.DMA((10,)),
+                pltpu.VMEM((batch, width), BF16),
+                pltpu.VMEM(norm_gain.shape, F32),
+                pltpu.VMEM((4 * columns + 2 * heads, width), BF16),
+                pltpu.VMEM(bias.shape, F32),
+                pltpu.VMEM((heads, batch), F32),
+                pltpu.VMEM((columns, batch), F32),
+            ],
             compiler_params=LIMITED,
             name="front_first",
-        )(place, *in_hbm(cell, current, *tail))
+        )(place, *in_hbm(*operands))
     per = width // far
     return pl.pallas_call(
         functools.partial(later_front, layer=layer, head_size=head_size),
         grid=(1,),
         out_shape=out_shape,
         out_specs=out_specs,
-        in_specs=head_specs + [whole(current[0].shape)] * 4 + tail_specs,
+        in_specs=[smem()]
+        + [whole(current[0].shape)] * 4
+        + [whole(norm_gain.shape)]
+        + [one_layer((columns, width), layer)] * 4
+        + [
+            one_layer((2 * heads, width), layer),
+            whole(bias.shape),
+            one_layer((heads, batch), layer),
+            one_layer((columns, batch), layer),
+        ],
         scratch_shapes=[
-            pltpu.SemaphoreType.DMA,
             pltpu.VMEM((far, per, batch), BF16),
             pltpu.VMEM((width, batch), BF16),
         ],
         compiler_params=LIMITED,
         name="front_later",
-    )(place, *in_hbm(cell), *current, *tail)
+    )(place, *current, norm_gain, *projections, gates, bias, stab, norm)
 
 
 def head_rows(everyone_ref, columns):
@@ -259,80 +315,80 @@
     )(*operands)
 
 
-def update_kernel(layers, *refs):
-    everyone_refs, value_refs, rows_refs, held_refs, norm_refs, stab_refs = (
-        refs[k * layers : (k + 1) * layers] for k in range(6)
-    )
-    _, cell_ref, norms_ref, stabs_ref, turned_ref, decay_ref, added_ref = refs[6 * layers :]
-    step = pl.program_id(0) % CHUNKS
+def update_kernel(everyone_ref, value_ref, rows_ref, held_ref, *rest):
+    *small, cell_ref, turned_ref, decay_ref, added_ref = rest
+    step = pl.program_id(0)
     chunk, columns, keys = cell_ref.shape
     batch = added_ref.shape[1] // 2
 
-    def one(layer):
-        @pl.when(step == 0)
-        def _():
-            rows = rows_refs[layer]
-            turned_ref[...] = head_rows(everyone_refs[layer], columns).T
-            decay_ref[...] = jnp.broadcast_to(rows[0:1, :], (2 * batch, 2 * batch)).T
-            scaled = value_refs[layer][...] * rows[0:1, batch:]
-            added_ref[...] = jnp.concatenate([scaled, scaled], axis=1)
-            norms_ref[layer] = norm_refs[layer][...]
-            stabs_ref[layer] = stab_refs[layer][...]
-
-        added = pltpu.roll(added_ref[...], batch - step * chunk, 1)
-        for i in range(chunk):
-            b = step * chunk + i
-            key = turned_ref[pl.ds(batch + b, 1), :]
-            decay = decay_ref[pl.ds(b, 1), :]
-            decay = jnp.concatenate([decay] * (keys // decay.shape[1]), axis=1)
-            cell_ref[i] = decay * held_refs[layer][i] + added[:, i : i + 1] * key
-
-    for layer in range(layers):
-        pl.when(pl.program_id(0) // CHUNKS == layer)(functools.partial(one, layer))
-
-
-def update(memory, after):
-    layers = len(memory)
-    everyone, value, rows, held, norm, stab = zip(*memory)
-    columns, batch = value[0].shape
-    keys = held[0].shape[-1]
+    @pl.when(step == 0)
+    def _():
+        turned_ref[...] = head_rows(everyone_ref, columns).T
+        decay_ref[...] = jnp.broadcast_to(rows_ref[0:1, :], (2 * batch, 2 * batch)).T
+        scaled = value_ref[...] * rows_ref[0:1, batch:]
+        added_ref[...] = jnp.concatenate([scaled, scaled], axis=1)
+
+    added = pltpu.roll(added_ref[...], batch - step * chunk, 1)
+    for i in range(chunk):
+        b = step * chunk + i
+        key = turned_ref[pl.ds(batch + b, 1), :]
+        decay = decay_ref[pl.ds(b, 1), :]
+        decay = jnp.concatenate([decay] * (keys // decay.shape[1]), axis=1)
+        cell_ref[i] = decay * held_ref[i] + added[:, i : i + 1] * key
+
+
+def update(layer, layers, everyone, value, rows, held, into, after):
+    columns, batch = value.shape
+    keys = held.shape[-1]
     chunk = batch // CHUNKS
-    out_shape = (
-        jax.ShapeDtypeStruct((layers, *held[0].shape), F32),
-        jax.ShapeDtypeStruct((layers, *norm[0].shape), F32),
-        jax.ShapeDtypeStruct((layers, *stab[0].shape), F32),
-    )
-
-    def held_spec(layer):
-        return pl.BlockSpec((chunk, columns, keys), lambda i: (jnp.clip(i - layer * CHUNKS, 0, CHUNKS - 1), 0, 0))
-
-    def wholes(values):
-        return [whole(each.shape) for each in values]
-
-    return pl.pallas_call(
-        functools.partial(update_kernel, layers),
-        grid=(layers * CHUNKS,),
-        out_shape=out_shape,
-        in_specs=wholes(everyone)
-        + wholes(value)
-        + wholes(rows)
-        + [held_spec(layer) for layer in range(layers)]
-        + wholes(norm)
-        + wholes(stab)
-        + [pl.BlockSpec(memory_space=pl.ANY)],
-        out_specs=(
-            pl.BlockSpec((None, chunk, columns, keys), lambda i: (i // CHUNKS, i % CHUNKS, 0, 0)),
-            whole(out_shape[1].shape),
-            whole(out_shape[2].shape),
-        ),
+    operands = [everyone, value, rows, held, after]
+    in_specs = [
+        whole(everyone.shape),
+        whole(value.shape),
+        whole(rows.shape),
+        pl.BlockSpec((chunk, columns, keys), lambda i: (i, 0, 0)),
+        anywhere(),
+    ]
+    aliases = {}
+    if into is not None:
+        operands.extend(in_hbm(into))
+        in_specs.append(anywhere())
+        aliases = {5: 0}
+    return pl.pallas_call(
+        update_kernel,
+        grid=(CHUNKS,),
+        out_shape=jax.ShapeDtypeStruct((layers, *held.shape), F32),
+        in_specs=in_specs,
+        out_specs=pl.BlockSpec((None, chunk, columns, keys), lambda i: (layer, i, 0, 0)),
         scratch_shapes=[
             pltpu.VMEM((2 * batch, keys), F32),
             pltpu.VMEM((2 * batch, 2 * batch), F32),
             pltpu.VMEM((columns, 2 * batch), F32),
         ],
+        input_output_aliases=aliases,
         compiler_params=LIMITED,
         name="update",
-    )(*everyone, *value, *rows, *held, *norm, *stab, after)
+    )(*operands)
+
+
+def stack_kernel(layers, *refs):
+    for layer in range(layers):
+        refs[-2][layer] = refs[layer][...]
+        refs[-1][layer] = refs[layers + layer][...]
+
+
+def stacked(norms, stabs):
+    layers = len(norms)
+    out_shape = [jax.ShapeDtypeStruct((layers, *each[0].shape), F32) for each in (norms, stabs)]
+    return pl.pallas_call(
+        functools.partial(stack_kernel, layers),
+        grid=(1,),
+        out_shape=out_shape,
+        in_specs=[whole(each.shape) for each in (*norms, *stabs)],
+        out_specs=[whole(out.shape) for out in out_shape],
+        compiler_params=LIMITED,
+        name="stack",
+    )(*norms, *stabs)
 
 
 def proj_result(place_ref, pieces, weight_ref, residual_ref, stage_ref):
@@ -384,24 +440,30 @@
     stab = stabilizer.transpose(0, 2, 1)
     norm = normalizer.transpose(0, 2, 1)
     projections = (query_weight, key_weight, value_weight, outgate_weight)
-    residual = None
     current = tokens
-    memory = []
+    cells = None
+    held = [None] * layers
+    norms, stabs = [], []
     for layer in range(layers):
-        message, value, opened, rows, new_norm, new_stab, held, *own_input = front(
+        last = layer + 1 == layers
+        message, value, opened, rows, new_norm, new_stab, *more = front(
             layer, place, current, norm_gain, projections, gates, forget_bias, stab, norm, cell_state
         )
-        residual = own_input[0] if own_input else residual
+        norms.append(new_norm)
+        stabs.append(new_stab)
+        if layer == 0:
+            held[0], residual = more
         everyone = exchanged(message, near_groups(lax.axis_size("tp"), group))
-        copies = read(everyone, value, opened, rows, held)
-        memory.append((everyone, value, rows, held, new_norm, new_stab))
-        last = layer + 1 == layers
-        pieces, states = gathered(copies, functools.partial(update, memory) if last else None)
-        residual, *copies = proj(layer, place, pieces, proj_weight, residual, not last)
-        if not last:
-            current, _ = gathered(copies[0])
-    cells, norms, stabs = states
-    return (residual.T, cells, norms.transpose(0, 2, 1), stabs.transpose(0, 2, 1))
+        copies = read(everyone, value, opened, rows, held[layer])
+        write = functools.partial(update, layer, layers, everyone, value, rows, held[layer], cells)
+        if last:
+            pieces, (cells, small) = gathered(copies, lambda own: (write(own), stacked(norms, stabs)))
+            (residual,) = proj(layer, place, pieces, proj_weight, residual, False)
+        else:
+            pieces, held[layer + 1] = gathered(copies, functools.partial(fetch, layer + 1, cell_state))
+            residual, copies = proj(layer, place, pieces, proj_weight, residual, True)
+            current, cells = gathered(copies, write)
+    return (residual.T, cells, small[0].transpose(0, 2, 1), small[1].transpose(0, 2, 1))
 
 
 def solution(mesh):

time: 162 us -> 160 us (0.988)
  starting transfers between devices: 18.9 us -> 15.7 us
    ppermute x9, starting transfers between devices: 18.9 us -> 15.7 us  [from_partner(): return lax.ppermute(value, 'tp', pairs)]
    pallas_call x1 -> x4, Pallas kernels: 4.79 us -> 7.2 us  [the longest x2 5.01 us: update(): pl.pallas_call(update_kernel, grid=(CHUNKS,), out_shape=jax.ShapeDtypeStr...]
  transfers between devices with their start and end apart: 9 -> 9, of which waited for: 3 -> 3; matrix products, arithmetic and copies ran while one was open for 0% -> 0% of each run, Pallas kernels for 3% -> 5%
where the time goes in v3:
time: 160 us; the launch traced here: 159 us
  blocking collectives  123 us (77%)
  Pallas kernels  16.8 us (10%)
  starting transfers between devices  15.7 us (10%)
  waiting for transfers between devices  2.71 us (2%)
    all_to_all x5, blocking collectives, exchanged(): lax.all_to_all(copies, 'tp', 0, 0, tiled=True, axis_index_groups=groups)  123 us
    ppermute x9, starting transfers between devices, from_partner(): return lax.ppermute(value, 'tp', pairs)  15.7 us
    pallas_call x2, Pallas kernels, update(): pl.pallas_call(update_kernel, grid=(CHUNKS,), out_shape=jax.ShapeDtypeStr...  5.01 us
  transfers between devices with their start and end apart: 9, of which 3 were waited for; matrix products, arithmetic and copies ran while one was open for 0% of the time, Pallas kernels for 5%

profile of v3, /device:TPU:37, one launch (start us, length us, event | category | flops | bytes accessed | tf_op | source)
XLA Modules:
  0.0 159.4 jit_solution(12468285168993048277)
XLA Ops:
  0.7 0.1 pad_add_fusion.place_ref
  0.7 2.8 %front_first.1 = (bf16[8,48,128]{2,1,0:T(8,128)(2,1)S(1)}, f32[32,64]{1,0:T(8,128)S(1)}, f32[32,64]{1,0:T(8,128)S(1)}, f32[8,128]{1,0:T(8,128)S(1)}, f32[32,64]{...) custom-call(s32[3]{0:T(128)S(1)} %pad_add_fusion.place_ref, ...), custom_call_target="tpu_custom_call" | custom-call | tf_op jit(solution)/shard_map/front_first/pallas_call | solution.py:222
  3.6 28.3 %all_to_all.25.everyone_ref = bf16[8,48,128]{2,1,0:T(8,128)(2,1)S(1)} all-to-all(bf16[8,48,128]{2,1,0:T(8,128)(2,1)S(1)} %get-tuple-element.30), channel_id=1, replica_groups={{0,1,2,3,4,5,6,7},{8,9,10,11,12,13,14,15},{16,17,18,19,20,21,22,23},{24..., dimensions={0} | all-to-all | bytes 196608 | tf_op jit(solution)/shard_map/all_to_all | solution.py:29
  31.8 0.0 copy-start.4
  31.8 1.2 read.2
  33.0 34.8 %all_to_all.26 = bf16[16,16,128]{2,1,0:T(8,128)(2,1)S(1)} all-to-all(bf16[16,16,128]{2,1,0:T(8,128)(2,1)S(1)} %read.2), channel_id=1, replica_groups={{0,4,8,12,16,20,24,28,32,36,40,44,48,52,56,60},{1,5,9,13,17,21,25,29,33..., dimensions={0} | all-to-all | bytes 131072 | tf_op jit(solution)/shard_map/all_to_all | solution.py:29
  67.8 0.2 collective-permute-start.1
  68.0 3.3 %collective-permute-start = (bf16[256,128]{1,0:T(8,128)(2,1)S(1)}, bf16[256,128]{1,0:T(8,128)(2,1)S(1)}, u32[]{:S(2)}, u32[]{:S(2)}) collective-permute-start(bf16[256,128]{1,0:T(8,128)(2,1)S(1)} %bitcast.21), channel_id=1, source_target_pairs={{0,1},{1,0},{2,3},{3,2},{4,5},{5,4},{6,7},{7,6},{8,9},{9,8},{10,11... | collective-permute-start | bytes 196616 | tf_op jit(solution)/shard_map/ppermute | solution.py:34
  71.4 1.6 fetch.1.cell_ref.held_ref
  72.9 0.0 copy-start
  73.0 0.0 copy-start.1
  73.0 0.0 copy-start.2
  73.0 0.0 copy-start.3
  73.0 0.0 copy-start.5
  73.0 0.0 copy-start.6
  73.0 0.0 copy-start.7
  73.0 0.0 copy-start.8
  73.0 0.0 copy-start.9
  73.1 0.0 collective-permute-done.1.second_ref
  73.1 2.6 %collective-permute-start.2 = (bf16[256,128]{1,0:T(8,128)(2,1)S(1)}, bf16[256,128]{1,0:T(8,128)(2,1)S(1)}, u32[]{:S(2)}, u32[]{:S(2)}) collective-permute-start(bf16[256,128]{1,0:T(8,128)(2,1)S(1)} %collective-permute-done.1.second_ref), channel_id=1, source_target_pairs={{0,1},{1,0},{2,3},{3,2},{4,5},{5,4},{6,7},{7,6},{8,9},{9,8},{10,11... | collective-permute-start | bytes 196616 | tf_op jit(solution)/shard_map/ppermute | solution.py:34
  75.6 0.0 collective-permute-done.first_ref
  75.6 0.9 collective-permute-done.2.third_ref
  76.5 0.0 copy-done.4
  76.5 1.0 proj.2
  77.6 25.4 %all_to_all.27 = bf16[16,16,128]{2,1,0:T(8,128)(2,1)S(1)} all-to-all(bf16[16,16,128]{2,1,0:T(8,128)(2,1)S(1)} %get-tuple-element.37), channel_id=1, replica_groups={{0,4,8,12,16,20,24,28,32,36,40,44,48,52,56,60},{1,5,9,13,17,21,25,29,33..., dimensions={0} | all-to-all | bytes 131072 | tf_op jit(solution)/shard_map/all_to_all | solution.py:29
  103.0 0.0 collective-permute-start.4
  103.0 3.2 %collective-permute-start.3 = (bf16[256,128]{1,0:T(8,128)(2,1)S(1)}, bf16[256,128]{1,0:T(8,128)(2,1)S(1)}, u32[]{:S(2)}, u32[]{:S(2)}) collective-permute-start(bf16[256,128]{1,0:T(8,128)(2,1)S(1)} %bitcast.17), channel_id=1, source_target_pairs={{0,1},{1,0},{2,3},{3,2},{4,5},{5,4},{6,7},{7,6},{8,9},{9,8},{10,11... | collective-permute-start | bytes 196616 | tf_op jit(solution)/shard_map/ppermute | solution.py:34
  106.2 2.5 %update.2.rest_1_ = f32[2,64,32,256]{3,2,1,0:T(8,128)} custom-call(bf16[8,48,128]{2,1,0:T(8,128)(2,1)S(1)} %all_to_all.25.everyone_ref, f32[32,64]{1,0:T(8,128)S(1)} %get-tuple-element.31.value_ref, f32[8,128]{1,0:T(8,128)S(1)} %get-tuple-element.33.rows_ref, f32[64,32,256]{2,1,0:T(8,128)S(1)} %get-tuple-element.34.cell_ref.held_ref, ...), custom_call_target="tpu_custom_call" | custom-call | tf_op jit(solution)/shard_map/update/pallas_call | solution.py:357
  108.7 0.0 collective-permute-done.4.second_ref
  108.7 1.8 %collective-permute-start.5 = (bf16[256,128]{1,0:T(8,128)(2,1)S(1)}, bf16[256,128]{1,0:T(8,128)(2,1)S(1)}, u32[]{:S(2)}, u32[]{:S(2)}) collective-permute-start(bf16[256,128]{1,0:T(8,128)(2,1)S(1)} %collective-permute-done.4.second_ref), channel_id=1, source_target_pairs={{0,1},{1,0},{2,3},{3,2},{4,5},{5,4},{6,7},{7,6},{8,9},{9,8},{10,11... | collective-permute-start | bytes 196616 | tf_op jit(solution)/shard_map/ppermute | solution.py:34
  110.4 0.0 collective-permute-done.3.first_ref
  110.4 0.9 collective-permute-done.5.third_ref
  111.3 0.0 copy-done
  111.3 0.0 copy-done.1
  111.3 0.0 copy-done.2
  111.3 0.0 copy-done.3
  111.3 0.0 copy-done.5
  111.4 0.0 copy-done.6
  111.4 0.0 copy-done.7
  111.4 0.0 copy-done.8
  111.4 0.0 copy-done.9
  111.4 1.8 %front_later.1 = (bf16[8,48,128]{2,1,0:T(8,128)(2,1)S(1)}, f32[32,64]{1,0:T(8,128)S(1)}, f32[32,64]{1,0:T(8,128)S(1)}, f32[8,128]{1,0:T(8,128)S(1)}, f32[32,64]{1,0:T(8,128)S(1)}, /*index=5*/f32[8,64]{1,0:T(8,128)S(1)}) custom-call(s32[3]{0:T(128)S(1)} %pad_add_fusion.place_ref, bf16[256,128]{1,0:T(8,128)(2,1)S(1)} %bitcast.19, ...), custom_call_target="tpu_custom_call" | custom-call | tf_op jit(solution)/shard_map/front_later/pallas_call | solution.py:242
  113.2 8.5 %all_to_all.28.everyone_ref = bf16[8,48,128]{2,1,0:T(8,128)(2,1)S(1)} all-to-all(bf16[8,48,128]{2,1,0:T(8,128)(2,1)S(1)} %get-tuple-element.39), channel_id=1, replica_groups={{0,1,2,3,4,5,6,7},{8,9,10,11,12,13,14,15},{16,17,18,19,20,21,22,23},{24..., dimensions={0} | all-to-all | bytes 196608 | tf_op jit(solution)/shard_map/all_to_all | solution.py:29
  121.7 1.2 read.3
  122.9 26.2 %all_to_all.29 = bf16[16,16,128]{2,1,0:T(8,128)(2,1)S(1)} all-to-all(bf16[16,16,128]{2,1,0:T(8,128)(2,1)S(1)} %read.3), channel_id=1, replica_groups={{0,4,8,12,16,20,24,28,32,36,40,44,48,52,56,60},{1,5,9,13,17,21,25,29,33..., dimensions={0} | all-to-all | bytes 131072 | tf_op jit(solution)/shard_map/all_to_all | solution.py:29
  149.2 0.2 collective-permute-start.7
  149.4 0.6 stack.17
  150.0 3.3 %collective-permute-start.6 = (bf16[256,128]{1,0:T(8,128)(2,1)S(1)}, bf16[256,128]{1,0:T(8,128)(2,1)S(1)}, u32[]{:S(2)}, u32[]{:S(2)}) collective-permute-start(bf16[256,128]{1,0:T(8,128)(2,1)S(1)} %bitcast.13), channel_id=1, source_target_pairs={{0,1},{1,0},{2,3},{3,2},{4,5},{5,4},{6,7},{7,6},{8,9},{9,8},{10,11... | collective-permute-start | bytes 196616 | tf_op jit(solution)/shard_map/ppermute | solution.py:34
  153.3 2.5 %update.3 = f32[2,64,32,256]{3,2,1,0:T(8,128)} custom-call(bf16[8,48,128]{2,1,0:T(8,128)(2,1)S(1)} %all_to_all.28.everyone_ref, f32[32,64]{1,0:T(8,128)S(1)} %get-tuple-element.40.value_ref, f32[8,128]{1,0:T(8,128)S(1)} %get-tuple-element.42.rows_ref, f32[64,32,256]{2,1,0:T(8,128)S(1)} %fetch.1.cell_ref.held_ref, ...), custom_call_target="tpu_custom_call", output_to_operand_aliasing={{}: (5, {})} | custom-call | tf_op jit(solution)/shard_map/update/pallas_call | solution.py:357
  155.8 0.0 collective-permute-done.7.second_ref
  155.8 1.1 collective-permute-start.8
  156.9 0.0 collective-permute-done.6.first_ref
  156.9 0.9 collective-permute-done.8.third_ref
  157.8 1.6 proj.3
Async XLA Ops:
  31.8 44.7 %copy-start.4 = (bf16[2,32,2048]{2,1,0:T(8,128)(2,1)S(1)}, bf16[2,32,2048]{2,1,0:T(8,128)(2,1)}, u32[]{:S(2)}) copy-start(bf16[2,32,2048]{2,1,0:T(8,128)(2,1)} %weight_ref.3) | copy-start | bytes 786436
  67.8 5.2 %collective-permute-start.1 = (bf16[256,128]{1,0:T(8,128)(2,1)S(1)}, bf16[256,128]{1,0:T(8,128)(2,1)S(1)}, u32[]{:S(2)}, u32[]{:S(2)}) collective-permute-start(bf16[256,128]{1,0:T(8,128)(2,1)S(1)} %bitcast.20), channel_id=1, source_target_pairs={{0,2},{1,3},{2,0},{3,1},{4,6},{5,7},{6,4},{7,5},{8,10},{9,11},{10,... | collective-permute-start | bytes 196616 | tf_op jit(solution)/shard_map/ppermute | solution.py:34
  68.0 7.6 %collective-permute-start = (bf16[256,128]{1,0:T(8,128)(2,1)S(1)}, bf16[256,128]{1,0:T(8,128)(2,1)S(1)}, u32[]{:S(2)}, u32[]{:S(2)}) collective-permute-start(bf16[256,128]{1,0:T(8,128)(2,1)S(1)} %bitcast.21), channel_id=1, source_target_pairs={{0,1},{1,0},{2,3},{3,2},{4,5},{5,4},{6,7},{7,6},{8,9},{9,8},{10,11... | collective-permute-start | bytes 196616 | tf_op jit(solution)/shard_map/ppermute | solution.py:34
  72.9 38.4 %copy-start = (bf16[2,32,2048]{2,1,0:T(8,128)(2,1)S(1)}, bf16[2,32,2048]{2,1,0:T(8,128)(2,1)}, u32[]{:S(2)}) copy-start(bf16[2,32,2048]{2,1,0:T(8,128)(2,1)} %wq_ref.1) | copy-start | bytes 786436
  73.0 38.4 %copy-start.1 = (bf16[2,32,2048]{2,1,0:T(8,128)(2,1)S(1)}, bf16[2,32,2048]{2,1,0:T(8,128)(2,1)}, u32[]{:S(2)}) copy-start(bf16[2,32,2048]{2,1,0:T(8,128)(2,1)} %wk_ref.1) | copy-start | bytes 786436
  73.0 38.4 %copy-start.2 = (bf16[2,32,2048]{2,1,0:T(8,128)(2,1)S(1)}, bf16[2,32,2048]{2,1,0:T(8,128)(2,1)}, u32[]{:S(2)}) copy-start(bf16[2,32,2048]{2,1,0:T(8,128)(2,1)} %wv_ref.1) | copy-start | bytes 786436
  73.0 38.4 %copy-start.3 = (bf16[2,32,2048]{2,1,0:T(8,128)(2,1)S(1)}, bf16[2,32,2048]{2,1,0:T(8,128)(2,1)}, u32[]{:S(2)}) copy-start(bf16[2,32,2048]{2,1,0:T(8,128)(2,1)} %wo_ref.1) | copy-start | bytes 786436
  73.0 38.3 %copy-start.5 = (bf16[2,2048,16]{1,2,0:T(8,128)(2,1)S(1)}, bf16[2,2048,16]{1,2,0:T(8,128)(2,1)}, u32[]{:S(2)}) copy-start(bf16[2,2048,16]{1,2,0:T(8,128)(2,1)} %param.18) | copy-start | bytes 393220
  73.0 38.3 %copy-start.6 = (f32[2,64,32]{1,2,0:T(8,128)S(1)}, f32[2,64,32]{1,2,0:T(8,128)}, u32[]{:S(2)}) copy-start(f32[2,64,32]{1,2,0:T(8,128)} %param.22) | copy-start | bytes 49156
  73.0 38.3 %copy-start.7 = (f32[2,2048]{1,0:T(2,128)S(1)}, f32[2,2048]{1,0:T(2,128)}, u32[]{:S(2)}) copy-start(f32[2,2048]{1,0:T(2,128)} %gain_ref.1) | copy-start | bytes 49156
  73.0 38.3 %copy-start.8 = (f32[2,64,8]{1,2,0:T(8,128)S(1)}, f32[2,64,8]{1,2,0:T(8,128)}, u32[]{:S(2)}) copy-start(f32[2,64,8]{1,2,0:T(8,128)} %param.23) | copy-start | bytes 12292
  73.0 38.3 %copy-start.9 = (f32[2,8]{1,0:T(2,128)S(1)}, f32[2,8]{1,0:T(2,128)}, u32[]{:S(2)}) copy-start(f32[2,8]{1,0:T(2,128)} %rest_0_.1) | copy-start | bytes 196
  73.1 3.5 %collective-permute-start.2 = (bf16[256,128]{1,0:T(8,128)(2,1)S(1)}, bf16[256,128]{1,0:T(8,128)(2,1)S(1)}, u32[]{:S(2)}, u32[]{:S(2)}) collective-permute-start(bf16[256,128]{1,0:T(8,128)(2,1)S(1)} %collective-permute-done.1.second_ref), channel_id=1, source_target_pairs={{0,1},{1,0},{2,3},{3,2},{4,5},{5,4},{6,7},{7,6},{8,9},{9,8},{10,11... | collective-permute-start | bytes 196616 | tf_op jit(solution)/shard_map/ppermute | solution.py:34
  103.0 5.7 %collective-permute-start.4 = (bf16[256,128]{1,0:T(8,128)(2,1)S(1)}, bf16[256,128]{1,0:T(8,128)(2,1)S(1)}, u32[]{:S(2)}, u32[]{:S(2)}) collective-permute-start(bf16[256,128]{1,0:T(8,128)(2,1)S(1)} %bitcast.16), channel_id=1, source_target_pairs={{0,2},{1,3},{2,0},{3,1},{4,6},{5,7},{6,4},{7,5},{8,10},{9,11},{10,... | collective-permute-start | bytes 196616 | tf_op jit(solution)/shard_map/ppermute | solution.py:34
  103.0 7.5 %collective-permute-start.3 = (bf16[256,128]{1,0:T(8,128)(2,1)S(1)}, bf16[256,128]{1,0:T(8,128)(2,1)S(1)}, u32[]{:S(2)}, u32[]{:S(2)}) collective-permute-start(bf16[256,128]{1,0:T(8,128)(2,1)S(1)} %bitcast.17), channel_id=1, source_target_pairs={{0,1},{1,0},{2,3},{3,2},{4,5},{5,4},{6,7},{7,6},{8,9},{9,8},{10,11... | collective-permute-start | bytes 196616 | tf_op jit(solution)/shard_map/ppermute | solution.py:34
  108.7 2.7 %collective-permute-start.5 = (bf16[256,128]{1,0:T(8,128)(2,1)S(1)}, bf16[256,128]{1,0:T(8,128)(2,1)S(1)}, u32[]{:S(2)}, u32[]{:S(2)}) collective-permute-start(bf16[256,128]{1,0:T(8,128)(2,1)S(1)} %collective-permute-done.4.second_ref), channel_id=1, source_target_pairs={{0,1},{1,0},{2,3},{3,2},{4,5},{5,4},{6,7},{7,6},{8,9},{9,8},{10,11... | collective-permute-start | bytes 196616 | tf_op jit(solution)/shard_map/ppermute | solution.py:34
  149.2 6.7 %collective-permute-start.7 = (bf16[256,128]{1,0:T(8,128)(2,1)S(1)}, bf16[256,128]{1,0:T(8,128)(2,1)S(1)}, u32[]{:S(2)}, u32[]{:S(2)}) collective-permute-start(bf16[256,128]{1,0:T(8,128)(2,1)S(1)} %bitcast.12), channel_id=1, source_target_pairs={{0,2},{1,3},{2,0},{3,1},{4,6},{5,7},{6,4},{7,5},{8,10},{9,11},{10,... | collective-permute-start | bytes 196616 | tf_op jit(solution)/shard_map/ppermute | solution.py:34
  150.0 7.0 %collective-permute-start.6 = (bf16[256,128]{1,0:T(8,128)(2,1)S(1)}, bf16[256,128]{1,0:T(8,128)(2,1)S(1)}, u32[]{:S(2)}, u32[]{:S(2)}) collective-permute-start(bf16[256,128]{1,0:T(8,128)(2,1)S(1)} %bitcast.13), channel_id=1, source_target_pairs={{0,1},{1,0},{2,3},{3,2},{4,5},{5,4},{6,7},{7,6},{8,9},{9,8},{10,11... | collective-permute-start | bytes 196616 | tf_op jit(solution)/shard_map/ppermute | solution.py:34
  155.8 2.0 %collective-permute-start.8 = (bf16[256,128]{1,0:T(8,128)(2,1)S(1)}, bf16[256,128]{1,0:T(8,128)(2,1)S(1)}, u32[]{:S(2)}, u32[]{:S(2)}) collective-permute-start(bf16[256,128]{1,0:T(8,128)(2,1)S(1)} %collective-permute-done.7.second_ref), channel_id=1, source_target_pairs={{0,1},{1,0},{2,3},{3,2},{4,5},{5,4},{6,7},{7,6},{8,9},{9,8},{10,11... | collective-permute-start | bytes 196616 | tf_op jit(solution)/shard_map/ppermute | solution.py:34

commit v4 on v3

--- a/solution.py
+++ b/solution.py
@@ -10,7 +10,7 @@
 EPSILON = 1e-06
 NEAR = 4
 CHUNKS = 4
-UNROLLED = 8
+UNROLLED = 32
 PIECES = 8
 F32 = jnp.float32
 BF16 = jnp.bfloat16
@@ -59,12 +59,12 @@
     return pl.BlockSpec(memory_space=pl.ANY)
 
 
-def smem():
-    return pl.BlockSpec(memory_space=pltpu.SMEM)
-
-
-def unpack(place_ref, pieces, stage_ref):
-    own = place_ref[1]
+def near_vmem():
+    return pl.BlockSpec(memory_space=pltpu.VMEM)
+
+
+def unpack(pieces, stage_ref):
+    own = lax.axis_index("tp") % NEAR
     far, per, batch = stage_ref.shape
     half = per // (2 * NEAR)
     for flip, piece in enumerate(pieces):
@@ -74,10 +74,10 @@
         stage_ref[:, pl.ds(start + half, half), :] = both[:, :, batch:]
 
 
-def front_rest(layer, place_ref, outs, bias_ref, stab_ref, norm_ref, message_ref, value_ref, open_ref, rows_ref, new_norm_ref, new_stab_ref, head_size):
+def front_rest(layer, outs, bias_ref, stab_ref, norm_ref, message_ref, value_ref, open_ref, rows_ref, new_norm_ref, new_stab_ref, head_size):
     columns, batch = norm_ref.shape
     heads = stab_ref.shape[0]
-    head = place_ref[0]
+    head = lax.axis_index("tp") // (head_size // columns)
     query = outs[:columns].astype(BF16)
     keys = (outs[columns : 2 * columns] * head_size ** (-0.5)).astype(BF16)
     value_ref[...] = outs[2 * columns : 3 * columns].astype(BF16).astype(F32)
@@ -127,7 +127,7 @@
 
 
 def first_front(
-    place_ref, cell_ref, tokens_hbm, gain_hbm, wq_hbm, wk_hbm, wv_hbm, wo_hbm, wg_hbm, bias_hbm, stab_hbm, norm_hbm, *rest, head_size
+    cell_ref, tokens_hbm, gain_hbm, wq_hbm, wk_hbm, wv_hbm, wo_hbm, wg_hbm, bias_hbm, stab_hbm, norm_hbm, *rest, head_size
 ):
     *outs, held_ref, own_ref, arrived, loaded, tokens_ref, gain_ref, weights_ref, bias_ref, stab_ref, norm_ref = rest
     columns = own_ref.shape[0]
@@ -148,8 +148,9 @@
     loads[0].wait()
     loads[1].wait()
     near = NEAR * columns
-    nearby = tokens_ref[:, pl.ds(pl.multiple_of(place_ref[2] * near, near), near)].astype(F32)
-    turned = pltpu.roll(nearby, (NEAR - place_ref[1]) % NEAR * columns, 1).T
+    device = lax.axis_index("tp")
+    nearby = tokens_ref[:, pl.ds(pl.multiple_of(device // NEAR * near, near), near)].astype(F32)
+    turned = pltpu.roll(nearby, (NEAR - device % NEAR) % NEAR * columns, 1).T
     own_ref[...] = turned[:columns].astype(BF16)
     current = tokens_ref[...].astype(F32)
     scale = lax.rsqrt(jnp.mean(current * current, axis=1, keepdims=True) + EPSILON)
@@ -157,14 +158,14 @@
     for load in loads[2:]:
         load.wait()
     dots = lax.dot_general(weights_ref[...], normed, (((1,), (1,)), ((), ())), preferred_element_type=F32)
-    front_rest(0, place_ref, dots, bias_ref, stab_ref, norm_ref, *outs, head_size=head_size)
+    front_rest(0, dots, bias_ref, stab_ref, norm_ref, *outs, head_size=head_size)
     for fetch in fetches:
         fetch.wait()
 
 
-def later_front(place_ref, own_ref, first_ref, second_ref, third_ref, gain_ref, wq_ref, wk_ref, wv_ref, wo_ref, wg_ref, *rest, layer, head_size):
+def later_front(own_ref, first_ref, second_ref, third_ref, gain_ref, wq_ref, wk_ref, wv_ref, wo_ref, wg_ref, *rest, layer, head_size):
     *rest, stage_ref, normed_ref = rest
-    unpack(place_ref, (own_ref, first_ref, second_ref, third_ref), stage_ref)
+    unpack((own_ref, first_ref, second_ref, third_ref), stage_ref)
     far, per, batch = stage_ref.shape
     current = stage_ref[...].astype(F32)
     square = jnp.sum(jnp.sum(current * current, axis=0), axis=0, keepdims=True)
@@ -172,9 +173,10 @@
     gain = jnp.concatenate([gain_ref[layer : layer + 1, i * per : (i + 1) * per] for i in range(far)]).T
     for i in range(far):
         normed_ref[i * per : (i + 1) * per, :] = (current[i] * scale * gain[:, i : i + 1]).astype(BF16)
-    weights = jnp.concatenate([wq_ref[...], wk_ref[...], wv_ref[...], wo_ref[...], wg_ref[...]])
+    weights = jnp.concatenate([wq_ref[layer], wk_ref[layer], wv_ref[layer], wo_ref[layer], wg_ref[layer]])
     outs = jnp.dot(weights, normed_ref[...], preferred_element_type=F32)
-    front_rest(layer, place_ref, outs, *rest, head_size=head_size)
+    bias_ref, stab_ref, norm_ref, *made = rest
+    front_rest(layer, outs, bias_ref, stab_ref.at[layer], norm_ref.at[layer], *made, head_size=head_size)
 
 
 def in_hbm(*values):
@@ -202,7 +204,7 @@
     )(*in_hbm(cell), after)
 
 
-def front(layer, place, current, norm_gain, projections, gates, bias, stab, norm, cell):
+def front(layer, current, norm_gain, projections, gates, bias, stab, norm, cell):
     _, columns, width = projections[0].shape
     heads, batch = stab.shape[1:]
     head_size = cell.shape[-1]
@@ -216,15 +218,13 @@
         jax.ShapeDtypeStruct((columns, batch), F32),
         jax.ShapeDtypeStruct((heads, batch), F32),
     ]
-    out_specs = [whole(out.shape) for out in out_shape]
     if layer == 0:
         operands = (cell, current, norm_gain, *projections, gates, bias, stab, norm)
         return pl.pallas_call(
             functools.partial(first_front, head_size=head_size),
-            grid=(1,),
             out_shape=out_shape + [jax.ShapeDtypeStruct(cell.shape[1:], F32), jax.ShapeDtypeStruct((columns, batch), BF16)],
-            out_specs=out_specs + [anywhere(), whole((columns, batch))],
-            in_specs=[smem()] + [anywhere()] * len(operands),
+            out_specs=[near_vmem()] * len(out_shape) + [anywhere(), near_vmem()],
+            in_specs=[anywhere()] * len(operands),
             scratch_shapes=[
                 pltpu.SemaphoreType.DMA((PIECES,)),
                 pltpu.SemaphoreType.DMA((10,)),
@@ -237,30 +237,21 @@
             ],
             compiler_params=LIMITED,
             name="front_first",
-        )(place, *in_hbm(*operands))
+        )(*in_hbm(*operands))
     per = width // far
+    operands = (*current, norm_gain, *projections, gates, bias, stab, norm)
     return pl.pallas_call(
         functools.partial(later_front, layer=layer, head_size=head_size),
-        grid=(1,),
         out_shape=out_shape,
-        out_specs=out_specs,
-        in_specs=[smem()]
-        + [whole(current[0].shape)] * 4
-        + [whole(norm_gain.shape)]
-        + [one_layer((columns, width), layer)] * 4
-        + [
-            one_layer((2 * heads, width), layer),
-            whole(bias.shape),
-            one_layer((heads, batch), layer),
-            one_layer((columns, batch), layer),
-        ],
+        out_specs=[near_vmem()] * len(out_shape),
+        in_specs=[near_vmem()] * len(operands),
         scratch_shapes=[
             pltpu.VMEM((far, per, batch), BF16),
             pltpu.VMEM((width, batch), BF16),
         ],
         compiler_params=LIMITED,
         name="front_later",
-    )(place, *current, norm_gain, *projections, gates, bias, stab, norm)
+    )(*operands)
 
 
 def head_rows(everyone_ref, columns):
@@ -305,10 +296,9 @@
     operands = (everyone, value, opened, rows, held)
     return pl.pallas_call(
         read_kernel,
-        grid=(1,),
         out_shape=out_shape,
-        in_specs=[whole(operand.shape) for operand in operands],
-        out_specs=whole(out_shape.shape),
+        in_specs=[near_vmem()] * len(operands),
+        out_specs=near_vmem(),
         scratch_shapes=[pltpu.VMEM((2 * batch, held.shape[-1]), F32)],
         compiler_params=LIMITED,
         name="read",
@@ -391,17 +381,17 @@
     )(*norms, *stabs)
 
 
-def proj_result(place_ref, pieces, weight_ref, residual_ref, stage_ref):
-    unpack(place_ref, pieces, stage_ref)
+def proj_result(layer, pieces, weight_ref, residual_ref, stage_ref):
+    unpack(pieces, stage_ref)
     far, per, batch = stage_ref.shape
-    summed = jnp.dot(weight_ref[...], stage_ref[...].reshape(far * per, batch), preferred_element_type=F32)
+    summed = jnp.dot(weight_ref[layer], stage_ref[...].reshape(far * per, batch), preferred_element_type=F32)
     return (residual_ref[...].astype(F32) + summed).astype(BF16)
 
 
-def proj_kernel(place_ref, own_ref, first_ref, second_ref, third_ref, weight_ref, residual_ref, result_ref, *rest):
+def proj_kernel(layer, own_ref, first_ref, second_ref, third_ref, weight_ref, residual_ref, result_ref, *rest):
     *copies, stage_ref = rest
     pieces = (own_ref, first_ref, second_ref, third_ref)
-    result = proj_result(place_ref, pieces, weight_ref, residual_ref, stage_ref)
+    result = proj_result(layer, pieces, weight_ref, residual_ref, stage_ref)
     result_ref[...] = result
     half = result.shape[0] // 2
     for copies_ref in copies:
@@ -409,21 +399,19 @@
         copies_ref[...] = jnp.broadcast_to(packed[None], copies_ref.shape)
 
 
-def proj(layer, place, pieces, weight, residual, send):
+def proj(layer, pieces, weight, residual, send):
     _, columns, width = weight.shape
     batch = residual.shape[1]
     far = lax.axis_size("tp") // NEAR
     out_shape = [jax.ShapeDtypeStruct((columns, batch), BF16)]
-    operands = [place, *pieces, weight, residual]
-    in_specs = [smem()] + [whole(pieces[0].shape)] * 4 + [one_layer((columns, width), layer), whole(residual.shape)]
+    operands = (*pieces, weight, residual)
     if send:
         out_shape.append(jax.ShapeDtypeStruct((far, columns // 2, 2 * batch), BF16))
     return pl.pallas_call(
-        proj_kernel,
-        grid=(1,),
+        functools.partial(proj_kernel, layer),
         out_shape=out_shape,
-        out_specs=[whole(out.shape) for out in out_shape],
-        in_specs=in_specs,
+        in_specs=[near_vmem()] * len(operands),
+        out_specs=[near_vmem()] * len(out_shape),
         scratch_shapes=[pltpu.VMEM((far, width // far, batch), BF16)],
         compiler_params=LIMITED,
         name="proj",
@@ -434,8 +422,6 @@
     layers, columns, _ = query_weight.shape
     head_size = cell_state.shape[-1]
     group = head_size // columns
-    device = lax.axis_index("tp")
-    place = jnp.stack([device // group, device % NEAR, device // NEAR]).astype(jnp.int32)
     gates = gate_weight.transpose(0, 2, 1)
     stab = stabilizer.transpose(0, 2, 1)
     norm = normalizer.transpose(0, 2, 1)
@@ -447,7 +433,7 @@
     for layer in range(layers):
         last = layer + 1 == layers
         message, value, opened, rows, new_norm, new_stab, *more = front(
-            layer, place, current, norm_gain, projections, gates, forget_bias, stab, norm, cell_state
+            layer, current, norm_gain, projections, gates, forget_bias, stab, norm, cell_state
         )
         norms.append(new_norm)
         stabs.append(new_stab)
@@ -458,10 +444,10 @@
         write = functools.partial(update, layer, layers, everyone, value, rows, held[layer], cells)
         if last:
             pieces, (cells, small) = gathered(copies, lambda own: (write(own), stacked(norms, stabs)))
-            (residual,) = proj(layer, place, pieces, proj_weight, residual, False)
+            (residual,) = proj(layer, pieces, proj_weight, residual, False)
         else:
             pieces, held[layer + 1] = gathered(copies, functools.partial(fetch, layer + 1, cell_state))
-            residual, copies = proj(layer, place, pieces, proj_weight, residual, True)
+            residual, copies = proj(layer, pieces, proj_weight, residual, True)
             current, cells = gathered(copies, write)
     return (residual.T, cells, small[0].transpose(0, 2, 1), small[1].transpose(0, 2, 1))
 

time: 160 us -> 157 us (0.981)
  Pallas kernels: 16.8 us -> 13.8 us
    pallas_call x5, Pallas kernels: 7.79 us -> 5.26 us  [the longest x1 2.3 us: front(): pl.pallas_call(functools.partial(first_front, head_size=head_size), out_s...]
where the time goes in v4:
time: 157 us; the launch traced here: 156 us
  blocking collectives  123 us (78%)
  starting transfers between devices  15.7 us (10%)
  Pallas kernels  13.8 us (9%)
  waiting for transfers between devices  2.71 us (2%)
    all_to_all x5, blocking collectives, exchanged(): lax.all_to_all(copies, 'tp', 0, 0, tiled=True, axis_index_groups=groups)  123 us
    ppermute x9, starting transfers between devices, from_partner(): return lax.ppermute(value, 'tp', pairs)  15.7 us
    pallas_call x2, Pallas kernels, update(): pl.pallas_call(update_kernel, grid=(CHUNKS,), out_shape=jax.ShapeDtypeStr...  5.01 us
  transfers between devices with their start and end apart: 9, of which 3 were waited for; matrix products, arithmetic and copies ran while one was open for 0% of the time, Pallas kernels for 5%

profile of v4, /device:TPU:37, one launch (start us, length us, event | category | flops | bytes accessed | tf_op | source)
XLA Modules:
  0.0 156.2 jit_solution(4724818212111533003)
XLA Ops:
  0.6 2.3 %front_first.1 = (bf16[8,48,128]{2,1,0:T(8,128)(2,1)S(1)}, f32[32,64]{1,0:T(8,128)S(1)}, f32[32,64]{1,0:T(8,128)S(1)}, f32[8,128]{1,0:T(8,128)S(1)}, f32[32,64]{...) custom-call(f32[2,64,32,256]{3,2,1,0:T(8,128)} %cell_ref.3, ...), custom_call_target="tpu_custom_call" | custom-call | tf_op jit(solution)/shard_map/front_first/pallas_call | solution.py:223
  2.9 28.3 %all_to_all.25.everyone_ref = bf16[8,48,128]{2,1,0:T(8,128)(2,1)S(1)} all-to-all(bf16[8,48,128]{2,1,0:T(8,128)(2,1)S(1)} %get-tuple-element.30), channel_id=1, replica_groups={{0,1,2,3,4,5,6,7},{8,9,10,11,12,13,14,15},{16,17,18,19,20,21,22,23},{24..., dimensions={0} | all-to-all | bytes 196608 | tf_op jit(solution)/shard_map/all_to_all | solution.py:29
  31.2 0.0 copy-start.4
  31.2 0.7 read.2
  31.9 34.8 %all_to_all.26 = bf16[16,16,128]{2,1,0:T(8,128)(2,1)S(1)} all-to-all(bf16[16,16,128]{2,1,0:T(8,128)(2,1)S(1)} %read.2), channel_id=1, replica_groups={{0,4,8,12,16,20,24,28,32,36,40,44,48,52,56,60},{1,5,9,13,17,21,25,29,33..., dimensions={0} | all-to-all | bytes 131072 | tf_op jit(solution)/shard_map/all_to_all | solution.py:29
  66.7 0.2 collective-permute-start.1
  66.9 3.3 %collective-permute-start = (bf16[256,128]{1,0:T(8,128)(2,1)S(1)}, bf16[256,128]{1,0:T(8,128)(2,1)S(1)}, u32[]{:S(2)}, u32[]{:S(2)}) collective-permute-start(bf16[256,128]{1,0:T(8,128)(2,1)S(1)} %bitcast.18), channel_id=1, source_target_pairs={{0,1},{1,0},{2,3},{3,2},{4,5},{5,4},{6,7},{7,6},{8,9},{9,8},{10,11... | collective-permute-start | bytes 196616 | tf_op jit(solution)/shard_map/ppermute | solution.py:34
  70.3 1.6 %fetch.1.cell_ref.held_ref = f32[64,32,256]{2,1,0:T(8,128)S(1)} custom-call(f32[2,64,32,256]{3,2,1,0:T(8,128)} %cell_ref.3, bf16[256,128]{1,0:T(8,128)(2,1)S(1)} %bitcast.19), custom_call_target="tpu_custom_call" | custom-call | tf_op jit(solution)/shard_map/fetch/pallas_call | solution.py:196
  71.8 0.0 copy-start
  71.9 0.0 copy-start.1
  71.9 0.0 copy-start.2
  71.9 0.0 copy-start.3
  71.9 0.0 copy-start.5
  71.9 0.0 copy-start.6
  71.9 0.0 copy-start.7
  71.9 0.0 copy-start.8
  71.9 0.0 copy-start.9
  72.0 0.0 collective-permute-done.1.second_ref
  72.0 2.6 %collective-permute-start.2 = (bf16[256,128]{1,0:T(8,128)(2,1)S(1)}, bf16[256,128]{1,0:T(8,128)(2,1)S(1)}, u32[]{:S(2)}, u32[]{:S(2)}) collective-permute-start(bf16[256,128]{1,0:T(8,128)(2,1)S(1)} %collective-permute-done.1.second_ref), channel_id=1, source_target_pairs={{0,1},{1,0},{2,3},{3,2},{4,5},{5,4},{6,7},{7,6},{8,9},{9,8},{10,11... | collective-permute-start | bytes 196616 | tf_op jit(solution)/shard_map/ppermute | solution.py:34
  74.5 0.0 collective-permute-done.first_ref
  74.5 0.9 collective-permute-done.2.third_ref
  75.4 0.0 copy-done.4
  75.4 0.5 proj.2
  75.9 25.4 %all_to_all.27 = bf16[16,16,128]{2,1,0:T(8,128)(2,1)S(1)} all-to-all(bf16[16,16,128]{2,1,0:T(8,128)(2,1)S(1)} %get-tuple-element.37), channel_id=1, replica_groups={{0,4,8,12,16,20,24,28,32,36,40,44,48,52,56,60},{1,5,9,13,17,21,25,29,33..., dimensions={0} | all-to-all | bytes 131072 | tf_op jit(solution)/shard_map/all_to_all | solution.py:29
  101.3 0.0 collective-permute-start.4
  101.3 3.2 %collective-permute-start.3 = (bf16[256,128]{1,0:T(8,128)(2,1)S(1)}, bf16[256,128]{1,0:T(8,128)(2,1)S(1)}, u32[]{:S(2)}, u32[]{:S(2)}) collective-permute-start(bf16[256,128]{1,0:T(8,128)(2,1)S(1)} %bitcast.14), channel_id=1, source_target_pairs={{0,1},{1,0},{2,3},{3,2},{4,5},{5,4},{6,7},{7,6},{8,9},{9,8},{10,11... | collective-permute-start | bytes 196616 | tf_op jit(solution)/shard_map/ppermute | solution.py:34
  104.5 2.5 %update.2.rest_1_ = f32[2,64,32,256]{3,2,1,0:T(8,128)} custom-call(bf16[8,48,128]{2,1,0:T(8,128)(2,1)S(1)} %all_to_all.25.everyone_ref, f32[32,64]{1,0:T(8,128)S(1)} %get-tuple-element.31.value_ref, f32[8,128]{1,0:T(8,128)S(1)} %get-tuple-element.33.rows_ref, f32[64,32,256]{2,1,0:T(8,128)S(1)} %get-tuple-element.34.cell_ref.held_ref, ...), custom_call_target="tpu_custom_call" | custom-call | tf_op jit(solution)/shard_map/update/pallas_call | solution.py:347
  107.0 0.0 collective-permute-done.4.second_ref
  107.0 1.8 %collective-permute-start.5 = (bf16[256,128]{1,0:T(8,128)(2,1)S(1)}, bf16[256,128]{1,0:T(8,128)(2,1)S(1)}, u32[]{:S(2)}, u32[]{:S(2)}) collective-permute-start(bf16[256,128]{1,0:T(8,128)(2,1)S(1)} %collective-permute-done.4.second_ref), channel_id=1, source_target_pairs={{0,1},{1,0},{2,3},{3,2},{4,5},{5,4},{6,7},{7,6},{8,9},{9,8},{10,11... | collective-permute-start | bytes 196616 | tf_op jit(solution)/shard_map/ppermute | solution.py:34
  108.8 0.0 collective-permute-done.3.first_ref
  108.8 0.9 collective-permute-done.5.third_ref
  109.7 0.0 copy-done
  109.7 0.0 copy-done.1
  109.7 0.0 copy-done.2
  109.7 0.0 copy-done.3
  109.7 0.0 copy-done.5
  109.7 0.0 copy-done.6
  109.7 0.0 copy-done.7
  109.7 0.0 copy-done.8
  109.7 0.0 copy-done.9
  109.8 1.3 front_later.1
  111.1 8.4 %all_to_all.28.everyone_ref = bf16[8,48,128]{2,1,0:T(8,128)(2,1)S(1)} all-to-all(bf16[8,48,128]{2,1,0:T(8,128)(2,1)S(1)} %get-tuple-element.39), channel_id=1, replica_groups={{0,1,2,3,4,5,6,7},{8,9,10,11,12,13,14,15},{16,17,18,19,20,21,22,23},{24..., dimensions={0} | all-to-all | bytes 196608 | tf_op jit(solution)/shard_map/all_to_all | solution.py:29
  119.5 0.7 read.3
  120.2 26.3 %all_to_all.29 = bf16[16,16,128]{2,1,0:T(8,128)(2,1)S(1)} all-to-all(bf16[16,16,128]{2,1,0:T(8,128)(2,1)S(1)} %read.3), channel_id=1, replica_groups={{0,4,8,12,16,20,24,28,32,36,40,44,48,52,56,60},{1,5,9,13,17,21,25,29,33..., dimensions={0} | all-to-all | bytes 131072 | tf_op jit(solution)/shard_map/all_to_all | solution.py:29
  146.5 0.2 collective-permute-start.7
  146.7 0.6 stack.1
  147.3 3.3 %collective-permute-start.6 = (bf16[256,128]{1,0:T(8,128)(2,1)S(1)}, bf16[256,128]{1,0:T(8,128)(2,1)S(1)}, u32[]{:S(2)}, u32[]{:S(2)}) collective-permute-start(bf16[256,128]{1,0:T(8,128)(2,1)S(1)} %bitcast.10), channel_id=1, source_target_pairs={{0,1},{1,0},{2,3},{3,2},{4,5},{5,4},{6,7},{7,6},{8,9},{9,8},{10,11... | collective-permute-start | bytes 196616 | tf_op jit(solution)/shard_map/ppermute | solution.py:34
  150.7 2.5 %update.3 = f32[2,64,32,256]{3,2,1,0:T(8,128)} custom-call(bf16[8,48,128]{2,1,0:T(8,128)(2,1)S(1)} %all_to_all.28.everyone_ref, f32[32,64]{1,0:T(8,128)S(1)} %get-tuple-element.40.value_ref, f32[8,128]{1,0:T(8,128)S(1)} %get-tuple-element.42.rows_ref, f32[64,32,256]{2,1,0:T(8,128)S(1)} %fetch.1.cell_ref.held_ref, ...), custom_call_target="tpu_custom_call", output_to_operand_aliasing={{}: (5, {})} | custom-call | tf_op jit(solution)/shard_map/update/pallas_call | solution.py:347
  153.2 0.0 collective-permute-done.7.second_ref
  153.2 1.1 collective-permute-start.8
  154.3 0.0 collective-permute-done.6.first_ref
  154.3 0.9 collective-permute-done.8.third_ref
  155.2 1.0 proj.3
Async XLA Ops:
  31.2 44.2 %copy-start.4 = (bf16[2,32,2048]{2,1,0:T(8,128)(2,1)S(1)}, bf16[2,32,2048]{2,1,0:T(8,128)(2,1)}, u32[]{:S(2)}) copy-start(bf16[2,32,2048]{2,1,0:T(8,128)(2,1)} %weight_ref.3) | copy-start | bytes 786436
  66.7 5.2 %collective-permute-start.1 = (bf16[256,128]{1,0:T(8,128)(2,1)S(1)}, bf16[256,128]{1,0:T(8,128)(2,1)S(1)}, u32[]{:S(2)}, u32[]{:S(2)}) collective-permute-start(bf16[256,128]{1,0:T(8,128)(2,1)S(1)} %bitcast.17), channel_id=1, source_target_pairs={{0,2},{1,3},{2,0},{3,1},{4,6},{5,7},{6,4},{7,5},{8,10},{9,11},{10,... | collective-permute-start | bytes 196616 | tf_op jit(solution)/shard_map/ppermute | solution.py:34
  66.9 7.6 %collective-permute-start = (bf16[256,128]{1,0:T(8,128)(2,1)S(1)}, bf16[256,128]{1,0:T(8,128)(2,1)S(1)}, u32[]{:S(2)}, u32[]{:S(2)}) collective-permute-start(bf16[256,128]{1,0:T(8,128)(2,1)S(1)} %bitcast.18), channel_id=1, source_target_pairs={{0,1},{1,0},{2,3},{3,2},{4,5},{5,4},{6,7},{7,6},{8,9},{9,8},{10,11... | collective-permute-start | bytes 196616 | tf_op jit(solution)/shard_map/ppermute | solution.py:34
  71.8 37.8 %copy-start = (bf16[2,32,2048]{2,1,0:T(8,128)(2,1)S(1)}, bf16[2,32,2048]{2,1,0:T(8,128)(2,1)}, u32[]{:S(2)}) copy-start(bf16[2,32,2048]{2,1,0:T(8,128)(2,1)} %wq_ref.1) | copy-start | bytes 786436
  71.9 37.8 %copy-start.1 = (bf16[2,32,2048]{2,1,0:T(8,128)(2,1)S(1)}, bf16[2,32,2048]{2,1,0:T(8,128)(2,1)}, u32[]{:S(2)}) copy-start(bf16[2,32,2048]{2,1,0:T(8,128)(2,1)} %wk_ref.1) | copy-start | bytes 786436
  71.9 37.8 %copy-start.2 = (bf16[2,32,2048]{2,1,0:T(8,128)(2,1)S(1)}, bf16[2,32,2048]{2,1,0:T(8,128)(2,1)}, u32[]{:S(2)}) copy-start(bf16[2,32,2048]{2,1,0:T(8,128)(2,1)} %wv_ref.1) | copy-start | bytes 786436
  71.9 37.8 %copy-start.3 = (bf16[2,32,2048]{2,1,0:T(8,128)(2,1)S(1)}, bf16[2,32,2048]{2,1,0:T(8,128)(2,1)}, u32[]{:S(2)}) copy-start(bf16[2,32,2048]{2,1,0:T(8,128)(2,1)} %wo_ref.1) | copy-start | bytes 786436
  71.9 37.8 %copy-start.5 = (bf16[2,2048,16]{1,2,0:T(8,128)(2,1)S(1)}, bf16[2,2048,16]{1,2,0:T(8,128)(2,1)}, u32[]{:S(2)}) copy-start(bf16[2,2048,16]{1,2,0:T(8,128)(2,1)} %param.18) | copy-start | bytes 393220
  71.9 37.8 %copy-start.6 = (f32[2,64,32]{1,2,0:T(8,128)S(1)}, f32[2,64,32]{1,2,0:T(8,128)}, u32[]{:S(2)}) copy-start(f32[2,64,32]{1,2,0:T(8,128)} %param.22) | copy-start | bytes 49156
  71.9 37.8 %copy-start.7 = (f32[2,2048]{1,0:T(2,128)S(1)}, f32[2,2048]{1,0:T(2,128)}, u32[]{:S(2)}) copy-start(f32[2,2048]{1,0:T(2,128)} %gain_ref.1) | copy-start | bytes 49156
  71.9 37.8 %copy-start.8 = (f32[2,64,8]{1,2,0:T(8,128)S(1)}, f32[2,64,8]{1,2,0:T(8,128)}, u32[]{:S(2)}) copy-start(f32[2,64,8]{1,2,0:T(8,128)} %param.23) | copy-start | bytes 12292
  71.9 37.8 %copy-start.9 = (f32[2,8]{1,0:T(2,128)S(1)}, f32[2,8]{1,0:T(2,128)}, u32[]{:S(2)}) copy-start(f32[2,8]{1,0:T(2,128)} %rest_0_.1) | copy-start | bytes 196
  72.0 3.5 %collective-permute-start.2 = (bf16[256,128]{1,0:T(8,128)(2,1)S(1)}, bf16[256,128]{1,0:T(8,128)(2,1)S(1)}, u32[]{:S(2)}, u32[]{:S(2)}) collective-permute-start(bf16[256,128]{1,0:T(8,128)(2,1)S(1)} %collective-permute-done.1.second_ref), channel_id=1, source_target_pairs={{0,1},{1,0},{2,3},{3,2},{4,5},{5,4},{6,7},{7,6},{8,9},{9,8},{10,11... | collective-permute-start | bytes 196616 | tf_op jit(solution)/shard_map/ppermute | solution.py:34
  101.3 5.7 %collective-permute-start.4 = (bf16[256,128]{1,0:T(8,128)(2,1)S(1)}, bf16[256,128]{1,0:T(8,128)(2,1)S(1)}, u32[]{:S(2)}, u32[]{:S(2)}) collective-permute-start(bf16[256,128]{1,0:T(8,128)(2,1)S(1)} %bitcast.13), channel_id=1, source_target_pairs={{0,2},{1,3},{2,0},{3,1},{4,6},{5,7},{6,4},{7,5},{8,10},{9,11},{10,... | collective-permute-start | bytes 196616 | tf_op jit(solution)/shard_map/ppermute | solution.py:34
  101.3 7.5 %collective-permute-start.3 = (bf16[256,128]{1,0:T(8,128)(2,1)S(1)}, bf16[256,128]{1,0:T(8,128)(2,1)S(1)}, u32[]{:S(2)}, u32[]{:S(2)}) collective-permute-start(bf16[256,128]{1,0:T(8,128)(2,1)S(1)} %bitcast.14), channel_id=1, source_target_pairs={{0,1},{1,0},{2,3},{3,2},{4,5},{5,4},{6,7},{7,6},{8,9},{9,8},{10,11... | collective-permute-start | bytes 196616 | tf_op jit(solution)/shard_map/ppermute | solution.py:34
  107.0 2.7 %collective-permute-start.5 = (bf16[256,128]{1,0:T(8,128)(2,1)S(1)}, bf16[256,128]{1,0:T(8,128)(2,1)S(1)}, u32[]{:S(2)}, u32[]{:S(2)}) collective-permute-start(bf16[256,128]{1,0:T(8,128)(2,1)S(1)} %collective-permute-done.4.second_ref), channel_id=1, source_target_pairs={{0,1},{1,0},{2,3},{3,2},{4,5},{5,4},{6,7},{7,6},{8,9},{9,8},{10,11... | collective-permute-start | bytes 196616 | tf_op jit(solution)/shard_map/ppermute | solution.py:34
  146.5 6.7 %collective-permute-start.7 = (bf16[256,128]{1,0:T(8,128)(2,1)S(1)}, bf16[256,128]{1,0:T(8,128)(2,1)S(1)}, u32[]{:S(2)}, u32[]{:S(2)}) collective-permute-start(bf16[256,128]{1,0:T(8,128)(2,1)S(1)} %bitcast.9), channel_id=1, source_target_pairs={{0,2},{1,3},{2,0},{3,1},{4,6},{5,7},{6,4},{7,5},{8,10},{9,11},{10,... | collective-permute-start | bytes 196616 | tf_op jit(solution)/shard_map/ppermute | solution.py:34
  147.3 7.0 %collective-permute-start.6 = (bf16[256,128]{1,0:T(8,128)(2,1)S(1)}, bf16[256,128]{1,0:T(8,128)(2,1)S(1)}, u32[]{:S(2)}, u32[]{:S(2)}) collective-permute-start(bf16[256,128]{1,0:T(8,128)(2,1)S(1)} %bitcast.10), channel_id=1, source_target_pairs={{0,1},{1,0},{2,3},{3,2},{4,5},{5,4},{6,7},{7,6},{8,9},{9,8},{10,11... | collective-permute-start | bytes 196616 | tf_op jit(solution)/shard_map/ppermute | solution.py:34
  153.2 2.0 %collective-permute-start.8 = (bf16[256,128]{1,0:T(8,128)(2,1)S(1)}, bf16[256,128]{1,0:T(8,128)(2,1)S(1)}, u32[]{:S(2)}, u32[]{:S(2)}) collective-permute-start(bf16[256,128]{1,0:T(8,128)(2,1)S(1)} %collective-permute-done.7.second_ref), channel_id=1, source_target_pairs={{0,1},{1,0},{2,3},{3,2},{4,5},{5,4},{6,7},{7,6},{8,9},{9,8},{10,11... | collective-permute-start | bytes 196616 | tf_op jit(solution)/shard_map/ppermute | solution.py:34

commit v5 on v4

--- a/solution.py
+++ b/solution.py
@@ -11,7 +11,7 @@
 NEAR = 4
 CHUNKS = 4
 UNROLLED = 32
-PIECES = 8
+PIECES = 4
 F32 = jnp.float32
 BF16 = jnp.bfloat16
 LIMITED = pltpu.CompilerParams(vmem_limit_bytes=16 * 2**20)
@@ -305,80 +305,69 @@
     )(*operands)
 
 
-def update_kernel(everyone_ref, value_ref, rows_ref, held_ref, *rest):
-    *small, cell_ref, turned_ref, decay_ref, added_ref = rest
-    step = pl.program_id(0)
-    chunk, columns, keys = cell_ref.shape
-    batch = added_ref.shape[1] // 2
-
-    @pl.when(step == 0)
-    def _():
-        turned_ref[...] = head_rows(everyone_ref, columns).T
-        decay_ref[...] = jnp.broadcast_to(rows_ref[0:1, :], (2 * batch, 2 * batch)).T
-        scaled = value_ref[...] * rows_ref[0:1, batch:]
-        added_ref[...] = jnp.concatenate([scaled, scaled], axis=1)
-
-    added = pltpu.roll(added_ref[...], batch - step * chunk, 1)
-    for i in range(chunk):
-        b = step * chunk + i
-        key = turned_ref[pl.ds(batch + b, 1), :]
-        decay = decay_ref[pl.ds(b, 1), :]
-        decay = jnp.concatenate([decay] * (keys // decay.shape[1]), axis=1)
-        cell_ref[i] = decay * held_ref[i] + added[:, i : i + 1] * key
-
-
-def update(layer, layers, everyone, value, rows, held, into, after):
+def update_kernel(layer, layers, everyone_ref, value_ref, rows_ref, held_ref, *rest):
+    *rest, fresh_ref, turned_ref, decay_ref, written = rest
+    columns, batch = value_ref.shape
+    keys = held_ref.shape[-1]
+    if layers:
+        norm_refs, stab_refs = rest[:layers], rest[layers : 2 * layers]
+        *_, cells_ref, norms_ref, stabs_ref = rest
+        for k in range(layers):
+            norms_ref[k] = norm_refs[k][...]
+            stabs_ref[k] = stab_refs[k][...]
+    else:
+        cells_ref = rest[-1]
+    turned_ref[...] = head_rows(everyone_ref, columns).T
+    decay_ref[...] = jnp.broadcast_to(rows_ref[0:1, :], (2 * batch, 2 * batch)).T
+    added = value_ref[...] * rows_ref[0:1, batch:]
+    chunk = batch // CHUNKS
+    writes = []
+    for k in range(CHUNKS):
+        for b in range(k * chunk, (k + 1) * chunk):
+            key = turned_ref[batch + b : batch + b + 1, :]
+            decay = decay_ref[b : b + 1, :]
+            decay = jnp.concatenate([decay] * (keys // decay.shape[1]), axis=1)
+            fresh_ref[b] = decay * held_ref[b] + added[:, b : b + 1] * key
+        part = pl.ds(k * chunk, chunk)
+        writes.append(pltpu.make_async_copy(fresh_ref.at[part], cells_ref.at[layer, part], written.at[k]))
+        writes[-1].start()
+    for write in writes:
+        write.wait()
+
+
+def update(layer, layers, everyone, value, rows, held, into, small, after):
     columns, batch = value.shape
     keys = held.shape[-1]
-    chunk = batch // CHUNKS
-    operands = [everyone, value, rows, held, after]
-    in_specs = [
-        whole(everyone.shape),
-        whole(value.shape),
-        whole(rows.shape),
-        pl.BlockSpec((chunk, columns, keys), lambda i: (i, 0, 0)),
-        anywhere(),
-    ]
+    operands = [everyone, value, rows, held, *small]
+    in_specs = [near_vmem()] * len(operands)
+    out_shape = [jax.ShapeDtypeStruct((layers, *held.shape), F32)]
+    out_specs = [anywhere()]
+    if small:
+        for each in (small[0], small[-1]):
+            out_shape.append(jax.ShapeDtypeStruct((layers, *each.shape), F32))
+            out_specs.append(near_vmem())
+    operands.append(after)
+    in_specs.append(anywhere())
     aliases = {}
     if into is not None:
+        aliases = {len(operands): 0}
         operands.extend(in_hbm(into))
         in_specs.append(anywhere())
-        aliases = {5: 0}
     return pl.pallas_call(
-        update_kernel,
-        grid=(CHUNKS,),
-        out_shape=jax.ShapeDtypeStruct((layers, *held.shape), F32),
+        functools.partial(update_kernel, layer, len(small) // 2),
+        out_shape=out_shape,
         in_specs=in_specs,
-        out_specs=pl.BlockSpec((None, chunk, columns, keys), lambda i: (layer, i, 0, 0)),
+        out_specs=out_specs,
         scratch_shapes=[
+            pltpu.VMEM(held.shape, F32),
             pltpu.VMEM((2 * batch, keys), F32),
             pltpu.VMEM((2 * batch, 2 * batch), F32),
-            pltpu.VMEM((columns, 2 * batch), F32),
+            pltpu.SemaphoreType.DMA((CHUNKS,)),
         ],
         input_output_aliases=aliases,
         compiler_params=LIMITED,
         name="update",
     )(*operands)
-
-
-def stack_kernel(layers, *refs):
-    for layer in range(layers):
-        refs[-2][layer] = refs[layer][...]
-        refs[-1][layer] = refs[layers + layer][...]
-
-
-def stacked(norms, stabs):
-    layers = len(norms)
-    out_shape = [jax.ShapeDtypeStruct((layers, *each[0].shape), F32) for each in (norms, stabs)]
-    return pl.pallas_call(
-        functools.partial(stack_kernel, layers),
-        grid=(1,),
-        out_shape=out_shape,
-        in_specs=[whole(each.shape) for each in (*norms, *stabs)],
-        out_specs=[whole(out.shape) for out in out_shape],
-        compiler_params=LIMITED,
-        name="stack",
-    )(*norms, *stabs)
 
 
 def proj_result(layer, pieces, weight_ref, residual_ref, stage_ref):
@@ -441,15 +430,17 @@
             held[0], residual = more
         everyone = exchanged(message, near_groups(lax.axis_size("tp"), group))
         copies = read(everyone, value, opened, rows, held[layer])
-        write = functools.partial(update, layer, layers, everyone, value, rows, held[layer], cells)
+        small = (*norms, *stabs) if last else ()
+        write = functools.partial(update, layer, layers, everyone, value, rows, held[layer], cells, small)
         if last:
-            pieces, (cells, small) = gathered(copies, lambda own: (write(own), stacked(norms, stabs)))
+            pieces, states = gathered(copies, write)
             (residual,) = proj(layer, pieces, proj_weight, residual, False)
         else:
             pieces, held[layer + 1] = gathered(copies, functools.partial(fetch, layer + 1, cell_state))
             residual, copies = proj(layer, pieces, proj_weight, residual, True)
-            current, cells = gathered(copies, write)
-    return (residual.T, cells, small[0].transpose(0, 2, 1), small[1].transpose(0, 2, 1))
+            current, (cells,) = gathered(copies, write)
+    cells, norms, stabs = states
+    return (residual.T, cells, norms.transpose(0, 2, 1), stabs.transpose(0, 2, 1))
 
 
 def solution(mesh):

time: 157 us -> 156 us (level)
  Pallas kernels: 13.8 us -> 11.9 us
  starting transfers between devices: 15.7 us -> 17.4 us
    pallas_call x3 -> x2, Pallas kernels: 5.63 us -> 3.9 us  [update(): pl.pallas_call(functools.partial(update_kernel, layer, len(small) // 2),...]
    ppermute x9, starting transfers between devices: 15.7 us -> 17.4 us  [from_partner(): return lax.ppermute(value, 'tp', pairs)]
  transfers between devices with their start and end apart: 9 -> 9, of which waited for: 3 -> 3; matrix products, arithmetic and copies ran while one was open for 0% -> 0% of each run, Pallas kernels for 5% -> 3%
where the time goes in v5:
time: 156 us
  blocking collectives  123 us (79%)
  starting transfers between devices  17.4 us (11%)
  Pallas kernels  11.9 us (8%)
  waiting for transfers between devices  2.71 us (2%)
    all_to_all x5, blocking collectives, exchanged(): lax.all_to_all(copies, 'tp', 0, 0, tiled=True, axis_index_groups=groups)  123 us
    ppermute x9, starting transfers between devices, from_partner(): return lax.ppermute(value, 'tp', pairs)  17.4 us
    pallas_call x2, Pallas kernels, update(): pl.pallas_call(functools.partial(update_kernel, layer, len(small) // 2),...  3.9 us
  transfers between devices with their start and end apart: 9, of which 3 were waited for; matrix products, arithmetic and copies ran while one was open for 0% of the time, Pallas kernels for 3%

profile of v5, /device:TPU:37, one launch (start us, length us, event | category | flops | bytes accessed | tf_op | source)
XLA Modules:
  0.0 156.1 jit_solution(11532357058607018307)
XLA Ops:
  0.6 2.2 %front_first.1 = (bf16[8,48,128]{2,1,0:T(8,128)(2,1)S(1)}, f32[32,64]{1,0:T(8,128)S(1)}, f32[32,64]{1,0:T(8,128)S(1)}, f32[8,128]{1,0:T(8,128)S(1)}, f32[32,64]{...) custom-call(f32[2,64,32,256]{3,2,1,0:T(8,128)} %cell_ref.3, ...), custom_call_target="tpu_custom_call" | custom-call | tf_op jit(solution)/shard_map/front_first/pallas_call | solution.py:223
  2.9 28.3 %all_to_all.25.everyone_ref = bf16[8,48,128]{2,1,0:T(8,128)(2,1)S(1)} all-to-all(bf16[8,48,128]{2,1,0:T(8,128)(2,1)S(1)} %get-tuple-element.31), channel_id=1, replica_groups={{0,1,2,3,4,5,6,7},{8,9,10,11,12,13,14,15},{16,17,18,19,20,21,22,23},{24..., dimensions={0} | all-to-all | bytes 196608 | tf_op jit(solution)/shard_map/all_to_all | solution.py:29
  31.1 0.0 copy-start.4
  31.1 0.7 read.2
  31.9 34.8 %all_to_all.26 = bf16[16,16,128]{2,1,0:T(8,128)(2,1)S(1)} all-to-all(bf16[16,16,128]{2,1,0:T(8,128)(2,1)S(1)} %read.2), channel_id=1, replica_groups={{0,4,8,12,16,20,24,28,32,36,40,44,48,52,56,60},{1,5,9,13,17,21,25,29,33..., dimensions={0} | all-to-all | bytes 131072 | tf_op jit(solution)/shard_map/all_to_all | solution.py:29
  66.7 0.2 collective-permute-start.1
  66.9 3.3 %collective-permute-start = (bf16[256,128]{1,0:T(8,128)(2,1)S(1)}, bf16[256,128]{1,0:T(8,128)(2,1)S(1)}, u32[]{:S(2)}, u32[]{:S(2)}) collective-permute-start(bf16[256,128]{1,0:T(8,128)(2,1)S(1)} %bitcast.18), channel_id=1, source_target_pairs={{0,1},{1,0},{2,3},{3,2},{4,5},{5,4},{6,7},{7,6},{8,9},{9,8},{10,11... | collective-permute-start | bytes 196616 | tf_op jit(solution)/shard_map/ppermute | solution.py:34
  70.2 1.5 fetch.1.cell_ref.held_ref
  71.8 0.0 copy-start
  71.8 0.0 copy-start.1
  71.8 0.0 copy-start.2
  71.8 0.0 copy-start.3
  71.8 0.0 copy-start.5
  71.8 0.0 copy-start.6
  71.8 0.0 copy-start.7
  71.8 0.0 copy-start.8
  71.9 0.0 copy-start.9
  71.9 0.0 collective-permute-done.1.second_ref
  71.9 2.6 %collective-permute-start.2 = (bf16[256,128]{1,0:T(8,128)(2,1)S(1)}, bf16[256,128]{1,0:T(8,128)(2,1)S(1)}, u32[]{:S(2)}, u32[]{:S(2)}) collective-permute-start(bf16[256,128]{1,0:T(8,128)(2,1)S(1)} %collective-permute-done.1.second_ref), channel_id=1, source_target_pairs={{0,1},{1,0},{2,3},{3,2},{4,5},{5,4},{6,7},{7,6},{8,9},{9,8},{10,11... | collective-permute-start | bytes 196616 | tf_op jit(solution)/shard_map/ppermute | solution.py:34
  74.5 0.0 collective-permute-done.first_ref
  74.5 0.9 collective-permute-done.2.third_ref
  75.4 0.0 copy-done.4
  75.4 0.5 proj.2
  75.9 25.4 %all_to_all.27 = bf16[16,16,128]{2,1,0:T(8,128)(2,1)S(1)} all-to-all(bf16[16,16,128]{2,1,0:T(8,128)(2,1)S(1)} %get-tuple-element.38), channel_id=1, replica_groups={{0,4,8,12,16,20,24,28,32,36,40,44,48,52,56,60},{1,5,9,13,17,21,25,29,33..., dimensions={0} | all-to-all | bytes 131072 | tf_op jit(solution)/shard_map/all_to_all | solution.py:29
  101.3 0.0 collective-permute-start.4
  101.3 3.2 %collective-permute-start.3 = (bf16[256,128]{1,0:T(8,128)(2,1)S(1)}, bf16[256,128]{1,0:T(8,128)(2,1)S(1)}, u32[]{:S(2)}, u32[]{:S(2)}) collective-permute-start(bf16[256,128]{1,0:T(8,128)(2,1)S(1)} %bitcast.14), channel_id=1, source_target_pairs={{0,1},{1,0},{2,3},{3,2},{4,5},{5,4},{6,7},{7,6},{8,9},{9,8},{10,11... | collective-permute-start | bytes 196616 | tf_op jit(solution)/shard_map/ppermute | solution.py:34
  104.5 1.6 %update.2.rest_5_ = f32[2,64,32,256]{3,2,1,0:T(8,128)} custom-call(bf16[8,48,128]{2,1,0:T(8,128)(2,1)S(1)} %all_to_all.25.everyone_ref, f32[32,64]{1,0:T(8,128)S(1)} %get-tuple-element.32.value_ref, f32[8,128]{1,0:T(8,128)S(1)} %get-tuple-element.34.rows_ref, f32[64,32,256]{2,1,0:T(8,128)S(1)} %get-tuple-element.35.cell_ref.held_ref, ...), custom_call_target="tpu_custom_call" | custom-call | tf_op jit(solution)/shard_map/update/pallas_call | solution.py:356
  106.1 0.0 collective-permute-done.4.second_ref
  106.1 2.6 %collective-permute-start.5 = (bf16[256,128]{1,0:T(8,128)(2,1)S(1)}, bf16[256,128]{1,0:T(8,128)(2,1)S(1)}, u32[]{:S(2)}, u32[]{:S(2)}) collective-permute-start(bf16[256,128]{1,0:T(8,128)(2,1)S(1)} %collective-permute-done.4.second_ref), channel_id=1, source_target_pairs={{0,1},{1,0},{2,3},{3,2},{4,5},{5,4},{6,7},{7,6},{8,9},{9,8},{10,11... | collective-permute-start | bytes 196616 | tf_op jit(solution)/shard_map/ppermute | solution.py:34
  108.7 0.0 collective-permute-done.3.first_ref
  108.7 0.9 collective-permute-done.5.third_ref
  109.6 0.0 copy-done
  109.6 0.0 copy-done.1
  109.6 0.0 copy-done.2
  109.6 0.0 copy-done.3
  109.6 0.0 copy-done.5
  109.6 0.0 copy-done.6
  109.7 0.0 copy-done.7
  109.7 0.0 copy-done.8
  109.7 0.0 copy-done.9
  109.7 1.3 front_later.1
  111.0 8.4 %all_to_all.28.everyone_ref = bf16[8,48,128]{2,1,0:T(8,128)(2,1)S(1)} all-to-all(bf16[8,48,128]{2,1,0:T(8,128)(2,1)S(1)} %get-tuple-element.40), channel_id=1, replica_groups={{0,1,2,3,4,5,6,7},{8,9,10,11,12,13,14,15},{16,17,18,19,20,21,22,23},{24..., dimensions={0} | all-to-all | bytes 196608 | tf_op jit(solution)/shard_map/all_to_all | solution.py:29
  119.4 0.7 read.3
  120.2 26.3 %all_to_all.29 = bf16[16,16,128]{2,1,0:T(8,128)(2,1)S(1)} all-to-all(bf16[16,16,128]{2,1,0:T(8,128)(2,1)S(1)} %read.3), channel_id=1, replica_groups={{0,4,8,12,16,20,24,28,32,36,40,44,48,52,56,60},{1,5,9,13,17,21,25,29,33..., dimensions={0} | all-to-all | bytes 131072 | tf_op jit(solution)/shard_map/all_to_all | solution.py:29
  146.4 0.2 collective-permute-start.7
  146.6 3.3 %collective-permute-start.6 = (bf16[256,128]{1,0:T(8,128)(2,1)S(1)}, bf16[256,128]{1,0:T(8,128)(2,1)S(1)}, u32[]{:S(2)}, u32[]{:S(2)}) collective-permute-start(bf16[256,128]{1,0:T(8,128)(2,1)S(1)} %bitcast.10), channel_id=1, source_target_pairs={{0,1},{1,0},{2,3},{3,2},{4,5},{5,4},{6,7},{7,6},{8,9},{9,8},{10,11... | collective-permute-start | bytes 196616 | tf_op jit(solution)/shard_map/ppermute | solution.py:34
  150.0 2.3 %update.3 = (f32[2,64,32,256]{3,2,1,0:T(8,128)}, f32[2,32,64]{2,1,0:T(8,128)}, f32[2,8,64]{2,1,0:T(8,128)}) custom-call(bf16[8,48,128]{2,1,0:T(8,128)(2,1)S(1)} %all_to_all.28.everyone_ref, f32[32,64]{1,0:T(8,128)S(1)} %get-tuple-element.41.value_ref, f32[8,128]{1,0:T(8,128)S(1)} %get-tuple-element.43.rows_ref, ...), custom_call_target="tpu_custom_call", output_to_operand_aliasing={{0}: (9, {})} | custom-call | tf_op jit(solution)/shard_map/update/pallas_call | solution.py:356
  152.2 0.0 collective-permute-done.7.second_ref
  152.2 2.0 %collective-permute-start.8 = (bf16[256,128]{1,0:T(8,128)(2,1)S(1)}, bf16[256,128]{1,0:T(8,128)(2,1)S(1)}, u32[]{:S(2)}, u32[]{:S(2)}) collective-permute-start(bf16[256,128]{1,0:T(8,128)(2,1)S(1)} %collective-permute-done.7.second_ref), channel_id=1, source_target_pairs={{0,1},{1,0},{2,3},{3,2},{4,5},{5,4},{6,7},{7,6},{8,9},{9,8},{10,11... | collective-permute-start | bytes 196616 | tf_op jit(solution)/shard_map/ppermute | solution.py:34
  154.2 0.0 collective-permute-done.6.first_ref
  154.2 0.9 collective-permute-done.8.third_ref
  155.1 1.0 proj.3
Async XLA Ops:
  31.1 44.2 %copy-start.4 = (bf16[2,32,2048]{2,1,0:T(8,128)(2,1)S(1)}, bf16[2,32,2048]{2,1,0:T(8,128)(2,1)}, u32[]{:S(2)}) copy-start(bf16[2,32,2048]{2,1,0:T(8,128)(2,1)} %weight_ref.3) | copy-start | bytes 786436
  66.7 5.2 %collective-permute-start.1 = (bf16[256,128]{1,0:T(8,128)(2,1)S(1)}, bf16[256,128]{1,0:T(8,128)(2,1)S(1)}, u32[]{:S(2)}, u32[]{:S(2)}) collective-permute-start(bf16[256,128]{1,0:T(8,128)(2,1)S(1)} %bitcast.17), channel_id=1, source_target_pairs={{0,2},{1,3},{2,0},{3,1},{4,6},{5,7},{6,4},{7,5},{8,10},{9,11},{10,... | collective-permute-start | bytes 196616 | tf_op jit(solution)/shard_map/ppermute | solution.py:34
  66.9 7.6 %collective-permute-start = (bf16[256,128]{1,0:T(8,128)(2,1)S(1)}, bf16[256,128]{1,0:T(8,128)(2,1)S(1)}, u32[]{:S(2)}, u32[]{:S(2)}) collective-permute-start(bf16[256,128]{1,0:T(8,128)(2,1)S(1)} %bitcast.18), channel_id=1, source_target_pairs={{0,1},{1,0},{2,3},{3,2},{4,5},{5,4},{6,7},{7,6},{8,9},{9,8},{10,11... | collective-permute-start | bytes 196616 | tf_op jit(solution)/shard_map/ppermute | solution.py:34
  71.8 37.9 %copy-start = (bf16[2,32,2048]{2,1,0:T(8,128)(2,1)S(1)}, bf16[2,32,2048]{2,1,0:T(8,128)(2,1)}, u32[]{:S(2)}) copy-start(bf16[2,32,2048]{2,1,0:T(8,128)(2,1)} %wq_ref.1) | copy-start | bytes 786436
  71.8 37.9 %copy-start.1 = (bf16[2,32,2048]{2,1,0:T(8,128)(2,1)S(1)}, bf16[2,32,2048]{2,1,0:T(8,128)(2,1)}, u32[]{:S(2)}) copy-start(bf16[2,32,2048]{2,1,0:T(8,128)(2,1)} %wk_ref.1) | copy-start | bytes 786436
  71.8 37.9 %copy-start.2 = (bf16[2,32,2048]{2,1,0:T(8,128)(2,1)S(1)}, bf16[2,32,2048]{2,1,0:T(8,128)(2,1)}, u32[]{:S(2)}) copy-start(bf16[2,32,2048]{2,1,0:T(8,128)(2,1)} %wv_ref.1) | copy-start | bytes 786436
  71.8 37.8 %copy-start.3 = (bf16[2,32,2048]{2,1,0:T(8,128)(2,1)S(1)}, bf16[2,32,2048]{2,1,0:T(8,128)(2,1)}, u32[]{:S(2)}) copy-start(bf16[2,32,2048]{2,1,0:T(8,128)(2,1)} %wo_ref.1) | copy-start | bytes 786436
  71.8 37.8 %copy-start.5 = (bf16[2,2048,16]{1,2,0:T(8,128)(2,1)S(1)}, bf16[2,2048,16]{1,2,0:T(8,128)(2,1)}, u32[]{:S(2)}) copy-start(bf16[2,2048,16]{1,2,0:T(8,128)(2,1)} %param.18) | copy-start | bytes 393220
  71.8 37.8 %copy-start.6 = (f32[2,64,32]{1,2,0:T(8,128)S(1)}, f32[2,64,32]{1,2,0:T(8,128)}, u32[]{:S(2)}) copy-start(f32[2,64,32]{1,2,0:T(8,128)} %param.22) | copy-start | bytes 49156
  71.8 37.8 %copy-start.7 = (f32[2,2048]{1,0:T(2,128)S(1)}, f32[2,2048]{1,0:T(2,128)}, u32[]{:S(2)}) copy-start(f32[2,2048]{1,0:T(2,128)} %gain_ref.1) | copy-start | bytes 49156
  71.8 37.8 %copy-start.8 = (f32[2,64,8]{1,2,0:T(8,128)S(1)}, f32[2,64,8]{1,2,0:T(8,128)}, u32[]{:S(2)}) copy-start(f32[2,64,8]{1,2,0:T(8,128)} %param.23) | copy-start | bytes 12292
  71.9 37.8 %copy-start.9 = (f32[2,8]{1,0:T(2,128)S(1)}, f32[2,8]{1,0:T(2,128)}, u32[]{:S(2)}) copy-start(f32[2,8]{1,0:T(2,128)} %rest_0_.1) | copy-start | bytes 196
  71.9 3.5 %collective-permute-start.2 = (bf16[256,128]{1,0:T(8,128)(2,1)S(1)}, bf16[256,128]{1,0:T(8,128)(2,1)S(1)}, u32[]{:S(2)}, u32[]{:S(2)}) collective-permute-start(bf16[256,128]{1,0:T(8,128)(2,1)S(1)} %collective-permute-done.1.second_ref), channel_id=1, source_target_pairs={{0,1},{1,0},{2,3},{3,2},{4,5},{5,4},{6,7},{7,6},{8,9},{9,8},{10,11... | collective-permute-start | bytes 196616 | tf_op jit(solution)/shard_map/ppermute | solution.py:34
  101.3 4.8 %collective-permute-start.4 = (bf16[256,128]{1,0:T(8,128)(2,1)S(1)}, bf16[256,128]{1,0:T(8,128)(2,1)S(1)}, u32[]{:S(2)}, u32[]{:S(2)}) collective-permute-start(bf16[256,128]{1,0:T(8,128)(2,1)S(1)} %bitcast.13), channel_id=1, source_target_pairs={{0,2},{1,3},{2,0},{3,1},{4,6},{5,7},{6,4},{7,5},{8,10},{9,11},{10,... | collective-permute-start | bytes 196616 | tf_op jit(solution)/shard_map/ppermute | solution.py:34
  101.3 7.5 %collective-permute-start.3 = (bf16[256,128]{1,0:T(8,128)(2,1)S(1)}, bf16[256,128]{1,0:T(8,128)(2,1)S(1)}, u32[]{:S(2)}, u32[]{:S(2)}) collective-permute-start(bf16[256,128]{1,0:T(8,128)(2,1)S(1)} %bitcast.14), channel_id=1, source_target_pairs={{0,1},{1,0},{2,3},{3,2},{4,5},{5,4},{6,7},{7,6},{8,9},{9,8},{10,11... | collective-permute-start | bytes 196616 | tf_op jit(solution)/shard_map/ppermute | solution.py:34
  106.1 3.5 %collective-permute-start.5 = (bf16[256,128]{1,0:T(8,128)(2,1)S(1)}, bf16[256,128]{1,0:T(8,128)(2,1)S(1)}, u32[]{:S(2)}, u32[]{:S(2)}) collective-permute-start(bf16[256,128]{1,0:T(8,128)(2,1)S(1)} %collective-permute-done.4.second_ref), channel_id=1, source_target_pairs={{0,1},{1,0},{2,3},{3,2},{4,5},{5,4},{6,7},{7,6},{8,9},{9,8},{10,11... | collective-permute-start | bytes 196616 | tf_op jit(solution)/shard_map/ppermute | solution.py:34
  146.4 5.8 %collective-permute-start.7 = (bf16[256,128]{1,0:T(8,128)(2,1)S(1)}, bf16[256,128]{1,0:T(8,128)(2,1)S(1)}, u32[]{:S(2)}, u32[]{:S(2)}) collective-permute-start(bf16[256,128]{1,0:T(8,128)(2,1)S(1)} %bitcast.9), channel_id=1, source_target_pairs={{0,2},{1,3},{2,0},{3,1},{4,6},{5,7},{6,4},{7,5},{8,10},{9,11},{10,... | collective-permute-start | bytes 196616 | tf_op jit(solution)/shard_map/ppermute | solution.py:34
  146.6 7.6 %collective-permute-start.6 = (bf16[256,128]{1,0:T(8,128)(2,1)S(1)}, bf16[256,128]{1,0:T(8,128)(2,1)S(1)}, u32[]{:S(2)}, u32[]{:S(2)}) collective-permute-start(bf16[256,128]{1,0:T(8,128)(2,1)S(1)} %bitcast.10), channel_id=1, source_target_pairs={{0,1},{1,0},{2,3},{3,2},{4,5},{5,4},{6,7},{7,6},{8,9},{9,8},{10,11... | collective-permute-start | bytes 196616 | tf_op jit(solution)/shard_map/ppermute | solution.py:34
  152.2 2.9 %collective-permute-start.8 = (bf16[256,128]{1,0:T(8,128)(2,1)S(1)}, bf16[256,128]{1,0:T(8,128)(2,1)S(1)}, u32[]{:S(2)}, u32[]{:S(2)}) collective-permute-start(bf16[256,128]{1,0:T(8,128)(2,1)S(1)} %collective-permute-done.7.second_ref), channel_id=1, source_target_pairs={{0,1},{1,0},{2,3},{3,2},{4,5},{5,4},{6,7},{7,6},{8,9},{9,8},{10,11... | collective-permute-start | bytes 196616 | tf_op jit(solution)/shard_map/ppermute | solution.py:34

commit v6 on v5

--- a/solution.py
+++ b/solution.py
@@ -39,11 +39,11 @@
     far = exchanged(copies, far_groups(lax.axis_size("tp"), NEAR))
     own = far.reshape(count * rows, lanes)
     second = from_partner(own, 2)
+    third = from_partner(own, 3)
     first = from_partner(own, 1)
     made = None
     if meanwhile is not None:
-        second, made = lax.optimization_barrier((second, meanwhile(own)))
-    third = from_partner(second, 1)
+        first, second, third, made = lax.optimization_barrier((first, second, third, meanwhile(own)))
     return (own, first, second, third), made
 
 

time: 156 us -> 155 us (level)
  starting transfers between devices: 17.4 us -> 14.4 us
    ppermute x9, starting transfers between devices: 17.4 us -> 14.4 us  [from_partner(): return lax.ppermute(value, 'tp', pairs)]
  transfers between devices with their start and end apart: 9 -> 9, of which waited for: 3 -> 3; matrix products, arithmetic and copies ran while one was open for 0% -> 0% of each run, Pallas kernels for 3% -> 4%
where the time goes in v6:
time: 155 us
  blocking collectives  123 us (79%)
  starting transfers between devices  14.4 us (9%)
  Pallas kernels  11.9 us (8%)
  waiting for transfers between devices  4.06 us (3%)
    all_to_all x5, blocking collectives, exchanged(): lax.all_to_all(copies, 'tp', 0, 0, tiled=True, axis_index_groups=groups)  123 us
    ppermute x9, starting transfers between devices, from_partner(): return lax.ppermute(value, 'tp', pairs)  14.4 us
    ppermute x9, waiting for transfers between devices, from_partner(): return lax.ppermute(value, 'tp', pairs)  4.06 us
    pallas_call x2, Pallas kernels, update(): pl.pallas_call(functools.partial(update_kernel, layer, len(small) // 2),...  3.9 us
  transfers between devices with their start and end apart: 9, of which 3 were waited for; matrix products, arithmetic and copies ran while one was open for 0% of the time, Pallas kernels for 4%

profile of v6, /device:TPU:37, one launch (start us, length us, event | category | flops | bytes accessed | tf_op | source)
XLA Modules:
  0.0 154.8 jit_solution(12920307601181076792)
XLA Ops:
  0.6 2.2 %front_first.1 = (bf16[8,48,128]{2,1,0:T(8,128)(2,1)S(1)}, f32[32,64]{1,0:T(8,128)S(1)}, f32[32,64]{1,0:T(8,128)S(1)}, f32[8,128]{1,0:T(8,128)S(1)}, f32[32,64]{...) custom-call(f32[2,64,32,256]{3,2,1,0:T(8,128)} %cell_ref.3, ...), custom_call_target="tpu_custom_call" | custom-call | tf_op jit(solution)/shard_map/front_first/pallas_call | solution.py:223
  2.9 28.3 %all_to_all.25.everyone_ref = bf16[8,48,128]{2,1,0:T(8,128)(2,1)S(1)} all-to-all(bf16[8,48,128]{2,1,0:T(8,128)(2,1)S(1)} %get-tuple-element.37), channel_id=1, replica_groups={{0,1,2,3,4,5,6,7},{8,9,10,11,12,13,14,15},{16,17,18,19,20,21,22,23},{24..., dimensions={0} | all-to-all | bytes 196608 | tf_op jit(solution)/shard_map/all_to_all | solution.py:29
  31.1 0.0 copy-start.4
  31.1 0.7 read.2
  31.9 34.8 %all_to_all.26 = bf16[16,16,128]{2,1,0:T(8,128)(2,1)S(1)} all-to-all(bf16[16,16,128]{2,1,0:T(8,128)(2,1)S(1)} %read.2), channel_id=1, replica_groups={{0,4,8,12,16,20,24,28,32,36,40,44,48,52,56,60},{1,5,9,13,17,21,25,29,33..., dimensions={0} | all-to-all | bytes 131072 | tf_op jit(solution)/shard_map/all_to_all | solution.py:29
  66.7 2.9 %collective-permute-start.2 = (bf16[256,128]{1,0:T(8,128)(2,1)S(1)}, bf16[256,128]{1,0:T(8,128)(2,1)S(1)}, u32[]{:S(2)}, u32[]{:S(2)}) collective-permute-start(bf16[256,128]{1,0:T(8,128)(2,1)S(1)} %bitcast.19), channel_id=1, source_target_pairs={{0,3},{1,2},{2,1},{3,0},{4,7},{5,6},{6,5},{7,4},{8,11},{9,10},{10,... | collective-permute-start | bytes 196616 | tf_op jit(solution)/shard_map/ppermute | solution.py:34
  69.6 2.0 %collective-permute-start.1 = (bf16[256,128]{1,0:T(8,128)(2,1)S(1)}, bf16[256,128]{1,0:T(8,128)(2,1)S(1)}, u32[]{:S(2)}, u32[]{:S(2)}) collective-permute-start(bf16[256,128]{1,0:T(8,128)(2,1)S(1)} %bitcast.20), channel_id=1, source_target_pairs={{0,2},{1,3},{2,0},{3,1},{4,6},{5,7},{6,4},{7,5},{8,10},{9,11},{10,... | collective-permute-start | bytes 196616 | tf_op jit(solution)/shard_map/ppermute | solution.py:34
  71.5 0.0 collective-permute-start
  71.5 1.5 %fetch.1.cell_ref.held_ref = f32[64,32,256]{2,1,0:T(8,128)S(1)} custom-call(f32[2,64,32,256]{3,2,1,0:T(8,128)} %cell_ref.3, bf16[256,128]{1,0:T(8,128)(2,1)S(1)} %bitcast.22), custom_call_target="tpu_custom_call" | custom-call | tf_op jit(solution)/shard_map/fetch/pallas_call | solution.py:196
  73.1 0.0 copy-start
  73.1 0.0 copy-start.1
  73.1 0.0 copy-start.2
  73.1 0.0 copy-start.3
  73.2 0.0 copy-start.5
  73.2 0.0 copy-start.6
  73.2 0.0 copy-start.7
  73.2 0.0 copy-start.8
  73.2 0.0 copy-start.9
  73.2 0.0 collective-permute-done.2.third_ref
  73.2 1.5 collective-permute-done.1.second_ref
  74.8 0.0 collective-permute-done.first_ref
  74.8 0.0 copy-done.4
  74.8 0.5 proj.2
  75.3 25.4 %all_to_all.27 = bf16[16,16,128]{2,1,0:T(8,128)(2,1)S(1)} all-to-all(bf16[16,16,128]{2,1,0:T(8,128)(2,1)S(1)} %get-tuple-element.46), channel_id=1, replica_groups={{0,4,8,12,16,20,24,28,32,36,40,44,48,52,56,60},{1,5,9,13,17,21,25,29,33..., dimensions={0} | all-to-all | bytes 131072 | tf_op jit(solution)/shard_map/all_to_all | solution.py:29
  100.7 2.5 %collective-permute-start.5 = (bf16[256,128]{1,0:T(8,128)(2,1)S(1)}, bf16[256,128]{1,0:T(8,128)(2,1)S(1)}, u32[]{:S(2)}, u32[]{:S(2)}) collective-permute-start(bf16[256,128]{1,0:T(8,128)(2,1)S(1)} %bitcast.14), channel_id=1, source_target_pairs={{0,3},{1,2},{2,1},{3,0},{4,7},{5,6},{6,5},{7,4},{8,11},{9,10},{10,... | collective-permute-start | bytes 196616 | tf_op jit(solution)/shard_map/ppermute | solution.py:34
  103.2 2.2 %collective-permute-start.4 = (bf16[256,128]{1,0:T(8,128)(2,1)S(1)}, bf16[256,128]{1,0:T(8,128)(2,1)S(1)}, u32[]{:S(2)}, u32[]{:S(2)}) collective-permute-start(bf16[256,128]{1,0:T(8,128)(2,1)S(1)} %bitcast.15), channel_id=1, source_target_pairs={{0,2},{1,3},{2,0},{3,1},{4,6},{5,7},{6,4},{7,5},{8,10},{9,11},{10,... | collective-permute-start | bytes 196616 | tf_op jit(solution)/shard_map/ppermute | solution.py:34
  105.4 0.0 collective-permute-start.3
  105.4 1.6 %update.2.rest_5_ = f32[2,64,32,256]{3,2,1,0:T(8,128)} custom-call(bf16[8,48,128]{2,1,0:T(8,128)(2,1)S(1)} %all_to_all.25.everyone_ref, f32[32,64]{1,0:T(8,128)S(1)} %get-tuple-element.38.value_ref, f32[8,128]{1,0:T(8,128)S(1)} %get-tuple-element.40.rows_ref, f32[64,32,256]{2,1,0:T(8,128)S(1)} %get-tuple-element.41.cell_ref.held_ref, ...), custom_call_target="tpu_custom_call" | custom-call | tf_op jit(solution)/shard_map/update/pallas_call | solution.py:356
  107.0 0.0 collective-permute-done.5.third_ref
  107.0 1.6 %collective-permute-done.4.second_ref = bf16[256,128]{1,0:T(8,128)(2,1)S(1)} collective-permute-done((bf16[256,128]{1,0:T(8,128)(2,1)S(1)}, bf16[256,128]{1,0:T(8,128)(2,1)S(1)}, u32[]{:S(2)}, u32[]{:S(2)}) %collective-permute-start.4) | collective-permute-done | bytes 65568 | tf_op jit(solution)/shard_map/ppermute | solution.py:34
  108.6 0.0 collective-permute-done.3.first_ref
  108.6 0.0 copy-done
  108.6 0.0 copy-done.1
  108.6 0.0 copy-done.2
  108.6 0.0 copy-done.3
  108.6 0.0 copy-done.5
  108.6 0.0 copy-done.6
  108.6 0.0 copy-done.7
  108.7 0.0 copy-done.8
  108.7 0.0 copy-done.9
  108.7 1.3 front_later.1
  110.0 8.9 %all_to_all.28.everyone_ref = bf16[8,48,128]{2,1,0:T(8,128)(2,1)S(1)} all-to-all(bf16[8,48,128]{2,1,0:T(8,128)(2,1)S(1)} %get-tuple-element.50), channel_id=1, replica_groups={{0,1,2,3,4,5,6,7},{8,9,10,11,12,13,14,15},{16,17,18,19,20,21,22,23},{24..., dimensions={0} | all-to-all | bytes 196608 | tf_op jit(solution)/shard_map/all_to_all | solution.py:29
  118.9 0.7 read.3
  119.6 26.0 %all_to_all.29 = bf16[16,16,128]{2,1,0:T(8,128)(2,1)S(1)} all-to-all(bf16[16,16,128]{2,1,0:T(8,128)(2,1)S(1)} %read.3), channel_id=1, replica_groups={{0,4,8,12,16,20,24,28,32,36,40,44,48,52,56,60},{1,5,9,13,17,21,25,29,33..., dimensions={0} | all-to-all | bytes 131072 | tf_op jit(solution)/shard_map/all_to_all | solution.py:29
  145.7 2.9 %collective-permute-start.8 = (bf16[256,128]{1,0:T(8,128)(2,1)S(1)}, bf16[256,128]{1,0:T(8,128)(2,1)S(1)}, u32[]{:S(2)}, u32[]{:S(2)}) collective-permute-start(bf16[256,128]{1,0:T(8,128)(2,1)S(1)} %bitcast.9), channel_id=1, source_target_pairs={{0,3},{1,2},{2,1},{3,0},{4,7},{5,6},{6,5},{7,4},{8,11},{9,10},{10,... | collective-permute-start | bytes 196616 | tf_op jit(solution)/shard_map/ppermute | solution.py:34
  148.5 2.0 %collective-permute-start.7 = (bf16[256,128]{1,0:T(8,128)(2,1)S(1)}, bf16[256,128]{1,0:T(8,128)(2,1)S(1)}, u32[]{:S(2)}, u32[]{:S(2)}) collective-permute-start(bf16[256,128]{1,0:T(8,128)(2,1)S(1)} %bitcast.10), channel_id=1, source_target_pairs={{0,2},{1,3},{2,0},{3,1},{4,6},{5,7},{6,4},{7,5},{8,10},{9,11},{10,... | collective-permute-start | bytes 196616 | tf_op jit(solution)/shard_map/ppermute | solution.py:34
  150.5 0.0 collective-permute-start.6
  150.5 2.3 %update.3 = (f32[2,64,32,256]{3,2,1,0:T(8,128)}, f32[2,32,64]{2,1,0:T(8,128)}, f32[2,8,64]{2,1,0:T(8,128)}) custom-call(bf16[8,48,128]{2,1,0:T(8,128)(2,1)S(1)} %all_to_all.28.everyone_ref, f32[32,64]{1,0:T(8,128)S(1)} %get-tuple-element.51.value_ref, f32[8,128]{1,0:T(8,128)S(1)} %get-tuple-element.53.rows_ref, ...), custom_call_target="tpu_custom_call", output_to_operand_aliasing={{0}: (9, {})} | custom-call | tf_op jit(solution)/shard_map/update/pallas_call | solution.py:356
  152.8 0.0 collective-permute-done.8.third_ref
  152.8 0.9 collective-permute-done.7.second_ref
  153.8 0.0 collective-permute-done.6.first_ref
  153.8 1.0 proj.3
Async XLA Ops:
  31.1 43.6 %copy-start.4 = (bf16[2,32,2048]{2,1,0:T(8,128)(2,1)S(1)}, bf16[2,32,2048]{2,1,0:T(8,128)(2,1)}, u32[]{:S(2)}) copy-start(bf16[2,32,2048]{2,1,0:T(8,128)(2,1)} %weight_ref.3) | copy-start | bytes 786436
  66.7 6.5 %collective-permute-start.2 = (bf16[256,128]{1,0:T(8,128)(2,1)S(1)}, bf16[256,128]{1,0:T(8,128)(2,1)S(1)}, u32[]{:S(2)}, u32[]{:S(2)}) collective-permute-start(bf16[256,128]{1,0:T(8,128)(2,1)S(1)} %bitcast.19), channel_id=1, source_target_pairs={{0,3},{1,2},{2,1},{3,0},{4,7},{5,6},{6,5},{7,4},{8,11},{9,10},{10,... | collective-permute-start | bytes 196616 | tf_op jit(solution)/shard_map/ppermute | solution.py:34
  69.6 5.2 %collective-permute-start.1 = (bf16[256,128]{1,0:T(8,128)(2,1)S(1)}, bf16[256,128]{1,0:T(8,128)(2,1)S(1)}, u32[]{:S(2)}, u32[]{:S(2)}) collective-permute-start(bf16[256,128]{1,0:T(8,128)(2,1)S(1)} %bitcast.20), channel_id=1, source_target_pairs={{0,2},{1,3},{2,0},{3,1},{4,6},{5,7},{6,4},{7,5},{8,10},{9,11},{10,... | collective-permute-start | bytes 196616 | tf_op jit(solution)/shard_map/ppermute | solution.py:34
  71.5 3.2 %collective-permute-start = (bf16[256,128]{1,0:T(8,128)(2,1)S(1)}, bf16[256,128]{1,0:T(8,128)(2,1)S(1)}, u32[]{:S(2)}, u32[]{:S(2)}) collective-permute-start(bf16[256,128]{1,0:T(8,128)(2,1)S(1)} %bitcast.21), channel_id=1, source_target_pairs={{0,1},{1,0},{2,3},{3,2},{4,5},{5,4},{6,7},{7,6},{8,9},{9,8},{10,11... | collective-permute-start | bytes 196616 | tf_op jit(solution)/shard_map/ppermute | solution.py:34
  73.1 35.5 %copy-start = (bf16[2,32,2048]{2,1,0:T(8,128)(2,1)S(1)}, bf16[2,32,2048]{2,1,0:T(8,128)(2,1)}, u32[]{:S(2)}) copy-start(bf16[2,32,2048]{2,1,0:T(8,128)(2,1)} %wq_ref.1) | copy-start | bytes 786436
  73.1 35.5 %copy-start.1 = (bf16[2,32,2048]{2,1,0:T(8,128)(2,1)S(1)}, bf16[2,32,2048]{2,1,0:T(8,128)(2,1)}, u32[]{:S(2)}) copy-start(bf16[2,32,2048]{2,1,0:T(8,128)(2,1)} %wk_ref.1) | copy-start | bytes 786436
  73.1 35.5 %copy-start.2 = (bf16[2,32,2048]{2,1,0:T(8,128)(2,1)S(1)}, bf16[2,32,2048]{2,1,0:T(8,128)(2,1)}, u32[]{:S(2)}) copy-start(bf16[2,32,2048]{2,1,0:T(8,128)(2,1)} %wv_ref.1) | copy-start | bytes 786436
  73.1 35.5 %copy-start.3 = (bf16[2,32,2048]{2,1,0:T(8,128)(2,1)S(1)}, bf16[2,32,2048]{2,1,0:T(8,128)(2,1)}, u32[]{:S(2)}) copy-start(bf16[2,32,2048]{2,1,0:T(8,128)(2,1)} %wo_ref.1) | copy-start | bytes 786436
  73.2 35.5 %copy-start.5 = (bf16[2,2048,16]{1,2,0:T(8,128)(2,1)S(1)}, bf16[2,2048,16]{1,2,0:T(8,128)(2,1)}, u32[]{:S(2)}) copy-start(bf16[2,2048,16]{1,2,0:T(8,128)(2,1)} %param.18) | copy-start | bytes 393220
  73.2 35.5 %copy-start.6 = (f32[2,64,32]{1,2,0:T(8,128)S(1)}, f32[2,64,32]{1,2,0:T(8,128)}, u32[]{:S(2)}) copy-start(f32[2,64,32]{1,2,0:T(8,128)} %param.22) | copy-start | bytes 49156
  73.2 35.5 %copy-start.7 = (f32[2,2048]{1,0:T(2,128)S(1)}, f32[2,2048]{1,0:T(2,128)}, u32[]{:S(2)}) copy-start(f32[2,2048]{1,0:T(2,128)} %gain_ref.1) | copy-start | bytes 49156
  73.2 35.5 %copy-start.8 = (f32[2,64,8]{1,2,0:T(8,128)S(1)}, f32[2,64,8]{1,2,0:T(8,128)}, u32[]{:S(2)}) copy-start(f32[2,64,8]{1,2,0:T(8,128)} %param.23) | copy-start | bytes 12292
  73.2 35.5 %copy-start.9 = (f32[2,8]{1,0:T(2,128)S(1)}, f32[2,8]{1,0:T(2,128)}, u32[]{:S(2)}) copy-start(f32[2,8]{1,0:T(2,128)} %rest_0_.1) | copy-start | bytes 196
  100.7 6.4 %collective-permute-start.5 = (bf16[256,128]{1,0:T(8,128)(2,1)S(1)}, bf16[256,128]{1,0:T(8,128)(2,1)S(1)}, u32[]{:S(2)}, u32[]{:S(2)}) collective-permute-start(bf16[256,128]{1,0:T(8,128)(2,1)S(1)} %bitcast.14), channel_id=1, source_target_pairs={{0,3},{1,2},{2,1},{3,0},{4,7},{5,6},{6,5},{7,4},{8,11},{9,10},{10,... | collective-permute-start | bytes 196616 | tf_op jit(solution)/shard_map/ppermute | solution.py:34
  103.2 5.4 %collective-permute-start.4 = (bf16[256,128]{1,0:T(8,128)(2,1)S(1)}, bf16[256,128]{1,0:T(8,128)(2,1)S(1)}, u32[]{:S(2)}, u32[]{:S(2)}) collective-permute-start(bf16[256,128]{1,0:T(8,128)(2,1)S(1)} %bitcast.15), channel_id=1, source_target_pairs={{0,2},{1,3},{2,0},{3,1},{4,6},{5,7},{6,4},{7,5},{8,10},{9,11},{10,... | collective-permute-start | bytes 196616 | tf_op jit(solution)/shard_map/ppermute | solution.py:34
  105.4 3.2 %collective-permute-start.3 = (bf16[256,128]{1,0:T(8,128)(2,1)S(1)}, bf16[256,128]{1,0:T(8,128)(2,1)S(1)}, u32[]{:S(2)}, u32[]{:S(2)}) collective-permute-start(bf16[256,128]{1,0:T(8,128)(2,1)S(1)} %bitcast.16), channel_id=1, source_target_pairs={{0,1},{1,0},{2,3},{3,2},{4,5},{5,4},{6,7},{7,6},{8,9},{9,8},{10,11... | collective-permute-start | bytes 196616 | tf_op jit(solution)/shard_map/ppermute | solution.py:34
  145.7 7.1 %collective-permute-start.8 = (bf16[256,128]{1,0:T(8,128)(2,1)S(1)}, bf16[256,128]{1,0:T(8,128)(2,1)S(1)}, u32[]{:S(2)}, u32[]{:S(2)}) collective-permute-start(bf16[256,128]{1,0:T(8,128)(2,1)S(1)} %bitcast.9), channel_id=1, source_target_pairs={{0,3},{1,2},{2,1},{3,0},{4,7},{5,6},{6,5},{7,4},{8,11},{9,10},{10,... | collective-permute-start | bytes 196616 | tf_op jit(solution)/shard_map/ppermute | solution.py:34
  148.5 5.2 %collective-permute-start.7 = (bf16[256,128]{1,0:T(8,128)(2,1)S(1)}, bf16[256,128]{1,0:T(8,128)(2,1)S(1)}, u32[]{:S(2)}, u32[]{:S(2)}) collective-permute-start(bf16[256,128]{1,0:T(8,128)(2,1)S(1)} %bitcast.10), channel_id=1, source_target_pairs={{0,2},{1,3},{2,0},{3,1},{4,6},{5,7},{6,4},{7,5},{8,10},{9,11},{10,... | collective-permute-start | bytes 196616 | tf_op jit(solution)/shard_map/ppermute | solution.py:34
  150.5 3.2 %collective-permute-start.6 = (bf16[256,128]{1,0:T(8,128)(2,1)S(1)}, bf16[256,128]{1,0:T(8,128)(2,1)S(1)}, u32[]{:S(2)}, u32[]{:S(2)}) collective-permute-start(bf16[256,128]{1,0:T(8,128)(2,1)S(1)} %bitcast.11), channel_id=1, source_target_pairs={{0,1},{1,0},{2,3},{3,2},{4,5},{5,4},{6,7},{7,6},{8,9},{9,8},{10,11... | collective-permute-start | bytes 196616 | tf_op jit(solution)/shard_map/ppermute | solution.py:34

commit v7 on v6

--- a/solution.py
+++ b/solution.py
@@ -6,6 +6,7 @@
 from jax.experimental import pallas as pl
 from jax.experimental.pallas import tpu as pltpu
 from jax.sharding import PartitionSpec as P
+
 
 EPSILON = 1e-06
 NEAR = 4
@@ -45,14 +46,6 @@
     if meanwhile is not None:
         first, second, third, made = lax.optimization_barrier((first, second, third, meanwhile(own)))
     return (own, first, second, third), made
-
-
-def whole(shape):
-    return pl.BlockSpec(shape, lambda *_: (0,) * len(shape))
-
-
-def one_layer(shape, layer):
-    return pl.BlockSpec((None, *shape), lambda *_: (layer,) + (0,) * len(shape))
 
 
 def anywhere():
@@ -166,7 +159,7 @@
 def later_front(own_ref, first_ref, second_ref, third_ref, gain_ref, wq_ref, wk_ref, wv_ref, wo_ref, wg_ref, *rest, layer, head_size):
     *rest, stage_ref, normed_ref = rest
     unpack((own_ref, first_ref, second_ref, third_ref), stage_ref)
-    far, per, batch = stage_ref.shape
+    far, per, _ = stage_ref.shape
     current = stage_ref[...].astype(F32)
     square = jnp.sum(jnp.sum(current * current, axis=0), axis=0, keepdims=True)
     scale = lax.rsqrt(square / (far * per) + EPSILON)
@@ -336,7 +329,7 @@
 
 
 def update(layer, layers, everyone, value, rows, held, into, small, after):
-    columns, batch = value.shape
+    _, batch = value.shape
     keys = held.shape[-1]
     operands = [everyone, value, rows, held, *small]
     in_specs = [near_vmem()] * len(operands)

time: 155 us -> 155 us (level)
  no operation moved by 1% of the time
where the time goes in v7:
time: 155 us
  blocking collectives  123 us (79%)
  starting transfers between devices  14.4 us (9%)
  Pallas kernels  11.9 us (8%)
  waiting for transfers between devices  4.06 us (3%)
    all_to_all x5, blocking collectives, exchanged(): lax.all_to_all(copies, 'tp', 0, 0, tiled=True, axis_index_groups=groups)  123 us
    ppermute x9, starting transfers between devices, from_partner(): return lax.ppermute(value, 'tp', pairs)  14.4 us
    ppermute x9, waiting for transfers between devices, from_partner(): return lax.ppermute(value, 'tp', pairs)  4.06 us
    pallas_call x2, Pallas kernels, update(): pl.pallas_call(functools.partial(update_kernel, layer, len(small) // 2),...  3.9 us
  transfers between devices with their start and end apart: 9, of which 3 were waited for; matrix products, arithmetic and copies ran while one was open for 0% of the time, Pallas kernels for 4%

profile of v7, /device:TPU:37, one launch (start us, length us, event | category | flops | bytes accessed | tf_op | source)
XLA Modules:
  0.0 154.8 jit_solution(12920307601181076792)
XLA Ops:
  0.6 2.2 %front_first.1 = (bf16[8,48,128]{2,1,0:T(8,128)(2,1)S(1)}, f32[32,64]{1,0:T(8,128)S(1)}, f32[32,64]{1,0:T(8,128)S(1)}, f32[8,128]{1,0:T(8,128)S(1)}, f32[32,64]{...) custom-call(f32[2,64,32,256]{3,2,1,0:T(8,128)} %cell_ref.3, ...), custom_call_target="tpu_custom_call" | custom-call | tf_op jit(solution)/shard_map/front_first/pallas_call | solution.py:216
  2.9 28.3 %all_to_all.25.everyone_ref = bf16[8,48,128]{2,1,0:T(8,128)(2,1)S(1)} all-to-all(bf16[8,48,128]{2,1,0:T(8,128)(2,1)S(1)} %get-tuple-element.37), channel_id=1, replica_groups={{0,1,2,3,4,5,6,7},{8,9,10,11,12,13,14,15},{16,17,18,19,20,21,22,23},{24..., dimensions={0} | all-to-all | bytes 196608 | tf_op jit(solution)/shard_map/all_to_all | solution.py:30
  31.1 0.0 copy-start.4
  31.1 0.7 read.2
  31.9 34.8 %all_to_all.26 = bf16[16,16,128]{2,1,0:T(8,128)(2,1)S(1)} all-to-all(bf16[16,16,128]{2,1,0:T(8,128)(2,1)S(1)} %read.2), channel_id=1, replica_groups={{0,4,8,12,16,20,24,28,32,36,40,44,48,52,56,60},{1,5,9,13,17,21,25,29,33..., dimensions={0} | all-to-all | bytes 131072 | tf_op jit(solution)/shard_map/all_to_all | solution.py:30
  66.7 2.9 %collective-permute-start.2 = (bf16[256,128]{1,0:T(8,128)(2,1)S(1)}, bf16[256,128]{1,0:T(8,128)(2,1)S(1)}, u32[]{:S(2)}, u32[]{:S(2)}) collective-permute-start(bf16[256,128]{1,0:T(8,128)(2,1)S(1)} %bitcast.19), channel_id=1, source_target_pairs={{0,3},{1,2},{2,1},{3,0},{4,7},{5,6},{6,5},{7,4},{8,11},{9,10},{10,... | collective-permute-start | bytes 196616 | tf_op jit(solution)/shard_map/ppermute | solution.py:35
  69.6 2.0 %collective-permute-start.1 = (bf16[256,128]{1,0:T(8,128)(2,1)S(1)}, bf16[256,128]{1,0:T(8,128)(2,1)S(1)}, u32[]{:S(2)}, u32[]{:S(2)}) collective-permute-start(bf16[256,128]{1,0:T(8,128)(2,1)S(1)} %bitcast.20), channel_id=1, source_target_pairs={{0,2},{1,3},{2,0},{3,1},{4,6},{5,7},{6,4},{7,5},{8,10},{9,11},{10,... | collective-permute-start | bytes 196616 | tf_op jit(solution)/shard_map/ppermute | solution.py:35
  71.5 0.0 collective-permute-start
  71.5 1.5 %fetch.1.cell_ref.held_ref = f32[64,32,256]{2,1,0:T(8,128)S(1)} custom-call(f32[2,64,32,256]{3,2,1,0:T(8,128)} %cell_ref.3, bf16[256,128]{1,0:T(8,128)(2,1)S(1)} %bitcast.22), custom_call_target="tpu_custom_call" | custom-call | tf_op jit(solution)/shard_map/fetch/pallas_call | solution.py:189
  73.1 0.0 copy-start
  73.1 0.0 copy-start.1
  73.1 0.0 copy-start.2
  73.1 0.0 copy-start.3
  73.2 0.0 copy-start.5
  73.2 0.0 copy-start.6
  73.2 0.0 copy-start.7
  73.2 0.0 copy-start.8
  73.2 0.0 copy-start.9
  73.2 0.0 collective-permute-done.2.third_ref
  73.2 1.5 collective-permute-done.1.second_ref
  74.8 0.0 collective-permute-done.first_ref
  74.8 0.0 copy-done.4
  74.8 0.5 proj.2
  75.3 25.4 %all_to_all.27 = bf16[16,16,128]{2,1,0:T(8,128)(2,1)S(1)} all-to-all(bf16[16,16,128]{2,1,0:T(8,128)(2,1)S(1)} %get-tuple-element.46), channel_id=1, replica_groups={{0,4,8,12,16,20,24,28,32,36,40,44,48,52,56,60},{1,5,9,13,17,21,25,29,33..., dimensions={0} | all-to-all | bytes 131072 | tf_op jit(solution)/shard_map/all_to_all | solution.py:30
  100.7 2.5 %collective-permute-start.5 = (bf16[256,128]{1,0:T(8,128)(2,1)S(1)}, bf16[256,128]{1,0:T(8,128)(2,1)S(1)}, u32[]{:S(2)}, u32[]{:S(2)}) collective-permute-start(bf16[256,128]{1,0:T(8,128)(2,1)S(1)} %bitcast.14), channel_id=1, source_target_pairs={{0,3},{1,2},{2,1},{3,0},{4,7},{5,6},{6,5},{7,4},{8,11},{9,10},{10,... | collective-permute-start | bytes 196616 | tf_op jit(solution)/shard_map/ppermute | solution.py:35
  103.2 2.2 %collective-permute-start.4 = (bf16[256,128]{1,0:T(8,128)(2,1)S(1)}, bf16[256,128]{1,0:T(8,128)(2,1)S(1)}, u32[]{:S(2)}, u32[]{:S(2)}) collective-permute-start(bf16[256,128]{1,0:T(8,128)(2,1)S(1)} %bitcast.15), channel_id=1, source_target_pairs={{0,2},{1,3},{2,0},{3,1},{4,6},{5,7},{6,4},{7,5},{8,10},{9,11},{10,... | collective-permute-start | bytes 196616 | tf_op jit(solution)/shard_map/ppermute | solution.py:35
  105.4 0.0 collective-permute-start.3
  105.4 1.6 %update.2.rest_5_ = f32[2,64,32,256]{3,2,1,0:T(8,128)} custom-call(bf16[8,48,128]{2,1,0:T(8,128)(2,1)S(1)} %all_to_all.25.everyone_ref, f32[32,64]{1,0:T(8,128)S(1)} %get-tuple-element.38.value_ref, f32[8,128]{1,0:T(8,128)S(1)} %get-tuple-element.40.rows_ref, f32[64,32,256]{2,1,0:T(8,128)S(1)} %get-tuple-element.41.cell_ref.held_ref, ...), custom_call_target="tpu_custom_call" | custom-call | tf_op jit(solution)/shard_map/update/pallas_call | solution.py:349
  107.0 0.0 collective-permute-done.5.third_ref
  107.0 1.6 %collective-permute-done.4.second_ref = bf16[256,128]{1,0:T(8,128)(2,1)S(1)} collective-permute-done((bf16[256,128]{1,0:T(8,128)(2,1)S(1)}, bf16[256,128]{1,0:T(8,128)(2,1)S(1)}, u32[]{:S(2)}, u32[]{:S(2)}) %collective-permute-start.4) | collective-permute-done | bytes 65568 | tf_op jit(solution)/shard_map/ppermute | solution.py:35
  108.6 0.0 collective-permute-done.3.first_ref
  108.6 0.0 copy-done
  108.6 0.0 copy-done.1
  108.6 0.0 copy-done.2
  108.6 0.0 copy-done.3
  108.6 0.0 copy-done.5
  108.6 0.0 copy-done.6
  108.6 0.0 copy-done.7
  108.7 0.0 copy-done.8
  108.7 0.0 copy-done.9
  108.7 1.3 front_later.1
  110.0 8.9 %all_to_all.28.everyone_ref = bf16[8,48,128]{2,1,0:T(8,128)(2,1)S(1)} all-to-all(bf16[8,48,128]{2,1,0:T(8,128)(2,1)S(1)} %get-tuple-element.50), channel_id=1, replica_groups={{0,1,2,3,4,5,6,7},{8,9,10,11,12,13,14,15},{16,17,18,19,20,21,22,23},{24..., dimensions={0} | all-to-all | bytes 196608 | tf_op jit(solution)/shard_map/all_to_all | solution.py:30
  118.9 0.7 read.3
  119.6 26.0 %all_to_all.29 = bf16[16,16,128]{2,1,0:T(8,128)(2,1)S(1)} all-to-all(bf16[16,16,128]{2,1,0:T(8,128)(2,1)S(1)} %read.3), channel_id=1, replica_groups={{0,4,8,12,16,20,24,28,32,36,40,44,48,52,56,60},{1,5,9,13,17,21,25,29,33..., dimensions={0} | all-to-all | bytes 131072 | tf_op jit(solution)/shard_map/all_to_all | solution.py:30
  145.7 2.9 %collective-permute-start.8 = (bf16[256,128]{1,0:T(8,128)(2,1)S(1)}, bf16[256,128]{1,0:T(8,128)(2,1)S(1)}, u32[]{:S(2)}, u32[]{:S(2)}) collective-permute-start(bf16[256,128]{1,0:T(8,128)(2,1)S(1)} %bitcast.9), channel_id=1, source_target_pairs={{0,3},{1,2},{2,1},{3,0},{4,7},{5,6},{6,5},{7,4},{8,11},{9,10},{10,... | collective-permute-start | bytes 196616 | tf_op jit(solution)/shard_map/ppermute | solution.py:35
  148.5 2.0 %collective-permute-start.7 = (bf16[256,128]{1,0:T(8,128)(2,1)S(1)}, bf16[256,128]{1,0:T(8,128)(2,1)S(1)}, u32[]{:S(2)}, u32[]{:S(2)}) collective-permute-start(bf16[256,128]{1,0:T(8,128)(2,1)S(1)} %bitcast.10), channel_id=1, source_target_pairs={{0,2},{1,3},{2,0},{3,1},{4,6},{5,7},{6,4},{7,5},{8,10},{9,11},{10,... | collective-permute-start | bytes 196616 | tf_op jit(solution)/shard_map/ppermute | solution.py:35
  150.5 0.0 collective-permute-start.6
  150.5 2.3 %update.3 = (f32[2,64,32,256]{3,2,1,0:T(8,128)}, f32[2,32,64]{2,1,0:T(8,128)}, f32[2,8,64]{2,1,0:T(8,128)}) custom-call(bf16[8,48,128]{2,1,0:T(8,128)(2,1)S(1)} %all_to_all.28.everyone_ref, f32[32,64]{1,0:T(8,128)S(1)} %get-tuple-element.51.value_ref, f32[8,128]{1,0:T(8,128)S(1)} %get-tuple-element.53.rows_ref, ...), custom_call_target="tpu_custom_call", output_to_operand_aliasing={{0}: (9, {})} | custom-call | tf_op jit(solution)/shard_map/update/pallas_call | solution.py:349
  152.8 0.0 collective-permute-done.8.third_ref
  152.8 0.9 collective-permute-done.7.second_ref
  153.8 0.0 collective-permute-done.6.first_ref
  153.8 1.0 proj.3
Async XLA Ops:
  31.1 43.6 %copy-start.4 = (bf16[2,32,2048]{2,1,0:T(8,128)(2,1)S(1)}, bf16[2,32,2048]{2,1,0:T(8,128)(2,1)}, u32[]{:S(2)}) copy-start(bf16[2,32,2048]{2,1,0:T(8,128)(2,1)} %weight_ref.3) | copy-start | bytes 786436
  66.7 6.5 %collective-permute-start.2 = (bf16[256,128]{1,0:T(8,128)(2,1)S(1)}, bf16[256,128]{1,0:T(8,128)(2,1)S(1)}, u32[]{:S(2)}, u32[]{:S(2)}) collective-permute-start(bf16[256,128]{1,0:T(8,128)(2,1)S(1)} %bitcast.19), channel_id=1, source_target_pairs={{0,3},{1,2},{2,1},{3,0},{4,7},{5,6},{6,5},{7,4},{8,11},{9,10},{10,... | collective-permute-start | bytes 196616 | tf_op jit(solution)/shard_map/ppermute | solution.py:35
  69.6 5.2 %collective-permute-start.1 = (bf16[256,128]{1,0:T(8,128)(2,1)S(1)}, bf16[256,128]{1,0:T(8,128)(2,1)S(1)}, u32[]{:S(2)}, u32[]{:S(2)}) collective-permute-start(bf16[256,128]{1,0:T(8,128)(2,1)S(1)} %bitcast.20), channel_id=1, source_target_pairs={{0,2},{1,3},{2,0},{3,1},{4,6},{5,7},{6,4},{7,5},{8,10},{9,11},{10,... | collective-permute-start | bytes 196616 | tf_op jit(solution)/shard_map/ppermute | solution.py:35
  71.5 3.2 %collective-permute-start = (bf16[256,128]{1,0:T(8,128)(2,1)S(1)}, bf16[256,128]{1,0:T(8,128)(2,1)S(1)}, u32[]{:S(2)}, u32[]{:S(2)}) collective-permute-start(bf16[256,128]{1,0:T(8,128)(2,1)S(1)} %bitcast.21), channel_id=1, source_target_pairs={{0,1},{1,0},{2,3},{3,2},{4,5},{5,4},{6,7},{7,6},{8,9},{9,8},{10,11... | collective-permute-start | bytes 196616 | tf_op jit(solution)/shard_map/ppermute | solution.py:35
  73.1 35.5 %copy-start = (bf16[2,32,2048]{2,1,0:T(8,128)(2,1)S(1)}, bf16[2,32,2048]{2,1,0:T(8,128)(2,1)}, u32[]{:S(2)}) copy-start(bf16[2,32,2048]{2,1,0:T(8,128)(2,1)} %wq_ref.1) | copy-start | bytes 786436
  73.1 35.5 %copy-start.1 = (bf16[2,32,2048]{2,1,0:T(8,128)(2,1)S(1)}, bf16[2,32,2048]{2,1,0:T(8,128)(2,1)}, u32[]{:S(2)}) copy-start(bf16[2,32,2048]{2,1,0:T(8,128)(2,1)} %wk_ref.1) | copy-start | bytes 786436
  73.1 35.5 %copy-start.2 = (bf16[2,32,2048]{2,1,0:T(8,128)(2,1)S(1)}, bf16[2,32,2048]{2,1,0:T(8,128)(2,1)}, u32[]{:S(2)}) copy-start(bf16[2,32,2048]{2,1,0:T(8,128)(2,1)} %wv_ref.1) | copy-start | bytes 786436
  73.1 35.5 %copy-start.3 = (bf16[2,32,2048]{2,1,0:T(8,128)(2,1)S(1)}, bf16[2,32,2048]{2,1,0:T(8,128)(2,1)}, u32[]{:S(2)}) copy-start(bf16[2,32,2048]{2,1,0:T(8,128)(2,1)} %wo_ref.1) | copy-start | bytes 786436
  73.2 35.5 %copy-start.5 = (bf16[2,2048,16]{1,2,0:T(8,128)(2,1)S(1)}, bf16[2,2048,16]{1,2,0:T(8,128)(2,1)}, u32[]{:S(2)}) copy-start(bf16[2,2048,16]{1,2,0:T(8,128)(2,1)} %param.18) | copy-start | bytes 393220
  73.2 35.5 %copy-start.6 = (f32[2,64,32]{1,2,0:T(8,128)S(1)}, f32[2,64,32]{1,2,0:T(8,128)}, u32[]{:S(2)}) copy-start(f32[2,64,32]{1,2,0:T(8,128)} %param.22) | copy-start | bytes 49156
  73.2 35.5 %copy-start.7 = (f32[2,2048]{1,0:T(2,128)S(1)}, f32[2,2048]{1,0:T(2,128)}, u32[]{:S(2)}) copy-start(f32[2,2048]{1,0:T(2,128)} %gain_ref.1) | copy-start | bytes 49156
  73.2 35.5 %copy-start.8 = (f32[2,64,8]{1,2,0:T(8,128)S(1)}, f32[2,64,8]{1,2,0:T(8,128)}, u32[]{:S(2)}) copy-start(f32[2,64,8]{1,2,0:T(8,128)} %param.23) | copy-start | bytes 12292
  73.2 35.5 %copy-start.9 = (f32[2,8]{1,0:T(2,128)S(1)}, f32[2,8]{1,0:T(2,128)}, u32[]{:S(2)}) copy-start(f32[2,8]{1,0:T(2,128)} %rest_0_.1) | copy-start | bytes 196
  100.7 6.4 %collective-permute-start.5 = (bf16[256,128]{1,0:T(8,128)(2,1)S(1)}, bf16[256,128]{1,0:T(8,128)(2,1)S(1)}, u32[]{:S(2)}, u32[]{:S(2)}) collective-permute-start(bf16[256,128]{1,0:T(8,128)(2,1)S(1)} %bitcast.14), channel_id=1, source_target_pairs={{0,3},{1,2},{2,1},{3,0},{4,7},{5,6},{6,5},{7,4},{8,11},{9,10},{10,... | collective-permute-start | bytes 196616 | tf_op jit(solution)/shard_map/ppermute | solution.py:35
  103.2 5.4 %collective-permute-start.4 = (bf16[256,128]{1,0:T(8,128)(2,1)S(1)}, bf16[256,128]{1,0:T(8,128)(2,1)S(1)}, u32[]{:S(2)}, u32[]{:S(2)}) collective-permute-start(bf16[256,128]{1,0:T(8,128)(2,1)S(1)} %bitcast.15), channel_id=1, source_target_pairs={{0,2},{1,3},{2,0},{3,1},{4,6},{5,7},{6,4},{7,5},{8,10},{9,11},{10,... | collective-permute-start | bytes 196616 | tf_op jit(solution)/shard_map/ppermute | solution.py:35
  105.4 3.2 %collective-permute-start.3 = (bf16[256,128]{1,0:T(8,128)(2,1)S(1)}, bf16[256,128]{1,0:T(8,128)(2,1)S(1)}, u32[]{:S(2)}, u32[]{:S(2)}) collective-permute-start(bf16[256,128]{1,0:T(8,128)(2,1)S(1)} %bitcast.16), channel_id=1, source_target_pairs={{0,1},{1,0},{2,3},{3,2},{4,5},{5,4},{6,7},{7,6},{8,9},{9,8},{10,11... | collective-permute-start | bytes 196616 | tf_op jit(solution)/shard_map/ppermute | solution.py:35
  145.7 7.1 %collective-permute-start.8 = (bf16[256,128]{1,0:T(8,128)(2,1)S(1)}, bf16[256,128]{1,0:T(8,128)(2,1)S(1)}, u32[]{:S(2)}, u32[]{:S(2)}) collective-permute-start(bf16[256,128]{1,0:T(8,128)(2,1)S(1)} %bitcast.9), channel_id=1, source_target_pairs={{0,3},{1,2},{2,1},{3,0},{4,7},{5,6},{6,5},{7,4},{8,11},{9,10},{10,... | collective-permute-start | bytes 196616 | tf_op jit(solution)/shard_map/ppermute | solution.py:35
  148.5 5.2 %collective-permute-start.7 = (bf16[256,128]{1,0:T(8,128)(2,1)S(1)}, bf16[256,128]{1,0:T(8,128)(2,1)S(1)}, u32[]{:S(2)}, u32[]{:S(2)}) collective-permute-start(bf16[256,128]{1,0:T(8,128)(2,1)S(1)} %bitcast.10), channel_id=1, source_target_pairs={{0,2},{1,3},{2,0},{3,1},{4,6},{5,7},{6,4},{7,5},{8,10},{9,11},{10,... | collective-permute-start | bytes 196616 | tf_op jit(solution)/shard_map/ppermute | solution.py:35
  150.5 3.2 %collective-permute-start.6 = (bf16[256,128]{1,0:T(8,128)(2,1)S(1)}, bf16[256,128]{1,0:T(8,128)(2,1)S(1)}, u32[]{:S(2)}, u32[]{:S(2)}) collective-permute-start(bf16[256,128]{1,0:T(8,128)(2,1)S(1)} %bitcast.11), channel_id=1, source_target_pairs={{0,1},{1,0},{2,3},{3,2},{4,5},{5,4},{6,7},{7,6},{8,9},{9,8},{10,11... | collective-permute-start | bytes 196616 | tf_op jit(solution)/shard_map/ppermute | solution.py:35
